TPU v7x, 32 devices: a whole 2x2x4 slice. The times are simulated.
32 devices in a mesh: sp: 16 (over z, y, core), tp: 2 (over x).
Axes of the slice: x: 2, y: 2, z: 4, core: 2. Of those that a mesh axis runs over, the one named last changes fastest.
Arguments:
- target: bfloat16 [2048, 2048], P('sp'), may hold values from -0.375 to 0.375
- source: bfloat16 [4096, 2048], P(('sp', 'tp')), may hold values from -0.375 to 0.375
- target_gain: float32 [2048], replicated, may hold values from 0.3 to 12
- source_gain: float32 [2048], replicated, may hold values from 0.3 to 12
- w_query: bfloat16 [2048, 1024], P(None, 'tp'), may hold values from -0.125 to 0.125
- w_key: bfloat16 [2048, 256], replicated, may hold values from -0.125 to 0.125
- w_value: bfloat16 [2048, 256], replicated, may hold values from -0.125 to 0.125
- attended: bfloat16 [2048, 1024], P('sp', 'tp'), may hold values from -6 to 6
- d_attended: bfloat16 [2048, 1024], P('sp', 'tp'), may hold values from -24 to 24
Outputs:
- d_target: bfloat16 [2048, 2048], P('sp')
- d_source: float32 [4096, 2048], P(('sp', 'tp'))
- d_w_query: float32 [2048, 1024], P('sp', 'tp')
All inputs are finite; a program needn't handle non-finite values.
Results may differ from a plain program's by a relative error of at most 0.02.
The roundings to bfloat16 on the way count: a program that leaves them out, or rounds other values in their place, can miss the bound.
Values may be sent and summed in bfloat16 or wider, within the bound.
No kernel may reach another device: no remote copies, remote signals or barrier semaphores. Data moves between devices by JAX's collectives and lax.ppermute only.
A program may use at most 64 MiB of HBM per device.

v0:
```python
import jax
import jax.numpy as jnp
from jax import lax
from jax.sharding import PartitionSpec as P

KVH = 2
HD = 128


EPS = 1e-06


def merged(shard, axis, combine):
    everything = jax.tree.map(lambda part: lax.all_gather(part, axis), shard)
    leading = jax.tree.map(lambda part: part[0], everything)

    def turn(k, so_far):
        return combine(so_far, jax.tree.map(lambda part: part[k], everything))

    return lax.fori_loop(1, lax.axis_size(axis), turn, leading)


def norm_rows(matrix, gain_vector):
    widened = matrix.astype(jnp.float32)
    inverse = lax.rsqrt(jnp.mean(widened * widened, axis=-1, keepdims=True) + EPS)
    return widened * inverse * gain_vector


def norm_back(matrix, gain_vector, cotangent):
    _, pullback = jax.vjp(lambda values: norm_rows(values, gain_vector), matrix.astype(jnp.float32))
    return pullback(cotangent)[0]


def block_count(row_count, most_rows):
    number = 1
    while row_count % (number * 2) == 0 and row_count // number > most_rows:
        number = number * 2
    return number


def merge_totals(earlier, latter):
    maxima = jnp.maximum(earlier[0], latter[0])
    totals = earlier[1] * jnp.exp(earlier[0] - maxima) + latter[1] * jnp.exp(latter[0] - maxima)
    return (maxima, totals)


def block_totals(queries, key_head, scaling):
    row_count = queries.shape[0]
    per_head = queries.reshape(row_count, -1, key_head.shape[1])
    scores = (
        jnp.einsum("rhd,sd->rhs", per_head, key_head, preferred_element_type=jnp.float32) * scaling
    )
    maxima = jnp.max(scores, axis=-1)
    totals = jnp.sum(jnp.exp(scores - maxima[..., None]), axis=-1)
    return (maxima, totals)


def score_grads(query_heads, grad_heads, delta_rows, log_total, key_head, value_head, scaling):
    scores = (
        jnp.einsum("rhd,sd->rhs", query_heads, key_head, preferred_element_type=jnp.float32)
        * scaling
    )
    weights = jnp.exp(scores - log_total[..., None])
    d_weights = jnp.einsum(
        "rhd,sd->rhs", grad_heads, value_head, preferred_element_type=jnp.float32
    )
    d_scores = (weights * (d_weights - delta_rows.astype(jnp.float32)[..., None])).astype(
        jnp.bfloat16
    )
    return (weights, d_scores)


def gradient_block(carried, blocks, key_head, value_head, scaling):
    key_acc, value_acc = carried
    queries, cotangent, delta_rows, log_total = blocks
    row_count = queries.shape[0]
    head_dim = key_head.shape[1]
    query_heads = queries.reshape(row_count, -1, head_dim)
    grad_heads = cotangent.reshape(row_count, -1, head_dim)
    weights, d_scores = score_grads(
        query_heads, grad_heads, delta_rows, log_total, key_head, value_head, scaling
    )
    key_acc = (
        key_acc
        + jnp.einsum("rhs,rhd->sd", d_scores, query_heads, preferred_element_type=jnp.float32)
        * scaling
    )
    value_acc = value_acc + jnp.einsum(
        "rhs,rhd->sd", weights.astype(jnp.bfloat16), grad_heads, preferred_element_type=jnp.float32
    )
    return ((key_acc, value_acc), None)


def local(target, source, target_gain, source_gain, w_query, w_key, w_value, attended, d_attended):
    tp_size = lax.axis_size("tp")
    local_rows = target.shape[0]
    source_rows = source.shape[0]
    query_width = w_query.shape[1]
    scaling = HD ** (-0.5)
    normed_target = norm_rows(target, target_gain).astype(jnp.bfloat16)
    normed_source = norm_rows(source, source_gain).astype(jnp.bfloat16)
    query = jnp.dot(normed_target, w_query, preferred_element_type=jnp.float32).astype(jnp.bfloat16)
    key_own = jnp.dot(normed_source, w_key, preferred_element_type=jnp.float32).astype(jnp.bfloat16)
    value_own = jnp.dot(normed_source, w_value, preferred_element_type=jnp.float32).astype(
        jnp.bfloat16
    )
    key_block, value_block = (
        lax.all_gather(key_own, "tp", axis=0, tiled=True),
        lax.all_gather(value_own, "tp", axis=0, tiled=True),
    )
    group_size = tp_size // KVH
    kv_index = lax.axis_index("tp") // group_size
    key_head = lax.dynamic_slice_in_dim(key_block, kv_index * HD, HD, 1)
    value_head = lax.dynamic_slice_in_dim(value_block, kv_index * HD, HD, 1)
    delta = jnp.einsum(
        "rhd,rhd->rh",
        d_attended.reshape(local_rows, -1, HD),
        attended.reshape(local_rows, -1, HD),
        preferred_element_type=jnp.float32,
    ).astype(jnp.bfloat16)
    all_queries = lax.all_gather(query, "sp", axis=0, tiled=True)
    target_total = all_queries.shape[0]
    number = block_count(target_total, 512)
    maxima, totals = lax.map(
        lambda blocked: block_totals(blocked, key_head, scaling),
        all_queries.reshape(number, target_total // number, query_width),
    )
    maxima = maxima.reshape(target_total, -1)
    totals = totals.reshape(target_total, -1)
    maxima, totals = merged((maxima, totals), "sp", merge_totals)
    log_total = maxima + jnp.log(totals)
    block_rows = key_head.shape[0]
    start_state = (
        jnp.zeros((block_rows, HD), jnp.float32),
        jnp.zeros((block_rows, HD), jnp.float32),
    )
    key_acc = start_state[0]
    value_acc = start_state[1]
    cotangent = lax.all_gather(d_attended, "sp", axis=0, tiled=True)
    delta_piece = lax.all_gather(delta, "sp", axis=0, tiled=True)
    row_count = cotangent.shape[0]
    pieces_count = block_count(row_count, 512)
    blocked = tuple(
        (
            member.reshape((pieces_count, row_count // pieces_count) + member.shape[1:])
            for member in (all_queries, cotangent, delta_piece, log_total)
        )
    )

    def fold_inner_step(state, blocks):
        return gradient_block(state, blocks, key_head, value_head, scaling)

    (key_acc, value_acc), grad_rows = lax.scan(fold_inner_step, (key_acc, value_acc), blocked)
    folded = (key_acc, value_acc)
    key_acc = folded[0]
    value_acc = folded[1]
    own_totals = lax.dynamic_slice_in_dim(
        log_total, lax.axis_index("sp") * local_rows, local_rows, 0
    )
    own_queries = query.reshape(local_rows, -1, HD)
    own_grads = d_attended.reshape(local_rows, -1, HD)
    query_start = jnp.zeros((local_rows, query_width // HD, HD), jnp.float32)
    keys_piece = lax.all_gather(key_head, "sp", axis=0, tiled=True)
    values_piece = lax.all_gather(value_head, "sp", axis=0, tiled=True)
    row_count = keys_piece.shape[0]
    pieces_count = block_count(row_count, 512)
    key_blocks = keys_piece.reshape(pieces_count, row_count // pieces_count, HD)
    value_blocks = values_piece.reshape(pieces_count, row_count // pieces_count, HD)

    def key_inner_step(state, blocks):
        keys_now, values_now = blocks
        _, d_scores = score_grads(
            own_queries, own_grads, delta, own_totals, keys_now, values_now, scaling
        )
        return (
            state
            + jnp.einsum("rhs,sd->rhd", d_scores, keys_now, preferred_element_type=jnp.float32)
            * scaling,
            None,
        )

    result, _ = lax.scan(key_inner_step, query_start, (key_blocks, value_blocks))
    d_query = result.reshape(local_rows, query_width).astype(jnp.bfloat16)
    d_w_query = lax.psum_scatter(
        jnp.einsum("rd,rc->dc", normed_target, d_query, preferred_element_type=jnp.float32),
        "sp",
        scatter_dimension=0,
        tiled=True,
    )
    partial_value = jnp.einsum("rc,dc->rd", d_query, w_query, preferred_element_type=jnp.float32)
    d_normed = lax.psum(partial_value.astype(jnp.bfloat16), "tp").astype(jnp.float32)
    d_target = norm_back(target, target_gain, d_normed).astype(jnp.bfloat16)
    stacked = jnp.stack([key_acc, value_acc], axis=1).reshape(tp_size, source_rows, 2 * HD)
    returned = lax.all_to_all(
        stacked.astype(jnp.bfloat16), "tp", split_axis=0, concat_axis=0, tiled=True
    ).astype(stacked.dtype)
    grouped = returned.reshape(KVH, group_size, source_rows, 2, HD).sum(axis=1)
    d_key = (
        grouped[:, :, 0, :].transpose(1, 0, 2).reshape(source_rows, KVH * HD).astype(jnp.bfloat16)
    )
    d_value = (
        grouped[:, :, 1, :].transpose(1, 0, 2).reshape(source_rows, KVH * HD).astype(jnp.bfloat16)
    )
    d_normed_source = jnp.einsum(
        "rc,dc->rd", d_key, w_key, preferred_element_type=jnp.float32
    ) + jnp.einsum("rc,dc->rd", d_value, w_value, preferred_element_type=jnp.float32)
    d_source = norm_back(source, source_gain, d_normed_source)
    return (d_target, d_source, d_w_query)


def solution(mesh):
    return jax.shard_map(
        local,
        mesh=mesh,
        in_specs=(
            P("sp", None),
            P(("sp", "tp"), None),
            P(),
            P(),
            P(None, "tp"),
            P(),
            P(),
            P("sp", "tp"),
            P("sp", "tp"),
        ),
        out_specs=(P("sp", None), P(("sp", "tp"), None), P("sp", "tp")),
        check_vma=False,
    )
```

profile of v0, /device:TPU:0, one launch (start us, length us, event | category | flops | bytes accessed | tf_op | source)
XLA Modules:
  0.0 290.3 jit_solution(17529582570570535842)
XLA Ops:
  7.2 1.4 fusion.48
  8.9 2.2 convolution_convert_fusion.1
  12.0 1.6 convolution_convert_fusion.3
  13.6 6.0 %all_gather.27 = bf16[256,256]{1,0:T(8,128)(2,1)S(1)} all-gather(bf16[128,256]{1,0:T(8,128)(2,1)S(1)} %convolution_convert_fusion.3), channel_id=1, replica_groups=mesh['sp'=16,'tp'=2] {'tp'}, dimensions={0}, use_global_device_ids=true | all-gather | bytes 196608 | tf_op jit(solution)/shard_map/all_gather | solution.py:108
  20.3 1.6 convolution_convert_fusion.2
  21.9 4.9 %all_gather.32 = bf16[256,256]{1,0:T(8,128)(2,1)S(1)} all-gather(bf16[128,256]{1,0:T(8,128)(2,1)S(1)} %convolution_convert_fusion.2), channel_id=1, replica_groups=mesh['sp'=16,'tp'=2] {'tp'}, dimensions={0}, use_global_device_ids=true | all-gather | bytes 196608 | tf_op jit(solution)/shard_map/all_gather | solution.py:109
  30.3 25.2 %all-gather.7.cloned.1.call-done = bf16[2048,512]{1,0:T(8,128)(2,1)} async-done(((bf16[128,512]{1,0:T(8,128)(2,1)}), bf16[2048,512]{1,0:T(8,128)(2,1)}) %all-gather.7.cloned.1.call-update) | async-done | bytes 2097168 | tf_op jit(solution)/shard_map/all_gather | solution.py:121
  55.5 4.2 %copy.78 = bf16[4,512,512]{1,2,0:T(8,128)(2,1)} copy(bf16[4,512,512]{2,1,0:T(8,128)(2,1)} %bitcast.167) | data formatting | bytes 4194304 | tf_op jit(solution)/shard_map/while | solution.py:124
  59.7 7.7 %while.53 = (s32[]{:T(128)}, f32[4,512,4]{1,2,0:T(4,128)S(1)}, f32[4,512,4]{1,2,0:T(4,128)S(1)}, bf16[4,512,512]{1,2,0:T(8,128)(2,1)}, bf16[256,128]{1,0:T(8,128)(2,1)S(1)}, /*index=5*/s32[]{:T(128)}) while((s32[]{:T(128)}, f32[4,512,4]{1,2,0:T(4,128)S(1)}, f32[4,512,4]{1,2,0:T(4,128)S(1)}, bf16[4,512,512]{1,2,0:T(8,128)(2,1)}, ...), condition=%wide.region_5.6_spmd, body=%wide.region_2.5_spmd.sunk | while | flops 136835072 | bytes 5890125 | solution.py:124
  67.4 20.9 %all_gather.31 = f32[16,2048,4]{1,2,0:T(4,128)S(1)} all-gather(f32[1,2048,4]{1,2,0:T(4,128)S(1)} %bitcast.179), channel_id=1, replica_groups=mesh['sp'=16,'tp'=2] {'sp'}, dimensions={0}, use_global_device_ids=true | all-gather | bytes 557056 | tf_op jit(solution)/shard_map/all_gather | solution.py:14
  88.3 19.2 %all_gather.30 = f32[16,2048,4]{1,2,0:T(4,128)S(1)} all-gather(f32[1,2048,4]{1,2,0:T(4,128)} %bitcast.178), channel_id=1, replica_groups=mesh['sp'=16,'tp'=2] {'sp'}, dimensions={0}, use_global_device_ids=true | all-gather | bytes 557056 | tf_op jit(solution)/shard_map/all_gather | solution.py:14
  108.7 25.1 %all-gather.9.cloned.1.call-done = bf16[4096,128]{1,0:T(8,128)(2,1)} async-done(((bf16[256,128]{1,0:T(8,128)(2,1)}), bf16[4096,128]{1,0:T(8,128)(2,1)}) %all-gather.9.cloned.1.call-update) | async-done | bytes 1048592 | tf_op jit(solution)/shard_map/all_gather | solution.py:164
  133.7 24.7 %while.55 = (s32[]{:T(128)}, f32[128,4,128]{2,0,1:T(8,128)S(1)}, bf16[8,512,128]{2,1,0:T(8,128)(2,1)}, bf16[128,4,128]{2,0,1:T(8,128)(2,1)}, f32[128,4]{0,1:T(4,...) while((s32[]{:T(128)}, f32[128,4,128]{2,0,1:T(8,128)S(1)}, ...), condition=%wide.region_9.10_spmd.clone, body=%wide.region_8.9_spmd.clone.sunk | while | flops 202834432 | bytes 3285615 | solution.py:182
  135.0 1.8 fusion.104
  136.8 1.3 convolution_subtract_fusion.2
  138.1 1.8 fusion.104
  139.9 1.3 convolution_subtract_fusion.2
  141.2 1.8 fusion.104
  143.0 1.3 convolution_subtract_fusion.2
  144.3 1.8 fusion.104
  146.1 1.3 convolution_subtract_fusion.2
  147.4 1.8 fusion.104
  149.2 1.3 convolution_subtract_fusion.2
  150.5 1.8 fusion.104
  152.3 1.3 convolution_subtract_fusion.2
  153.5 1.8 fusion.104
  156.6 1.8 fusion.104
  158.6 1.6 convolution_convert_fusion
  160.3 19.4 %all_gather.35 = bf16[2048,4]{0,1:T(4,128)(2,1)S(1)} all-gather(bf16[128,4]{0,1:T(4,128)(2,1)S(1)} %get-tuple-element.772), channel_id=1, replica_groups=mesh['sp'=16,'tp'=2] {'sp'}, dimensions={0}, use_global_device_ids=true | all-gather | bytes 17408 | tf_op jit(solution)/shard_map/all_gather | solution.py:140
  179.7 2.7 fusion.52
  183.3 42.9 %while.56 = (s32[]{:T(128)}, f32[256,128]{1,0:T(8,128)}, f32[256,128]{1,0:T(8,128)S(1)}, bf16[4,512,512]{1,2,0:T(8,128)(2,1)}, bf16[256,128]{1,0:T(8,128)(2,1)S(...) while((s32[]{:T(128)}, f32[256,128]{1,0:T(8,128)}, ...), condition=%wide.region_13.14_spmd.clone, body=%wide.region_12.13_spmd.clone.sunk | while | flops 541231104 | bytes 14340260 | solution.py:153
  184.4 1.9 fusion.112
  187.6 3.8 %fusion.113 = f32[256,128]{1,0:T(8,128)} fusion(bf16[512,4,128]{0,2,1:T(8,128)(2,1)} %bitcast.164, f32[512,4,256]{2,0,1:T(8,128)} %fusion.112, bf16[512,4,128]{0,2,1:T(8,128)(2,1)S(1)} %bitcast.161, f32[512,4]{0,1:T(4,128)S(1)} %bitcast_convert_fusion.2, f32[512,4]{0,1:T(4,128)S(1)} %dynamic-slice_bitcast_fusion.2, ...), kind=kOutput, calls=%fused_computation.39.clone.1 | convolution fusion | flops 271155200 | bytes 3489793 | tf_op jit(solution)/shard_map/while/body/eval_jaxpr/rhs,rhd->sd/dot_general | solution.py:85
  191.5 2.4 fusion.114
  195.0 1.9 fusion.112
  198.3 3.9 %fusion.113 = f32[256,128]{1,0:T(8,128)} fusion(bf16[512,4,128]{0,2,1:T(8,128)(2,1)} %bitcast.164, f32[512,4,256]{2,0,1:T(8,128)} %fusion.112, bf16[512,4,128]{0,2,1:T(8,128)(2,1)S(1)} %bitcast.161, f32[512,4]{0,1:T(4,128)S(1)} %bitcast_convert_fusion.2, f32[512,4]{0,1:T(4,128)S(1)} %dynamic-slice_bitcast_fusion.2, ...), kind=kOutput, calls=%fused_computation.39.clone.1 | convolution fusion | flops 271155200 | bytes 3489793 | tf_op jit(solution)/shard_map/while/body/eval_jaxpr/rhs,rhd->sd/dot_general | solution.py:85
  202.2 2.4 fusion.114
  205.7 1.9 fusion.112
  208.9 3.9 %fusion.113 = f32[256,128]{1,0:T(8,128)} fusion(bf16[512,4,128]{0,2,1:T(8,128)(2,1)} %bitcast.164, f32[512,4,256]{2,0,1:T(8,128)} %fusion.112, bf16[512,4,128]{0,2,1:T(8,128)(2,1)S(1)} %bitcast.161, f32[512,4]{0,1:T(4,128)S(1)} %bitcast_convert_fusion.2, f32[512,4]{0,1:T(4,128)S(1)} %dynamic-slice_bitcast_fusion.2, ...), kind=kOutput, calls=%fused_computation.39.clone.1 | convolution fusion | flops 271155200 | bytes 3489793 | tf_op jit(solution)/shard_map/while/body/eval_jaxpr/rhs,rhd->sd/dot_general | solution.py:85
  212.8 2.4 fusion.114
  216.4 1.9 fusion.112
  219.7 4.0 %fusion.113 = f32[256,128]{1,0:T(8,128)} fusion(bf16[512,4,128]{0,2,1:T(8,128)(2,1)} %bitcast.164, f32[512,4,256]{2,0,1:T(8,128)} %fusion.112, bf16[512,4,128]{0,2,1:T(8,128)(2,1)S(1)} %bitcast.161, f32[512,4]{0,1:T(4,128)S(1)} %bitcast_convert_fusion.2, f32[512,4]{0,1:T(4,128)S(1)} %dynamic-slice_bitcast_fusion.2, ...), kind=kOutput, calls=%fused_computation.39.clone.1 | convolution fusion | flops 271155200 | bytes 3489793 | tf_op jit(solution)/shard_map/while/body/eval_jaxpr/rhs,rhd->sd/dot_general | solution.py:85
  223.7 2.5 fusion.114
  227.5 6.9 %all_to_all.5 = bf16[2,128,256]{2,1,0:T(8,128)(2,1)S(1)} all-to-all(bf16[2,128,256]{2,1,0:T(8,128)(2,1)S(1)} %convert_element_type.103), channel_id=1, replica_groups=mesh['sp'=16,'tp'=2] {'tp'}, dimensions={0} | all-to-all | bytes 262144 | tf_op jit(solution)/shard_map/all_to_all | solution.py:194
  234.9 1.8 fusion.60
  238.6 1.3 fusion.51
  239.9 2.2 fusion.43
  242.1 41.4 %reduce-scatter.2.cloned.1.call-done = f32[128,512]{1,0:T(8,128)} async-done(((f32[2048,512]{1,0:T(8,128)}), f32[128,512]{1,0:T(8,128)}) %reduce-scatter.2.cloned.1.call-update) | async-done | bytes 262160 | tf_op jit(solution)/shard_map/reduce_scatter | solution.py:184
  (159 shorter events, 31.5 us)
Async XLA Ops:
  7.2 1.8 copy-start
  7.2 4.0 %copy-start.5 = (bf16[128,2048]{1,0:T(8,128)(2,1)S(1)}, bf16[128,2048]{1,0:T(8,128)(2,1)}, u32[]{:S(2)}) copy-start(bf16[128,2048]{1,0:T(8,128)(2,1)} %param.18) | copy-start | bytes 1572868
  7.2 4.8 %copy-start.14 = (f32[2048]{0:T(1024)S(1)}, f32[2048]{0:T(1024)}, u32[]{:S(2)}) copy-start(f32[2048]{0:T(1024)} %param.20) | copy-start | bytes 24580
  7.2 48.3 %all-gather.7.cloned.1.call-start = ((), (), s32[]{:S(2)}) async-start(), calls=%async_computation.3 | async-start | bytes 2228224 | tf_op jit(solution)/shard_map/all_gather | solution.py:121
  8.6 2.8 copy-start.15
  11.1 97.5 %all-gather.5.cloned.1.call-start = ((), (), s32[]{:S(2)}) async-start(), calls=%async_computation.2 | async-start | bytes 1114112 | tf_op jit(solution)/shard_map/all_gather | solution.py:163
  11.4 0.5 copy-start.19
  11.9 14.9 %copy-start.17 = (f32[128]{0:T(128)}, f32[128]{0:T(128)S(1)}, u32[]{:S(2)}) copy-start(f32[128]{0:T(128)S(1)} %fusion.57) | copy-start | bytes 1540
  11.9 16.2 %copy-start.8 = (bf16[128,512]{1,0:T(8,128)(2,1)S(1)}, bf16[128,512]{1,0:T(8,128)(2,1)}, u32[]{:S(2)}) copy-start(bf16[128,512]{1,0:T(8,128)(2,1)} %param.25) | copy-start | bytes 393220
  12.0 16.3 %copy-start.9 = (bf16[128,512]{1,0:T(8,128)(2,1)S(1)}, bf16[128,512]{1,0:T(8,128)(2,1)}, u32[]{:S(2)}) copy-start(bf16[128,512]{1,0:T(8,128)(2,1)} %convolution_convert_fusion.1) | copy-start | bytes 393220
  13.6 16.3 %copy-start.11 = (bf16[128,512]{1,0:T(8,128)(2,1)S(1)}, bf16[128,512]{1,0:T(8,128)(2,1)}, u32[]{:S(2)}) copy-start(bf16[128,512]{1,0:T(8,128)(2,1)} %param.24) | copy-start | bytes 393220
  20.3 113.5 %all-gather.9.cloned.1.call-start = ((), (), s32[]{:S(2)}) async-start(), calls=%async_computation.4 | async-start | bytes 1114112 | tf_op jit(solution)/shard_map/all_gather | solution.py:164
  27.5 155.0 %all-gather.11.cloned.1.call-start = ((), (), s32[]{:S(2)}) async-start(), calls=%async_computation.6 | async-start | bytes 2228224 | tf_op jit(solution)/shard_map/all_gather | solution.py:139
  28.1 210.5 %all-reduce.2.cloned.1.call-start = ((), (), s32[]{:S(2)}) async-start(), calls=%async_computation.5 | async-start | bytes 1048576 | tf_op jit(solution)/shard_map/psum | solution.py:191
  55.5 4.2 %copy-start.2 = (bf16[256,128]{1,0:T(8,128)(2,1)S(1)}, bf16[256,128]{1,0:T(8,128)(2,1)}, u32[]{:S(2)}) copy-start(bf16[256,128]{1,0:T(8,128)(2,1)} %constant_dynamic-slice_fusion.5) | copy-start | bytes 196612
  67.4 20.9 %copy-start.13 = (f32[4,512,4]{1,2,0:T(4,128)}, f32[4,512,4]{1,2,0:T(4,128)S(1)}, u32[]{:S(2)}) copy-start(f32[4,512,4]{1,2,0:T(4,128)S(1)} %get-tuple-element.254) | copy-start | bytes 98308
  158.4 21.3 %copy-start.3 = (bf16[128,2048]{1,0:T(8,128)(2,1)S(1)}, bf16[128,2048]{1,0:T(8,128)(2,1)}, u32[]{:S(2)}) copy-start(bf16[128,2048]{1,0:T(8,128)(2,1)} %param.17) | copy-start | bytes 1572868
  158.4 21.3 %copy-start.12 = (f32[2048]{0:T(1024)S(1)}, f32[2048]{0:T(1024)}, u32[]{:S(2)}) copy-start(f32[2048]{0:T(1024)} %param.19) | copy-start | bytes 24580
  160.2 123.3 %reduce-scatter.2.cloned.1.call-start = ((), (), s32[]{:S(2)}) async-start(), calls=%async_computation.7 | async-start | bytes 4456448 | tf_op jit(solution)/shard_map/reduce_scatter | solution.py:184
  182.5 0.9 copy-start.10
  184.4 1.9 copy-start.1
  195.0 1.9 copy-start.1
  205.7 1.9 copy-start.1
  216.4 1.9 copy-start.1
  227.2 9.5 %copy-start.6 = (bf16[128,2048]{1,0:T(8,128)(2,1)S(1)}, bf16[128,2048]{1,0:T(8,128)(2,1)}, u32[]{:S(2)}) copy-start(bf16[128,2048]{1,0:T(8,128)(2,1)} %param.18) | copy-start | bytes 1572868
  234.9 1.8 copy-start.7
  236.7 0.6 copy-start.20
  236.7 0.7 copy-start.18
  237.3 1.3 copy-start.4
  237.3 2.6 copy-start.16
Sparse Core Ops, SparseCore 0:
  11.3 44.1 all-gather.6
  57.6 36.9 all-gather.4
  96.8 36.9 all-gather.8
  135.7 40.4 all-gather.10
  178.9 27.3 all-reduce.1
  210.6 72.8 reduce-scatter.1
where the time goes:
time: 292 us; the launch traced here: 290 us
  waiting for transfers between devices  92.4 us (32%)
  blocking collectives  77.4 us (27%)
  matrix products  71.2 us (24%)
  local copies, waits for them, and re-layouts  23.9 us (8%)
  between operations  14.5 us (5%)
  other arithmetic  9.92 us (3%)
    reduce_scatter x1, waiting for transfers between devices, local(): lax.psum_scatter(jnp.einsum('rd,rc->dc', normed_target, d_query, preferre...  41.4 us
    all_gather x2, blocking collectives, merged(): everything = jax.tree.map(lambda part: lax.all_gather(part, axis), shard)  40.1 us
    all_gather x1, waiting for transfers between devices, local(): all_queries = lax.all_gather(query, 'sp', axis=0, tiled=True)  25.2 us
    all_gather x1, waiting for transfers between devices, local(): values_piece = lax.all_gather(value_head, 'sp', axis=0, tiled=True)  25.1 us
    all_gather x1, blocking collectives, local(): delta_piece = lax.all_gather(delta, 'sp', axis=0, tiled=True)  19.4 us
    dot_general x4, matrix products, gradient_block(): jnp.einsum('rhs,rhd->sd', d_scores, query_heads, preferred_element_type=j...  15.7 us
    dot_general x8, matrix products, key_inner_step(): jnp.einsum('rhs,sd->rhd', d_scores, keys_now, preferred_element_type=jnp....  14.2 us
    dynamic_slice x16, local copies, waits for them, and re-layouts, local(): lax.map(lambda blocked: block_totals(blocked, key_head, scaling), all_que...  13.9 us
  transfers between devices with their start and end apart: 6, of which 3 were waited for; matrix products, arithmetic and copies ran while one was open for 34% of the time, Pallas kernels for 0%

commit v1 on v0

v1 whole, which is shorter than its diff:
```python
import functools

import jax
import jax.numpy as jnp
from jax import lax
from jax.experimental import pallas as pl
from jax.experimental.pallas import tpu as pltpu
from jax.sharding import PartitionSpec as P


KVH = 2
HD = 128
EPS = 1e-06
LOG2E = 1.4426950408889634
FRONT_MIB = 60


F32 = jnp.float32
BF16 = jnp.bfloat16


def swap(x, axis, k):
    n = lax.axis_size(axis)
    return lax.ppermute(x, axis, [(i, i ^ k) for i in range(n)])


def dot(a, b, ca, cb):
    return lax.dot_general(a, b, (((ca,), (cb,)), ((), ())), preferred_element_type=F32)


def normed(x, gain):
    wide = x.astype(F32)
    inverse = lax.rsqrt(jnp.mean(wide * wide, axis=-1, keepdims=True) + EPS)
    return (wide * inverse * gain).astype(BF16)


def norm_back(x, gain, cotangent):
    wide = x.astype(F32)
    inverse = lax.rsqrt(jnp.mean(wide * wide, axis=-1, keepdims=True) + EPS)
    scaled = cotangent * gain
    inner = jnp.mean(wide * scaled, axis=-1, keepdims=True)
    return inverse * scaled - wide * (inverse * inverse * inverse * inner)


def chunk_copy(src, dst, sem, s, size):
    at = pl.ds(s * size, size)
    return pltpu.make_async_copy(src.at[at, :], dst.at[at, :], sem.at[s])


def source_kernel(steps, kv_ref, x_any, g_any, wk_any, wv_any, *refs):
    outs = refs[:KVH]
    x_ref, g_ref, wk_ref, wv_ref, k_ref, v_ref, sem, k_sem, v_sem = refs[KVH:]
    chunk = wk_ref.shape[0] // steps
    first = [
        pltpu.make_async_copy(x_any, x_ref, sem.at[0]),
        pltpu.make_async_copy(g_any, g_ref, sem.at[1]),
    ]
    wks = [chunk_copy(wk_any, wk_ref, k_sem, s, chunk) for s in range(steps)]
    wvs = [chunk_copy(wv_any, wv_ref, v_sem, s, chunk) for s in range(steps)]
    for copy in first:
        copy.start()
    for s in range(steps):
        wks[s].start()
        wvs[s].start()
    for copy in first:
        copy.wait()
    x_ref[...] = normed(x_ref[...], g_ref[...])
    k_acc, v_acc = None, None
    for s in range(steps):
        part = slice(s * chunk, (s + 1) * chunk)
        wks[s].wait()
        k = dot(x_ref[:, part], wk_ref[part, :], 1, 0)
        wvs[s].wait()
        v = dot(x_ref[:, part], wv_ref[part, :], 1, 0)
        k_acc = k if k_acc is None else k_acc + k
        v_acc = v if v_acc is None else v_acc + v
    k_ref[...] = k_acc.astype(BF16)
    v_ref[...] = v_acc.astype(BF16)
    for r in range(KVH):
        at = pl.ds(pl.multiple_of((kv_ref[0] ^ r) * HD, HD), HD)
        outs[r][:, :HD] = k_ref[:, at]
        outs[r][:, HD:] = v_ref[:, at]


def target_kernel(steps, sp, half, me_ref, x_any, g_any, wq_any, at_any, da_any, *refs):
    q_ref, near_ref, far_ref = refs[:3]
    x_ref, g_ref, wq_ref, at_ref, da_ref, nt_ref, sem, q_sem = refs[3:]
    dim = wq_ref.shape[0]
    chunk = dim // steps
    rows = x_ref.shape[0]
    dblk = dim // sp
    pairs = ((x_any, x_ref), (g_any, g_ref), (da_any, da_ref), (at_any, at_ref))
    copies = [pltpu.make_async_copy(a, b, sem.at[i]) for i, (a, b) in enumerate(pairs)]
    wqs = [chunk_copy(wq_any, wq_ref, q_sem, s, chunk) for s in range(steps)]
    for copy in copies + wqs:
        copy.start()
    for copy in copies[:2]:
        copy.wait()
    x_ref[...] = normed(x_ref[...], g_ref[...])
    for s in range(steps):
        part = slice(s * chunk, (s + 1) * chunk)
        nt_ref[part, :] = x_ref[:, part].T
    for copy in copies[2:]:
        copy.wait()
    prod = da_ref[...].astype(F32) * at_ref[...].astype(F32)
    q_ref[rows:, :] = jnp.zeros_like(q_ref[rows:, :])
    for h in range(prod.shape[1] // HD):
        d = jnp.sum(prod[:, h * HD : (h + 1) * HD].T, axis=0, keepdims=True)
        q_ref[rows : rows + 1, h * HD : h * HD + rows] = d.astype(BF16)
    me = me_ref[0]
    n = 0
    for j in range(sp):
        if j & half:
            continue
        here = pl.multiple_of((me ^ j) * dblk, dblk)
        there = pl.multiple_of((me ^ j ^ half) * dblk, dblk)
        near_ref[n * dblk : (n + 1) * dblk, :] = nt_ref[pl.ds(here, dblk), :]
        far_ref[n * dblk : (n + 1) * dblk, :] = nt_ref[pl.ds(there, dblk), :]
        n += 1
    q_acc = None
    for s in range(steps):
        part = slice(s * chunk, (s + 1) * chunk)
        wqs[s].wait()
        q = dot(x_ref[:, part], wq_ref[part, :], 1, 0)
        q_acc = q if q_acc is None else q_acc + q
    q_ref[:rows, :] = q_acc.astype(BF16)


def scores_kernel(nk, nb, rows, scaling, *refs):
    kvs, qs = refs[:nk], refs[nk : nk + nb]
    p_ref, st_ref, k_ref, v_ref, kt_ref = refs[nk + nb :]
    at = 0
    for kv in kvs:
        size = kv.shape[0]
        k_ref[at : at + size, :] = kv[:, :HD]
        v_ref[at : at + size, :] = kv[:, HD:]
        at += size
    kt_ref[...] = k_ref[...].T
    for h in range(p_ref.shape[0]):
        lanes = slice(h * HD, (h + 1) * HD)
        for pair in range(nb // 2):
            q = jnp.concatenate(
                [qs[2 * pair + i][:rows, lanes] for i in range(2)], axis=0
            )
            cols = slice(pair * 2 * rows, (pair + 1) * 2 * rows)
            s = dot(k_ref[...], q, 1, 1)
            top = jnp.max(s, axis=0, keepdims=True)
            p = jnp.exp2((s - top) * (scaling * LOG2E))
            p_ref[h, :, cols] = p.astype(BF16)
            st_ref[h, 0:1, cols] = top * (scaling * LOG2E)
            st_ref[h, 1:2, cols] = jnp.sum(p, axis=0, keepdims=True)


def grads_kernel(nb, rows, v_ref, kt_ref, p_ref, *refs):
    qs, gs = refs[:nb], refs[nb : 2 * nb]
    ds_ref, dq_ref = refs[2 * nb :]
    for h in range(p_ref.shape[0]):
        lanes = slice(h * HD, (h + 1) * HD)
        for pair in range(nb // 2):
            both = (2 * pair, 2 * pair + 1)
            g = jnp.concatenate([gs[i][:, lanes] for i in both], axis=0)
            delta = jnp.concatenate([qs[i][rows : rows + 1, lanes] for i in both], axis=1).astype(F32)
            cols = slice(pair * 2 * rows, (pair + 1) * 2 * rows)
            dw = dot(v_ref[...], g, 1, 1)
            ds = (p_ref[h, :, cols].astype(F32) * (dw - delta)).astype(BF16)
            ds_ref[h, :, cols] = ds
            dq_ref[h, :, cols] = dot(kt_ref[...], ds, 1, 0)


def lse_kernel(heads, a_ref, b_ref, o_ref):
    o_ref[...] = jnp.zeros_like(o_ref)
    for h in range(heads):
        ta, tb = a_ref[h, 0:1, :], b_ref[h, 0:1, :]
        top = jnp.maximum(ta, tb)
        total = a_ref[h, 1:2, :] * jnp.exp2(ta - top) + b_ref[h, 1:2, :] * jnp.exp2(tb - top)
        o_ref[h : h + 1, :] = top
        o_ref[heads + h : heads + h + 1, :] = total


def scale_kernel(nb, rows, heads, scaling, *refs):
    own_a, own_b = refs[:2]
    sts = refs[2 : nb + 1]
    dqa_ref, dqb_ref, c_ref, sent_ref, kept_ref = refs[nb + 1 :]
    places = [(kept_ref, 0), (sent_ref, 0), (kept_ref, 1), (sent_ref, 1)]
    for h in range(heads):
        tops = [own_a[h, 0:1, :], own_b[h, 0:1, :]]
        sums = [own_a[h, 1:2, :], own_b[h, 1:2, :]]
        for k in range(1, nb):
            order = [slice((j ^ k) * rows, (j ^ k) * rows + rows) for j in range(nb)]
            st = sts[k - 1]
            tops.append(jnp.concatenate([st[h : h + 1, o] for o in order], axis=1))
            low = heads + h
            sums.append(jnp.concatenate([st[low : low + 1, o] for o in order], axis=1))
        top = functools.reduce(jnp.maximum, tops)
        total = sum(s * jnp.exp2(t - top) for t, s in zip(tops, sums))
        ca = jnp.exp2(tops[0] - top) / total
        cb = jnp.exp2(tops[1] - top) / total
        c_ref[h, 0:1, :] = ca
        c_ref[h, 1:2, :] = cb
        for k in range(nb):
            part = slice(k * rows, (k + 1) * rows)
            block = dqa_ref[h, :, part] * (ca[:, part] * scaling)
            block = block + dqb_ref[h, :, part] * (cb[:, part] * scaling)
            ref, spot = places[k]
            ref[spot * rows : (spot + 1) * rows, h * HD : (h + 1) * HD] = block.T.astype(ref.dtype)


def keyvalue_kernel(nz, nb, rows, scaling, *refs):
    qs, gs = refs[:nb], refs[nb : 2 * nb]
    c_ref, pa_ref, pb_ref, dsa_ref, dsb_ref = refs[2 * nb : 2 * nb + 5]
    outs = refs[2 * nb + 5 :]
    size = outs[0].shape[0]
    for i, (p_ref, ds_ref) in enumerate(((pa_ref, dsa_ref), (pb_ref, dsb_ref))):
        count = p_ref.shape[1] // size
        key_acc, value_acc = [None] * count, [None] * count
        for h in range(p_ref.shape[0]):
            lanes = slice(h * HD, (h + 1) * HD)
            c = c_ref[h, i : i + 1, :].astype(BF16)
            q = jnp.concatenate([m[:rows, lanes] for m in qs], axis=0)
            g = jnp.concatenate([m[:, lanes] for m in gs], axis=0)
            for z in range(count):
                part = slice(z * size, (z + 1) * size)
                key = dot(ds_ref[h, part, :] * c, q, 1, 0)
                value = dot(p_ref[h, part, :] * c, g, 1, 0)
                key_acc[z] = key if h == 0 else key_acc[z] + key
                value_acc[z] = value if h == 0 else value_acc[z] + value
        for z in range(count):
            out = outs[i * (nz // 2) + z]
            out[:, :HD] = (key_acc[z] * scaling).astype(out.dtype)
            out[:, HD:] = value_acc[z].astype(out.dtype)


def first_kernel(nz, dblk, rows, pair_ref, other_ref, near_ref, far_ref, dq_ref, own_ref, o_ref):
    own = (pair_ref[:rows, :].astype(F32) + other_ref[rows:, :].astype(F32)).astype(BF16)
    dq_ref[:rows, :] = own
    own_ref[...] = own
    dq_ref[rows:, :] = (pair_ref[rows:, :].astype(F32) + other_ref[:rows, :].astype(F32)).astype(BF16)
    dq = dq_ref[...]
    for k in range(nz):
        at = slice((2 * k + 1) * dblk, (2 * k + 2) * dblk)
        left = jnp.concatenate([near_ref[at, :], far_ref[at, :]], axis=1)
        o_ref[k * dblk : (k + 1) * dblk, :] = dot(left, dq, 1, 0).astype(BF16)


def second_kernel(nz, dblk, dq_ref, near_ref, far_ref, got_ref, *outs):
    dq = dq_ref[...]
    for k in range(nz):
        at = slice(2 * k * dblk, (2 * k + 1) * dblk)
        left = jnp.concatenate([near_ref[at, :], far_ref[at, :]], axis=1)
        total = dot(left, dq, 1, 0) + got_ref[k * dblk : (k + 1) * dblk, :].astype(F32)
        outs[k][...] = total.astype(outs[k].dtype)


def pair_kernel(*refs):
    n = len(refs) // 3
    for kept, got, out in zip(refs[:n], refs[n : 2 * n], refs[2 * n :]):
        out[...] = (kept[...] + got[...].astype(F32)).astype(BF16)


def zsum_kernel(nz, *refs):
    own_ref, rest_ref = refs[nz:]
    total = refs[0][...].astype(F32)
    for k in range(1, nz):
        total = total + refs[k][...].astype(F32)
    size = own_ref.shape[0]
    own_ref[...] = total[:size].astype(BF16)
    rest_ref[...] = total[size:].astype(BF16)


def dtarget_kernel(tp, idx_ref, x_ref, g_ref, *refs):
    dqs, w_ref = refs[:tp], refs[tp]
    mine, theirs = refs[tp + 1 : 2 * tp], refs[2 * tp : 3 * tp - 1]
    o_ref, acc = refs[3 * tp - 1 :]
    acc[...] = dot(dqs[0][...], w_ref[...], 1, 1)
    size = acc.shape[1] // 2
    for flip, halves in enumerate((mine, theirs)):
        at = pl.ds(pl.multiple_of((idx_ref[0] ^ flip) * size, size), size)
        for d in range(1, tp):
            acc[:, at] += dot(dqs[d][...], halves[d - 1][...], 1, 1)
    o_ref[...] = norm_back(x_ref[...], g_ref[...], acc[...]).astype(BF16)


def dsource_kernel(idx_ref, x_ref, g_ref, wk_ref, wv_ref, *refs):
    o_ref = refs[KVH]
    total = None
    for r in range(KVH):
        at = pl.ds(pl.multiple_of((idx_ref[0] ^ r) * HD, HD), HD)
        part = dot(refs[r][:, :HD], wk_ref[:, at], 1, 1) + dot(refs[r][:, HD:], wv_ref[:, at], 1, 1)
        total = part if total is None else total + part
    o_ref[...] = norm_back(x_ref[...], g_ref[...], total)


def whole(shape):
    return pl.BlockSpec(shape, lambda *_: (0,) * len(shape))


def estimate(flops, mib):
    return pl.CostEstimate(flops=flops, bytes_accessed=mib << 20, transcendentals=0)


def call(body, out_shape, args, flops=1 << 24, mib=2, mb=12, index=(), scratch=(), specs=None):
    outs = out_shape if isinstance(out_shape, list) else [out_shape]
    specs = specs or [whole(a.shape) for a in args]
    out_specs = [whole(o.shape) for o in outs]
    scalars = [i.astype(jnp.int32).reshape(1) for i in index]
    got = pl.pallas_call(
        body,
        grid_spec=pltpu.PrefetchScalarGridSpec(
            num_scalar_prefetch=len(scalars),
            grid=(1,),
            in_specs=specs,
            out_specs=out_specs,
            scratch_shapes=list(scratch),
        ),
        out_shape=outs,
        compiler_params=pltpu.CompilerParams(vmem_limit_bytes=mb << 20),
        cost_estimate=estimate(flops, mib),
    )(*scalars, *args)
    return got if isinstance(out_shape, list) else got[0]


def local(target, source, target_gain, source_gain, w_query, w_key, w_value, attended, d_attended):
    sp, tp = lax.axis_size("sp"), lax.axis_size("tp")
    me, mt = lax.axis_index("sp"), lax.axis_index("tp")
    rows, dim = target.shape
    srows = source.shape[0]
    width = w_query.shape[1]
    heads = width // HD
    group = tp // KVH
    nb = 4
    nz = sp // nb
    half = nb // 2
    scaling = HD ** (-0.5)
    kv_index = mt // group
    dblk = dim // sp
    steps = 4
    kvw = KVH * HD
    shape = jax.ShapeDtypeStruct
    t_gain, s_gain = target_gain.reshape(1, dim), source_gain.reshape(1, dim)

    hbm = pl.BlockSpec(memory_space=pltpu.HBM)
    near_rows = dim // 2
    by_head = call(
        functools.partial(source_kernel, steps),
        [shape((srows, 2 * HD), BF16)] * KVH,
        (source, s_gain, w_key, w_value),
        flops=4 * srows * dim * kvw,
        mb=FRONT_MIB,
        index=(kv_index,),
        specs=[hbm] * 4,
        scratch=[
            pltpu.VMEM((srows, dim), BF16),
            pltpu.VMEM((1, dim), F32),
            pltpu.VMEM((dim, kvw), BF16),
            pltpu.VMEM((dim, kvw), BF16),
            pltpu.VMEM((srows, kvw), BF16),
            pltpu.VMEM((srows, kvw), BF16),
            pltpu.SemaphoreType.DMA((2,)),
            pltpu.SemaphoreType.DMA((steps,)),
            pltpu.SemaphoreType.DMA((steps,)),
        ],
    )
    q_ext, near, far = call(
        functools.partial(target_kernel, steps, sp, half),
        [shape((rows + 16, width), BF16)] + [shape((near_rows, rows), BF16)] * 2,
        (target, t_gain, w_query, attended, d_attended),
        flops=2 * rows * dim * width,
        mb=FRONT_MIB,
        index=(me,),
        specs=[hbm] * 5,
        scratch=[
            pltpu.VMEM((rows, dim), BF16),
            pltpu.VMEM((1, dim), F32),
            pltpu.VMEM((dim, width), BF16),
            pltpu.VMEM((rows, width), BF16),
            pltpu.VMEM((rows, width), BF16),
            pltpu.VMEM((dim, rows), BF16),
            pltpu.SemaphoreType.DMA((4,)),
            pltpu.SemaphoreType.DMA((steps,)),
        ],
    )

    def away(x, k, step=None):
        return swap(x, "sp", (step or k) * nb)

    def gathered(blocks):
        odd = [away(blocks[k], k, 1) for k in range(1, nz, 2)]
        pairs = call(
            pair_kernel, [shape(x.shape, BF16) for x in odd[1:]], (*blocks[2::2], *odd[1:]), mib=1
        )
        return [blocks[0], odd[0]] + [away(x, 2 * i + 2) for i, x in enumerate(pairs)]

    rest = [swap(by_head[d // group], "tp", d) for d in range(1, tp)]
    kv_own = jnp.concatenate([by_head[0]] + rest, axis=0)
    chunks = [range(nz // 2), range(nz // 2, nz)]
    kvs = []
    for ks in chunks:
        kvs.append([kv_own if k == 0 else away(kv_own, k) for k in ks])
    qs = [q_ext] + [swap(q_ext, "sp", k) for k in range(1, nb)]
    gs = [d_attended] + [swap(d_attended, "sp", k) for k in range(1, nb)]
    far = swap(far, "sp", half)

    held, _ = lax.optimization_barrier((w_query, kv_own))
    piece = lax.dynamic_slice_in_dim(held, (me & 1) * (dim // 2), dim // 2, 0)
    wq_mine = [swap(piece, "tp", d) for d in range(1, tp)]
    wq_theirs = [swap(w, "sp", 1) for w in wq_mine]

    trows = nb * rows
    stshape = shape((heads, 8, trows), F32)
    dqshape = shape((heads, HD, trows), F32)

    def scores(c):
        part = sum(kv.shape[0] for kv in kvs[c])
        return call(
            functools.partial(scores_kernel, len(kvs[c]), nb, rows, scaling),
            [
                shape((heads, part, trows), BF16),
                stshape,
                shape((part, HD), BF16),
                shape((part, HD), BF16),
                shape((HD, part), BF16),
            ],
            (*kvs[c], *qs),
            flops=4 * heads * part * trows * HD,
        )

    def grads(probs, values, keys_t):
        return call(
            functools.partial(grads_kernel, nb, rows),
            [shape(probs.shape, BF16), dqshape],
            (values, keys_t, probs, *qs, *gs),
            flops=6 * probs.size * HD,
        )

    p_a, st_a, _, v_a, kt_a = scores(0)
    ds_a, dq_a = grads(p_a, v_a, kt_a)
    p_b, st_b, _, v_b, kt_b = scores(1)
    stats = call(functools.partial(lse_kernel, heads), shape((8 * -(-heads // 4), trows), F32), (st_a, st_b), mib=1)
    sts = [swap(stats, "sp", k) for k in range(1, nb)]
    ds_b, dq_b = grads(p_b, v_b, kt_b)
    coef, sent, kept = call(
        functools.partial(scale_kernel, nb, rows, heads, scaling),
        [stshape, shape((2 * rows, width), BF16), shape((2 * rows, width), F32)],
        (st_a, st_b, *sts, dq_a, dq_b),
    )
    src = tp * srows
    dkvs = call(
        functools.partial(keyvalue_kernel, nz, nb, rows, scaling),
        [shape((src, 2 * HD), BF16 if z % 2 else F32) for z in range(nz)],
        (*qs, *gs, coef, p_a, p_b, ds_a, ds_b),
        flops=6 * heads * nz * src * trows * HD,
    )

    pair_b = (kept + swap(sent, "sp", 1).astype(F32)).astype(BF16)
    other = swap(pair_b, "sp", half)

    dq_two, dq_own, partial = call(
        functools.partial(first_kernel, nz, dblk, rows),
        [shape((2 * rows, width), BF16), shape((rows, width), BF16), shape((nz * dblk, width), BF16)],
        (pair_b, other, near, far),
        flops=4 * rows * nz * dblk * width,
    )
    got = swap(partial, "sp", 1)
    mine = call(
        functools.partial(second_kernel, nz, dblk),
        [shape((dblk, width), BF16 if k % 2 else F32) for k in range(nz)],
        (dq_two, near, far, got),
        flops=4 * rows * nz * dblk * width,
    )
    d_w_query, *arrived = gathered(mine)
    for x in arrived:
        d_w_query = d_w_query + x.astype(F32)

    dqs = [dq_own] + [swap(dq_own, "tp", d) for d in range(1, tp)]
    d_target = call(
        functools.partial(dtarget_kernel, tp),
        shape((rows, dim), BF16),
        (target, t_gain, *dqs, w_query, *wq_mine, *wq_theirs),
        flops=2 * rows * dim * width * tp,
        index=(me & 1,),
        scratch=[pltpu.VMEM((rows, dim), F32)],
    )

    dkvs = gathered(dkvs)
    own, others = call(
        functools.partial(zsum_kernel, len(dkvs)),
        [shape((srows, 2 * HD), BF16), shape((src - srows, 2 * HD), BF16)],
        dkvs,
    )
    relative = [own] + [None] * (KVH - 1)
    for d in range(1, tp):
        block = swap(others[(d - 1) * srows : d * srows], "tp", d)
        r = d // group
        if relative[r] is None:
            relative[r] = block
        else:
            relative[r] = relative[r].astype(F32) + block.astype(F32)
    d_source = call(
        dsource_kernel,
        shape((srows, dim), F32),
        (source, s_gain, w_key, w_value, *[x.astype(BF16) for x in relative]),
        flops=4 * srows * dim * kvw,
        index=(kv_index,),
    )
    return (d_target, d_source, d_w_query)


def solution(mesh):
    return jax.shard_map(
        local,
        mesh=mesh,
        in_specs=(
            P("sp", None),
            P(("sp", "tp"), None),
            P(),
            P(),
            P(None, "tp"),
            P(),
            P(),
            P("sp", "tp"),
            P("sp", "tp"),
        ),
        out_specs=(P("sp", None), P(("sp", "tp"), None), P("sp", "tp")),
        check_vma=False,
    )
```

time: 292 us -> 90.7 us (0.31)
  blocking collectives: 77.4 us -> 0 us
  matrix products: 71.2 us -> 0 us
  waiting for transfers between devices: 92.4 us -> 32 us
  starting transfers between devices: 0.24 us -> 32.4 us
  local copies, waits for them, and re-layouts: 23.9 us -> 0.98 us
  Pallas kernels: 0 us -> 22.6 us
  between operations: 14.5 us -> 0.89 us
  other arithmetic: 9.92 us -> 0.82 us
    dot_general x39 -> x0, matrix products: 71.2 us -> none  [the longest x4 15.7 us: gradient_block(): jnp.einsum('rhs,rhd->sd', d_scores, query_heads, preferred_element_type=j...]
    all_gather x5 -> x0, blocking collectives: 70.5 us -> none  [the longest x2 40.1 us: merged(): everything = jax.tree.map(lambda part: lax.all_gather(part, axis), shard)]
    all_gather x4 -> x0, waiting for transfers between devices: 50.3 us -> none  [the longest x1 25.2 us: local(): all_queries = lax.all_gather(query, 'sp', axis=0, tiled=True)]
    reduce_scatter x1 -> x0, waiting for transfers between devices: 41.4 us -> none  [local(): lax.psum_scatter(jnp.einsum('rd,rc->dc', normed_target, d_query, preferre...]
    ppermute x0 -> x27, starting transfers between devices: none -> 32.4 us  [swap(): return lax.ppermute(x, axis, [(i, i ^ k) for i in range(n)])]
    ppermute x0 -> x27, waiting for transfers between devices: none -> 32 us  [swap(): return lax.ppermute(x, axis, [(i, i ^ k) for i in range(n)])]
    pallas_call x0 -> x16, Pallas kernels: none -> 22.6 us  [call(): pl.pallas_call(body, grid_spec=pltpu.PrefetchScalarGridSpec(num_scalar_pr...]
    dynamic_slice x19 -> x1, local copies, waits for them, and re-layouts: 15.2 us -> 0.07 us  [local(): piece = lax.dynamic_slice_in_dim(held, (me & 1) * (dim // 2), dim // 2, 0)]
  transfers between devices with their start and end apart: 6 -> 27, of which waited for: 3 -> 9; matrix products, arithmetic and copies ran while one was open for 34% -> 2% of each run, Pallas kernels for 0% -> 19%
where the time goes in v1:
time: 90.7 us; the launch traced here: 89.7 us
  starting transfers between devices  32.4 us (36%)
  waiting for transfers between devices  32 us (35%)
  Pallas kernels  22.6 us (25%)
  local copies, waits for them, and re-layouts  0.98 us (1%)
    ppermute x27, starting transfers between devices, swap(): return lax.ppermute(x, axis, [(i, i ^ k) for i in range(n)])  32.4 us
    ppermute x27, waiting for transfers between devices, swap(): return lax.ppermute(x, axis, [(i, i ^ k) for i in range(n)])  32 us
    pallas_call x16, Pallas kernels, call(): pl.pallas_call(body, grid_spec=pltpu.PrefetchScalarGridSpec(num_scalar_pr...  22.6 us
  transfers between devices with their start and end apart: 27, of which 9 were waited for; matrix products, arithmetic and copies ran while one was open for 2% of the time, Pallas kernels for 19%

profile of v1, /device:TPU:0, one launch (start us, length us, event | category | flops | bytes accessed | tf_op | source)
XLA Modules:
  0.0 89.7 jit_solution(16377839015655974779)
XLA Ops:
  0.6 3.1 %shard_map.113 = (bf16[144,512]{1,0:T(8,128)(2,1)}, bf16[1024,128]{1,0:T(8,128)(2,1)}, bf16[1024,128]{1,0:T(8,128)(2,1)}) custom-call(s32[1]{0:T(128)} %bitcast.4.me_ref, bf16[128,2048]{1,0:T(8,128)(2,1)} %x_ref.2, f32[1,2048]{1,0:T(1,128)} %bitcast.7, bf16[2048,512]{1,0:T(8,128)(2,1)} %refs_2_.1, bf16[128,512]{1,0:T(8,128)(2,1)} %at_any.1, ...), custom_call_target="tpu_custom_call" | custom-call | flops 268435456 | bytes 2097152 | tf_op jit(solution)/shard_map/pallas_call | solution.py:306
  3.8 0.6 collective-permute-start.2
  4.3 2.6 %collective-permute-start.3 = (bf16[144,512]{1,0:T(8,128)(2,1)}, bf16[144,512]{1,0:T(8,128)(2,1)S(1)}, u32[]{:S(2)}, u32[]{:S(2)}) collective-permute-start(bf16[144,512]{1,0:T(8,128)(2,1)} %get-tuple-element.39.refs_2_.refs_0_), channel_id=1, source_target_pairs={{0,4},{2,6},{4,0},{6,2},{8,12},{10,14},{12,8},{14,10},{16,20},{18,... | collective-permute-start | bytes 442376 | tf_op jit(solution)/shard_map/ppermute | solution.py:24
  6.9 3.4 %shard_map.112 = (bf16[128,256]{1,0:T(8,128)(2,1)}, bf16[128,256]{1,0:T(8,128)(2,1)}) custom-call(s32[1]{0:T(128)} %bitcast.2.kv_ref.idx_ref, bf16[128,2048]{1,0:T(8,128)(2,1)} %x_ref.3, f32[1,2048]{1,0:T(1,128)} %bitcast.5, bf16[2048,256]{1,0:T(8,128)(2,1)} %wk_ref.1, bf16[2048,256]{1,0:T(8,128)(2,1)} %wv_ref.1), custom_call_target="tpu_custom_call" | custom-call | flops 268435456 | bytes 2097152 | tf_op jit(solution)/shard_map/pallas_call | solution.py:306
  10.3 1.8 %collective-permute-start = (bf16[128,256]{1,0:T(8,128)(2,1)}, bf16[128,256]{1,0:T(8,128)(2,1)S(1)}, u32[]{:S(2)}, u32[]{:S(2)}) collective-permute-start(bf16[128,256]{1,0:T(8,128)(2,1)} %get-tuple-element.38), channel_id=1, source_target_pairs={{0,1},{1,0},{2,3},{3,2},{4,5},{5,4},{6,7},{7,6},{8,9},{9,8},{10,11... | collective-permute-start | bytes 196616 | tf_op jit(solution)/shard_map/ppermute | solution.py:24
  12.1 0.8 constant_dynamic-update-slice_fusion.1
  12.9 2.0 %collective-permute-done = bf16[128,256]{1,0:T(8,128)(2,1)S(1)} collective-permute-done((bf16[128,256]{1,0:T(8,128)(2,1)}, bf16[128,256]{1,0:T(8,128)(2,1)S(1)}, u32[]{:S(2)}, u32[]{:S(2)}) %collective-permute-start) | collective-permute-done | bytes 65568 | tf_op jit(solution)/shard_map/ppermute | solution.py:24
  14.9 2.8 %collective-permute-start.5 = (bf16[256,256]{1,0:T(8,128)(2,1)S(1)}, bf16[256,256]{1,0:T(8,128)(2,1)S(1)}, u32[]{:S(2)}, u32[]{:S(2)}) collective-permute-start(bf16[256,256]{1,0:T(8,128)(2,1)S(1)} %constant_dynamic-update-slice_fusion.refs_0_), channel_id=1, source_target_pairs={{0,16},{2,18},{4,20},{6,22},{8,24},{10,26},{12,28},{14,30},{16,0},... | collective-permute-start | bytes 393224 | tf_op jit(solution)/shard_map/ppermute | solution.py:24
  17.8 1.6 %collective-permute-start.11 = (bf16[128,512]{1,0:T(8,128)(2,1)S(1)}, bf16[128,512]{1,0:T(8,128)(2,1)S(1)}, u32[]{:S(2)}, u32[]{:S(2)}) collective-permute-start(bf16[128,512]{1,0:T(8,128)(2,1)S(1)} %copy-done.3), channel_id=1, source_target_pairs={{0,4},{2,6},{4,0},{6,2},{8,12},{10,14},{12,8},{14,10},{16,20},{18,... | collective-permute-start | bytes 393224 | tf_op jit(solution)/shard_map/ppermute | solution.py:24
  19.4 0.3 collective-permute-start.12
  19.6 1.3 %collective-permute-start.6 = (bf16[256,256]{1,0:T(8,128)(2,1)S(1)}, bf16[256,256]{1,0:T(8,128)(2,1)S(1)}, u32[]{:S(2)}, u32[]{:S(2)}) collective-permute-start(bf16[256,256]{1,0:T(8,128)(2,1)S(1)} %constant_dynamic-update-slice_fusion.refs_0_), channel_id=1, source_target_pairs={{0,24},{2,26},{4,28},{6,30},{8,16},{10,18},{12,20},{14,22},{16,8},... | collective-permute-start | bytes 393224 | tf_op jit(solution)/shard_map/ppermute | solution.py:24
  21.0 2.9 %collective-permute-done.5.refs_0_ = bf16[256,256]{1,0:T(8,128)(2,1)S(1)} collective-permute-done((bf16[256,256]{1,0:T(8,128)(2,1)S(1)}, bf16[256,256]{1,0:T(8,128)(2,1)S(1)}, u32[]{:S(2)}, u32[]{:S(2)}) %collective-permute-start.5) | collective-permute-done | bytes 131104 | tf_op jit(solution)/shard_map/ppermute | solution.py:24
  23.9 3.5 %collective-permute-start.1 = (bf16[256,256]{1,0:T(8,128)(2,1)S(1)}, bf16[256,256]{1,0:T(8,128)(2,1)S(1)}, u32[]{:S(2)}, u32[]{:S(2)}) collective-permute-start(bf16[256,256]{1,0:T(8,128)(2,1)S(1)} %constant_dynamic-update-slice_fusion.refs_0_), channel_id=1, source_target_pairs={{0,8},{2,10},{4,12},{6,14},{8,0},{10,2},{12,4},{14,6},{16,24},{18,... | collective-permute-start | bytes 393224 | tf_op jit(solution)/shard_map/ppermute | solution.py:24
  27.4 3.5 %collective-permute-done.1.refs_1_ = bf16[256,256]{1,0:T(8,128)(2,1)S(1)} collective-permute-done((bf16[256,256]{1,0:T(8,128)(2,1)S(1)}, bf16[256,256]{1,0:T(8,128)(2,1)S(1)}, u32[]{:S(2)}, u32[]{:S(2)}) %collective-permute-start.1) | collective-permute-done | bytes 131104 | tf_op jit(solution)/shard_map/ppermute | solution.py:24
  31.0 1.5 %collective-permute-start.17 = (bf16[1024,512]{1,0:T(8,128)(2,1)S(1)}, bf16[1024,512]{1,0:T(8,128)(2,1)S(1)}, u32[]{:S(2)}, u32[]{:S(2)}) collective-permute-start(bf16[1024,512]{1,0:T(8,128)(2,1)S(1)} %constant_dynamic-slice_fusion), channel_id=1, source_target_pairs={{0,1},{1,0},{2,3},{3,2},{4,5},{5,4},{6,7},{7,6},{8,9},{9,8},{10,11... | collective-permute-start | bytes 3145736 | tf_op jit(solution)/shard_map/ppermute | solution.py:24
  32.4 1.5 %shard_map.114 = (bf16[4,512,512]{2,1,0:T(8,128)(2,1)S(1)}, f32[4,8,512]{2,1,0:T(8,128)S(1)}, bf16[512,128]{1,0:T(8,128)(2,1)}, bf16[512,128]{1,0:T(8,128)(2,1)S(1)}, bf16[128,512]{1,0:T(8,128)(2,1)S(1)}) custom-call(bf16[256,256]{1,0:T(8,128)(2,1)S(1)} %constant_dynamic-update-slice_fusion.refs_0_, bf16[256,256]{1,0:T(8,128)(2,1)S(1)} %collective-permute-done.1.refs_1_, ...), custom_call_target="tpu_custom_call" | custom-call | flops 536870912 | bytes 2097152 | tf_op jit(solution)/shard_map/pallas_call | solution.py:306
  34.0 1.5 %shard_map.115 = (bf16[4,512,512]{2,1,0:T(8,128)(2,1)S(1)}, f32[4,8,512]{2,1,0:T(8,128)S(1)}, bf16[512,128]{1,0:T(8,128)(2,1)}, bf16[512,128]{1,0:T(8,128)(2,1)S(1)}, bf16[128,512]{1,0:T(8,128)(2,1)S(1)}) custom-call(bf16[256,256]{1,0:T(8,128)(2,1)S(1)} %collective-permute-done.5.refs_0_, bf16[256,256]{1,0:T(8,128)(2,1)S(1)} %collective-permute-done.6.refs_1_, ...), custom_call_target="tpu_custom_call" | custom-call | flops 536870912 | bytes 2097152 | tf_op jit(solution)/shard_map/pallas_call | solution.py:306
  35.6 0.1 collective-permute-start.7
  35.6 1.6 %collective-permute-start.8 = (f32[8,512]{1,0:T(8,128)S(1)}, f32[8,512]{1,0:T(8,128)S(1)}, u32[]{:S(2)}, u32[]{:S(2)}) collective-permute-start(f32[8,512]{1,0:T(8,128)S(1)} %shard_map.116), channel_id=1, source_target_pairs={{0,4},{2,6},{4,0},{6,2},{8,12},{10,14},{12,8},{14,10},{16,20},{18,... | collective-permute-start | bytes 49160 | tf_op jit(solution)/shard_map/ppermute | solution.py:24
  37.2 0.3 collective-permute-start.9
  37.5 2.5 %shard_map.118 = (bf16[4,512,512]{2,1,0:T(8,128)(2,1)S(1)}, f32[4,128,512]{2,1,0:T(8,128)S(1)}) custom-call(bf16[512,128]{1,0:T(8,128)(2,1)S(1)} %get-tuple-element.46.v_ref, bf16[128,512]{1,0:T(8,128)(2,1)S(1)} %get-tuple-element.47.kt_ref, bf16[4,512,512]{2,1,0:T(8,128)(2,1)S(1)} %get-tuple-element.48.p_ref.refs_10_, bf16[144,512]{1,0:T(8,128)(2,1)S(1)} %copy-done.6, ...), custom_call_target="tpu_custom_call" | custom-call | flops 805306368 | bytes 2097152 | tf_op jit(solution)/shard_map/pallas_call | solution.py:306
  40.0 2.5 %shard_map.117 = (bf16[4,512,512]{2,1,0:T(8,128)(2,1)S(1)}, f32[4,128,512]{2,1,0:T(8,128)S(1)}) custom-call(bf16[512,128]{1,0:T(8,128)(2,1)S(1)} %get-tuple-element.42.v_ref, bf16[128,512]{1,0:T(8,128)(2,1)S(1)} %get-tuple-element.43.kt_ref, bf16[4,512,512]{2,1,0:T(8,128)(2,1)S(1)} %get-tuple-element.44.p_ref.refs_9_, bf16[144,512]{1,0:T(8,128)(2,1)S(1)} %copy-done.6, ...), custom_call_target="tpu_custom_call" | custom-call | flops 805306368 | bytes 2097152 | tf_op jit(solution)/shard_map/pallas_call | solution.py:306
  42.5 0.3 shard_map.119
  42.9 0.4 collective-permute-start.13
  43.3 1.5 %collective-permute-start.15 = (bf16[1024,128]{1,0:T(8,128)(2,1)S(1)}, bf16[1024,128]{1,0:T(8,128)(2,1)S(1)}, u32[]{:S(2)}, u32[]{:S(2)}) collective-permute-start(bf16[1024,128]{1,0:T(8,128)(2,1)S(1)} %copy-done.10), channel_id=1, source_target_pairs={{0,4},{2,6},{4,0},{6,2},{8,12},{10,14},{12,8},{14,10},{16,20},{18,... | collective-permute-start | bytes 786440 | tf_op jit(solution)/shard_map/ppermute | solution.py:24
  44.8 0.1 add_convert_fusion.pair_ref
  44.9 1.2 %collective-permute-start.14 = (bf16[256,512]{1,0:T(8,128)(2,1)S(1)}, bf16[256,512]{1,0:T(8,128)(2,1)S(1)}, u32[]{:S(2)}, u32[]{:S(2)}) collective-permute-start(bf16[256,512]{1,0:T(8,128)(2,1)S(1)} %add_convert_fusion.pair_ref), channel_id=1, source_target_pairs={{0,4},{2,6},{4,0},{6,2},{8,12},{10,14},{12,8},{14,10},{16,20},{18,... | collective-permute-start | bytes 786440 | tf_op jit(solution)/shard_map/ppermute | solution.py:24
  46.1 9.2 %collective-permute-done.17.refs_3_ = bf16[1024,512]{1,0:T(8,128)(2,1)S(1)} collective-permute-done((bf16[1024,512]{1,0:T(8,128)(2,1)S(1)}, bf16[1024,512]{1,0:T(8,128)(2,1)S(1)}, u32[]{:S(2)}, u32[]{:S(2)}) %collective-permute-start.17) | collective-permute-done | bytes 1048608 | tf_op jit(solution)/shard_map/ppermute | solution.py:24
  55.4 1.9 %collective-permute-done.14.other_ref = bf16[256,512]{1,0:T(8,128)(2,1)S(1)} collective-permute-done((bf16[256,512]{1,0:T(8,128)(2,1)S(1)}, bf16[256,512]{1,0:T(8,128)(2,1)S(1)}, u32[]{:S(2)}, u32[]{:S(2)}) %collective-permute-start.14) | collective-permute-done | bytes 262176 | tf_op jit(solution)/shard_map/ppermute | solution.py:24
  57.3 0.3 shard_map.120
  57.6 0.1 collective-permute-start.23
  57.7 2.6 %shard_map.122 = (f32[256,256]{1,0:T(8,128)S(1)}, bf16[256,256]{1,0:T(8,128)(2,1)S(1)}, f32[256,256]{1,0:T(8,128)S(1)}, bf16[256,256]{1,0:T(8,128)(2,1)S(1)}) custom-call(bf16[144,512]{1,0:T(8,128)(2,1)S(1)} %copy-done.6, bf16[144,512]{1,0:T(8,128)(2,1)S(1)} %collective-permute-done.2.refs_3_.refs_1_, ...), custom_call_target="tpu_custom_call" | custom-call | flops 1610612736 | bytes 2097152 | tf_op jit(solution)/shard_map/pallas_call | solution.py:306
  60.3 1.8 %collective-permute-start.20 = (bf16[256,256]{1,0:T(8,128)(2,1)S(1)}, bf16[256,256]{1,0:T(8,128)(2,1)S(1)}, u32[]{:S(2)}, u32[]{:S(2)}) collective-permute-start(bf16[256,256]{1,0:T(8,128)(2,1)S(1)} %get-tuple-element.62), channel_id=1, source_target_pairs={{0,8},{2,10},{4,12},{6,14},{8,0},{10,2},{12,4},{14,6},{16,24},{18,... | collective-permute-start | bytes 393224 | tf_op jit(solution)/shard_map/ppermute | solution.py:24
  62.1 0.3 shard_map.126
  62.4 0.4 collective-permute-start.25
  62.8 1.7 %collective-permute-start.19 = (bf16[256,256]{1,0:T(8,128)(2,1)S(1)}, bf16[256,256]{1,0:T(8,128)(2,1)S(1)}, u32[]{:S(2)}, u32[]{:S(2)}) collective-permute-start(bf16[256,256]{1,0:T(8,128)(2,1)S(1)} %get-tuple-element.60), channel_id=1, source_target_pairs={{0,8},{2,10},{4,12},{6,14},{8,0},{10,2},{12,4},{14,6},{16,24},{18,... | collective-permute-start | bytes 393224 | tf_op jit(solution)/shard_map/ppermute | solution.py:24
  64.5 2.2 %collective-permute-done.20.refs_1_ = bf16[256,256]{1,0:T(8,128)(2,1)S(1)} collective-permute-done((bf16[256,256]{1,0:T(8,128)(2,1)S(1)}, bf16[256,256]{1,0:T(8,128)(2,1)S(1)}, u32[]{:S(2)}, u32[]{:S(2)}) %collective-permute-start.20) | collective-permute-done | bytes 131104 | tf_op jit(solution)/shard_map/ppermute | solution.py:24
  66.8 3.4 %collective-permute-start.21 = (bf16[256,256]{1,0:T(8,128)(2,1)S(1)}, bf16[256,256]{1,0:T(8,128)(2,1)S(1)}, u32[]{:S(2)}, u32[]{:S(2)}) collective-permute-start(bf16[256,256]{1,0:T(8,128)(2,1)S(1)} %shard_map.123), channel_id=1, source_target_pairs={{0,16},{2,18},{4,20},{6,22},{8,24},{10,26},{12,28},{14,30},{16,0},... | collective-permute-start | bytes 393224 | tf_op jit(solution)/shard_map/ppermute | solution.py:24
  70.2 1.7 %collective-permute-start.24 = (bf16[128,512]{1,0:T(8,128)(2,1)S(1)}, bf16[128,512]{1,0:T(8,128)(2,1)S(1)}, u32[]{:S(2)}, u32[]{:S(2)}) collective-permute-start(bf16[128,512]{1,0:T(8,128)(2,1)S(1)} %get-tuple-element.68), channel_id=1, source_target_pairs={{0,8},{2,10},{4,12},{6,14},{8,0},{10,2},{12,4},{14,6},{16,24},{18,... | collective-permute-start | bytes 393224 | tf_op jit(solution)/shard_map/ppermute | solution.py:24
  72.0 1.0 %collective-permute-start.26 = (bf16[128,512]{1,0:T(8,128)(2,1)S(1)}, bf16[128,512]{1,0:T(8,128)(2,1)S(1)}, u32[]{:S(2)}, u32[]{:S(2)}) collective-permute-start(bf16[128,512]{1,0:T(8,128)(2,1)S(1)} %shard_map.127), channel_id=1, source_target_pairs={{0,16},{2,18},{4,20},{6,22},{8,24},{10,26},{12,28},{14,30},{16,0},... | collective-permute-start | bytes 393224 | tf_op jit(solution)/shard_map/ppermute | solution.py:24
  73.0 2.8 %collective-permute-done.19.refs_1_ = bf16[256,256]{1,0:T(8,128)(2,1)S(1)} collective-permute-done((bf16[256,256]{1,0:T(8,128)(2,1)S(1)}, bf16[256,256]{1,0:T(8,128)(2,1)S(1)}, u32[]{:S(2)}, u32[]{:S(2)}) %collective-permute-start.19) | collective-permute-done | bytes 131104 | tf_op jit(solution)/shard_map/ppermute | solution.py:24
  75.9 0.6 collective-permute-start.22
  76.5 3.7 %collective-permute-done.22.refs_1_ = bf16[128,256]{1,0:T(8,128)(2,1)S(1)} collective-permute-done((bf16[128,256]{1,0:T(8,128)(2,1)S(1)}, bf16[128,256]{1,0:T(8,128)(2,1)S(1)}, u32[]{:S(2)}, u32[]{:S(2)}) %collective-permute-start.22) | collective-permute-done | bytes 65568 | tf_op jit(solution)/shard_map/ppermute | solution.py:24
  80.3 1.9 %shard_map.125 = f32[128,2048]{1,0:T(8,128)} custom-call(s32[1]{0:T(128)} %bitcast.2.kv_ref.idx_ref, bf16[128,2048]{1,0:T(8,128)(2,1)S(1)} %copy-done.4, f32[1,2048]{1,0:T(1,128)S(1)} %bitcast.6, bf16[2048,256]{1,0:T(8,128)(2,1)S(1)} %copy-done.1, bf16[2048,256]{1,0:T(8,128)(2,1)S(1)} %copy-done.2, bf16[128,256]{1,0:T(8,128)(2,1)S(1)} %get-tuple-element.63.refs_0_, ...), custom_call_target="tpu_custom_call" | custom-call | flops 268435456 | bytes 2097152 | tf_op jit(solution)/shard_map/pallas_call | solution.py:306
  82.1 0.5 collective-permute-start.16
  82.7 0.7 convert_add_fusion
  83.4 3.7 %collective-permute-done.16.refs_1_ = bf16[128,512]{1,0:T(8,128)(2,1)S(1)} collective-permute-done((bf16[128,512]{1,0:T(8,128)(2,1)S(1)}, bf16[128,512]{1,0:T(8,128)(2,1)S(1)}, u32[]{:S(2)}, u32[]{:S(2)}) %collective-permute-start.16) | collective-permute-done | bytes 131104 | tf_op jit(solution)/shard_map/ppermute | solution.py:24
  87.1 2.6 %shard_map.121 = bf16[128,2048]{1,0:T(8,128)(2,1)} custom-call(s32[1]{0:T(128)} %bitcast.idx_ref, bf16[128,2048]{1,0:T(8,128)(2,1)S(1)} %copy-done.5, f32[1,2048]{1,0:T(1,128)S(1)} %bitcast.8, bf16[128,512]{1,0:T(8,128)(2,1)S(1)} %get-tuple-element.54.refs_0_, bf16[128,512]{1,0:T(8,128)(2,1)S(1)} %collective-permute-done.16.refs_1_, ...), custom_call_target="tpu_custom_call" | custom-call | flops 536870912 | bytes 2097152 | tf_op jit(solution)/shard_map/pallas_call | solution.py:306
  (49 shorter events, 0.3 us)
Async XLA Ops:
  3.7 14.0 %copy-start.3 = (bf16[128,512]{1,0:T(8,128)(2,1)S(1)}, bf16[128,512]{1,0:T(8,128)(2,1)}, u32[]{:S(2)}) copy-start(bf16[128,512]{1,0:T(8,128)(2,1)} %refs_4_.5) | copy-start | bytes 393220
  3.8 23.6 %copy-start = (bf16[2048,512]{1,0:T(8,128)(2,1)S(1)}, bf16[2048,512]{1,0:T(8,128)(2,1)}, u32[]{:S(2)}) copy-start(bf16[2048,512]{1,0:T(8,128)(2,1)} %refs_2_.1) | copy-start | bytes 6291460
  3.8 14.0 %collective-permute-start.2 = (bf16[144,512]{1,0:T(8,128)(2,1)}, bf16[144,512]{1,0:T(8,128)(2,1)S(1)}, u32[]{:S(2)}, u32[]{:S(2)}) collective-permute-start(bf16[144,512]{1,0:T(8,128)(2,1)} %get-tuple-element.39.refs_2_.refs_0_), channel_id=1, source_target_pairs={{0,2},{2,0},{4,6},{6,4},{8,10},{10,8},{12,14},{14,12},{16,18},{18,... | collective-permute-start | bytes 442376 | tf_op jit(solution)/shard_map/ppermute | solution.py:24
  4.3 15.0 %collective-permute-start.3 = (bf16[144,512]{1,0:T(8,128)(2,1)}, bf16[144,512]{1,0:T(8,128)(2,1)S(1)}, u32[]{:S(2)}, u32[]{:S(2)}) collective-permute-start(bf16[144,512]{1,0:T(8,128)(2,1)} %get-tuple-element.39.refs_2_.refs_0_), channel_id=1, source_target_pairs={{0,4},{2,6},{4,0},{6,2},{8,12},{10,14},{12,8},{14,10},{16,20},{18,... | collective-permute-start | bytes 442376 | tf_op jit(solution)/shard_map/ppermute | solution.py:24
  6.9 12.7 %collective-permute-start.4 = (bf16[144,512]{1,0:T(8,128)(2,1)}, bf16[144,512]{1,0:T(8,128)(2,1)S(1)}, u32[]{:S(2)}, u32[]{:S(2)}) collective-permute-start(bf16[144,512]{1,0:T(8,128)(2,1)} %get-tuple-element.39.refs_2_.refs_0_), channel_id=1, source_target_pairs={{0,6},{2,4},{4,2},{6,0},{8,14},{10,12},{12,10},{14,8},{16,22},{18,... | collective-permute-start | bytes 442376 | tf_op jit(solution)/shard_map/ppermute | solution.py:24
  6.9 25.5 %copy-start.6 = (bf16[144,512]{1,0:T(8,128)(2,1)S(1)}, bf16[144,512]{1,0:T(8,128)(2,1)}, u32[]{:S(2)}) copy-start(bf16[144,512]{1,0:T(8,128)(2,1)} %get-tuple-element.39.refs_2_.refs_0_) | copy-start | bytes 442372
  10.3 4.6 %collective-permute-start = (bf16[128,256]{1,0:T(8,128)(2,1)}, bf16[128,256]{1,0:T(8,128)(2,1)S(1)}, u32[]{:S(2)}, u32[]{:S(2)}) collective-permute-start(bf16[128,256]{1,0:T(8,128)(2,1)} %get-tuple-element.38), channel_id=1, source_target_pairs={{0,1},{1,0},{2,3},{3,2},{4,5},{5,4},{6,7},{7,6},{8,9},{9,8},{10,11... | collective-permute-start | bytes 196616 | tf_op jit(solution)/shard_map/ppermute | solution.py:24
  14.9 8.9 %collective-permute-start.5 = (bf16[256,256]{1,0:T(8,128)(2,1)S(1)}, bf16[256,256]{1,0:T(8,128)(2,1)S(1)}, u32[]{:S(2)}, u32[]{:S(2)}) collective-permute-start(bf16[256,256]{1,0:T(8,128)(2,1)S(1)} %constant_dynamic-update-slice_fusion.refs_0_), channel_id=1, source_target_pairs={{0,16},{2,18},{4,20},{6,22},{8,24},{10,26},{12,28},{14,30},{16,0},... | collective-permute-start | bytes 393224 | tf_op jit(solution)/shard_map/ppermute | solution.py:24
  17.8 17.9 %collective-permute-start.10 = (bf16[128,512]{1,0:T(8,128)(2,1)S(1)}, bf16[128,512]{1,0:T(8,128)(2,1)S(1)}, u32[]{:S(2)}, u32[]{:S(2)}) collective-permute-start(bf16[128,512]{1,0:T(8,128)(2,1)S(1)} %copy-done.3), channel_id=1, source_target_pairs={{0,2},{2,0},{4,6},{6,4},{8,10},{10,8},{12,14},{14,12},{16,18},{18,... | collective-permute-start | bytes 393224 | tf_op jit(solution)/shard_map/ppermute | solution.py:24
  17.8 19.4 %collective-permute-start.11 = (bf16[128,512]{1,0:T(8,128)(2,1)S(1)}, bf16[128,512]{1,0:T(8,128)(2,1)S(1)}, u32[]{:S(2)}, u32[]{:S(2)}) collective-permute-start(bf16[128,512]{1,0:T(8,128)(2,1)S(1)} %copy-done.3), channel_id=1, source_target_pairs={{0,4},{2,6},{4,0},{6,2},{8,12},{10,14},{12,8},{14,10},{16,20},{18,... | collective-permute-start | bytes 393224 | tf_op jit(solution)/shard_map/ppermute | solution.py:24
  19.4 18.1 %collective-permute-start.12 = (bf16[128,512]{1,0:T(8,128)(2,1)S(1)}, bf16[128,512]{1,0:T(8,128)(2,1)S(1)}, u32[]{:S(2)}, u32[]{:S(2)}) collective-permute-start(bf16[128,512]{1,0:T(8,128)(2,1)S(1)} %copy-done.3), channel_id=1, source_target_pairs={{0,6},{2,4},{4,2},{6,0},{8,14},{10,12},{12,10},{14,8},{16,22},{18,... | collective-permute-start | bytes 393224 | tf_op jit(solution)/shard_map/ppermute | solution.py:24
  19.6 14.3 %collective-permute-start.6 = (bf16[256,256]{1,0:T(8,128)(2,1)S(1)}, bf16[256,256]{1,0:T(8,128)(2,1)S(1)}, u32[]{:S(2)}, u32[]{:S(2)}) collective-permute-start(bf16[256,256]{1,0:T(8,128)(2,1)S(1)} %constant_dynamic-update-slice_fusion.refs_0_), channel_id=1, source_target_pairs={{0,24},{2,26},{4,28},{6,30},{8,16},{10,18},{12,20},{14,22},{16,8},... | collective-permute-start | bytes 393224 | tf_op jit(solution)/shard_map/ppermute | solution.py:24
  23.9 7.1 %collective-permute-start.1 = (bf16[256,256]{1,0:T(8,128)(2,1)S(1)}, bf16[256,256]{1,0:T(8,128)(2,1)S(1)}, u32[]{:S(2)}, u32[]{:S(2)}) collective-permute-start(bf16[256,256]{1,0:T(8,128)(2,1)S(1)} %constant_dynamic-update-slice_fusion.refs_0_), channel_id=1, source_target_pairs={{0,8},{2,10},{4,12},{6,14},{8,0},{10,2},{12,4},{14,6},{16,24},{18,... | collective-permute-start | bytes 393224 | tf_op jit(solution)/shard_map/ppermute | solution.py:24
  31.0 24.4 %collective-permute-start.17 = (bf16[1024,512]{1,0:T(8,128)(2,1)S(1)}, bf16[1024,512]{1,0:T(8,128)(2,1)S(1)}, u32[]{:S(2)}, u32[]{:S(2)}) collective-permute-start(bf16[1024,512]{1,0:T(8,128)(2,1)S(1)} %constant_dynamic-slice_fusion), channel_id=1, source_target_pairs={{0,1},{1,0},{2,3},{3,2},{4,5},{5,4},{6,7},{7,6},{8,9},{9,8},{10,11... | collective-permute-start | bytes 3145736 | tf_op jit(solution)/shard_map/ppermute | solution.py:24
  35.6 7.0 %collective-permute-start.7 = (f32[8,512]{1,0:T(8,128)S(1)}, f32[8,512]{1,0:T(8,128)S(1)}, u32[]{:S(2)}, u32[]{:S(2)}) collective-permute-start(f32[8,512]{1,0:T(8,128)S(1)} %shard_map.116), channel_id=1, source_target_pairs={{0,2},{2,0},{4,6},{6,4},{8,10},{10,8},{12,14},{14,12},{16,18},{18,... | collective-permute-start | bytes 49160 | tf_op jit(solution)/shard_map/ppermute | solution.py:24
  35.6 6.9 %collective-permute-start.8 = (f32[8,512]{1,0:T(8,128)S(1)}, f32[8,512]{1,0:T(8,128)S(1)}, u32[]{:S(2)}, u32[]{:S(2)}) collective-permute-start(f32[8,512]{1,0:T(8,128)S(1)} %shard_map.116), channel_id=1, source_target_pairs={{0,4},{2,6},{4,0},{6,2},{8,12},{10,14},{12,8},{14,10},{16,20},{18,... | collective-permute-start | bytes 49160 | tf_op jit(solution)/shard_map/ppermute | solution.py:24
  37.2 5.3 %collective-permute-start.9 = (f32[8,512]{1,0:T(8,128)S(1)}, f32[8,512]{1,0:T(8,128)S(1)}, u32[]{:S(2)}, u32[]{:S(2)}) collective-permute-start(f32[8,512]{1,0:T(8,128)S(1)} %shard_map.116), channel_id=1, source_target_pairs={{0,6},{2,4},{4,2},{6,0},{8,14},{10,12},{12,10},{14,8},{16,22},{18,... | collective-permute-start | bytes 49160 | tf_op jit(solution)/shard_map/ppermute | solution.py:24
  40.0 3.3 %copy-start.10 = (bf16[1024,128]{1,0:T(8,128)(2,1)S(1)}, bf16[1024,128]{1,0:T(8,128)(2,1)}, u32[]{:S(2)}) copy-start(bf16[1024,128]{1,0:T(8,128)(2,1)} %get-tuple-element.53) | copy-start | bytes 786436
  42.5 14.8 %copy-start.7 = (bf16[1024,128]{1,0:T(8,128)(2,1)S(1)}, bf16[1024,128]{1,0:T(8,128)(2,1)}, u32[]{:S(2)}) copy-start(bf16[1024,128]{1,0:T(8,128)(2,1)} %get-tuple-element.52.near_ref) | copy-start | bytes 786436
  42.9 1.9 %collective-permute-start.13 = (bf16[256,512]{1,0:T(8,128)(2,1)S(1)}, bf16[256,512]{1,0:T(8,128)(2,1)S(1)}, u32[]{:S(2)}, u32[]{:S(2)}) collective-permute-start(bf16[256,512]{1,0:T(8,128)(2,1)S(1)} %get-tuple-element.51), channel_id=1, source_target_pairs={{0,2},{2,0},{4,6},{6,4},{8,10},{10,8},{12,14},{14,12},{16,18},{18,... | collective-permute-start | bytes 786440 | tf_op jit(solution)/shard_map/ppermute | solution.py:24
  43.3 12.1 %collective-permute-start.15 = (bf16[1024,128]{1,0:T(8,128)(2,1)S(1)}, bf16[1024,128]{1,0:T(8,128)(2,1)S(1)}, u32[]{:S(2)}, u32[]{:S(2)}) collective-permute-start(bf16[1024,128]{1,0:T(8,128)(2,1)S(1)} %copy-done.10), channel_id=1, source_target_pairs={{0,4},{2,6},{4,0},{6,2},{8,12},{10,14},{12,8},{14,10},{16,20},{18,... | collective-permute-start | bytes 786440 | tf_op jit(solution)/shard_map/ppermute | solution.py:24
  44.9 12.4 %collective-permute-start.14 = (bf16[256,512]{1,0:T(8,128)(2,1)S(1)}, bf16[256,512]{1,0:T(8,128)(2,1)S(1)}, u32[]{:S(2)}, u32[]{:S(2)}) collective-permute-start(bf16[256,512]{1,0:T(8,128)(2,1)S(1)} %add_convert_fusion.pair_ref), channel_id=1, source_target_pairs={{0,4},{2,6},{4,0},{6,2},{8,12},{10,14},{12,8},{14,10},{16,20},{18,... | collective-permute-start | bytes 786440 | tf_op jit(solution)/shard_map/ppermute | solution.py:24
  55.4 31.7 %collective-permute-start.18 = (bf16[1024,512]{1,0:T(8,128)(2,1)S(1)}, bf16[1024,512]{1,0:T(8,128)(2,1)S(1)}, u32[]{:S(2)}, u32[]{:S(2)}) collective-permute-start(bf16[1024,512]{1,0:T(8,128)(2,1)S(1)} %collective-permute-done.17.refs_3_), channel_id=1, source_target_pairs={{0,2},{2,0},{4,6},{6,4},{8,10},{10,8},{12,14},{14,12},{16,18},{18,... | collective-permute-start | bytes 3145736 | tf_op jit(solution)/shard_map/ppermute | solution.py:24
  57.6 4.5 %collective-permute-start.23 = (bf16[512,512]{1,0:T(8,128)(2,1)S(1)}, bf16[512,512]{1,0:T(8,128)(2,1)S(1)}, u32[]{:S(2)}, u32[]{:S(2)}) collective-permute-start(bf16[512,512]{1,0:T(8,128)(2,1)S(1)} %get-tuple-element.66), channel_id=1, source_target_pairs={{0,2},{2,0},{4,6},{6,4},{8,10},{10,8},{12,14},{14,12},{16,18},{18,... | collective-permute-start | bytes 1572872 | tf_op jit(solution)/shard_map/ppermute | solution.py:24
  60.3 20.0 %copy-start.1 = (bf16[2048,256]{1,0:T(8,128)(2,1)S(1)}, bf16[2048,256]{1,0:T(8,128)(2,1)}, u32[]{:S(2)}) copy-start(bf16[2048,256]{1,0:T(8,128)(2,1)} %wk_ref.1) | copy-start | bytes 3145732
  60.3 19.9 %copy-start.2 = (bf16[2048,256]{1,0:T(8,128)(2,1)S(1)}, bf16[2048,256]{1,0:T(8,128)(2,1)}, u32[]{:S(2)}) copy-start(bf16[2048,256]{1,0:T(8,128)(2,1)} %wv_ref.1) | copy-start | bytes 3145732
  60.3 19.9 %copy-start.4 = (bf16[128,2048]{1,0:T(8,128)(2,1)S(1)}, bf16[128,2048]{1,0:T(8,128)(2,1)}, u32[]{:S(2)}) copy-start(bf16[128,2048]{1,0:T(8,128)(2,1)} %x_ref.3) | copy-start | bytes 1572868
  60.3 19.9 %copy-start.8 = (f32[2048]{0:T(1024)S(1)}, f32[2048]{0:T(1024)}, u32[]{:S(2)}) copy-start(f32[2048]{0:T(1024)} %param.12) | copy-start | bytes 24580
  60.3 6.4 %collective-permute-start.20 = (bf16[256,256]{1,0:T(8,128)(2,1)S(1)}, bf16[256,256]{1,0:T(8,128)(2,1)S(1)}, u32[]{:S(2)}, u32[]{:S(2)}) collective-permute-start(bf16[256,256]{1,0:T(8,128)(2,1)S(1)} %get-tuple-element.62), channel_id=1, source_target_pairs={{0,8},{2,10},{4,12},{6,14},{8,0},{10,2},{12,4},{14,6},{16,24},{18,... | collective-permute-start | bytes 393224 | tf_op jit(solution)/shard_map/ppermute | solution.py:24
  62.4 9.5 %collective-permute-start.25 = (bf16[128,512]{1,0:T(8,128)(2,1)S(1)}, bf16[128,512]{1,0:T(8,128)(2,1)S(1)}, u32[]{:S(2)}, u32[]{:S(2)}) collective-permute-start(bf16[128,512]{1,0:T(8,128)(2,1)S(1)} %get-tuple-element.70), channel_id=1, source_target_pairs={{0,8},{2,10},{4,12},{6,14},{8,0},{10,2},{12,4},{14,6},{16,24},{18,... | collective-permute-start | bytes 393224 | tf_op jit(solution)/shard_map/ppermute | solution.py:24
  62.8 13.1 %collective-permute-start.19 = (bf16[256,256]{1,0:T(8,128)(2,1)S(1)}, bf16[256,256]{1,0:T(8,128)(2,1)S(1)}, u32[]{:S(2)}, u32[]{:S(2)}) collective-permute-start(bf16[256,256]{1,0:T(8,128)(2,1)S(1)} %get-tuple-element.60), channel_id=1, source_target_pairs={{0,8},{2,10},{4,12},{6,14},{8,0},{10,2},{12,4},{14,6},{16,24},{18,... | collective-permute-start | bytes 393224 | tf_op jit(solution)/shard_map/ppermute | solution.py:24
  66.8 9.1 %collective-permute-start.21 = (bf16[256,256]{1,0:T(8,128)(2,1)S(1)}, bf16[256,256]{1,0:T(8,128)(2,1)S(1)}, u32[]{:S(2)}, u32[]{:S(2)}) collective-permute-start(bf16[256,256]{1,0:T(8,128)(2,1)S(1)} %shard_map.123), channel_id=1, source_target_pairs={{0,16},{2,18},{4,20},{6,22},{8,24},{10,26},{12,28},{14,30},{16,0},... | collective-permute-start | bytes 393224 | tf_op jit(solution)/shard_map/ppermute | solution.py:24
  70.2 12.4 %collective-permute-start.24 = (bf16[128,512]{1,0:T(8,128)(2,1)S(1)}, bf16[128,512]{1,0:T(8,128)(2,1)S(1)}, u32[]{:S(2)}, u32[]{:S(2)}) collective-permute-start(bf16[128,512]{1,0:T(8,128)(2,1)S(1)} %get-tuple-element.68), channel_id=1, source_target_pairs={{0,8},{2,10},{4,12},{6,14},{8,0},{10,2},{12,4},{14,6},{16,24},{18,... | collective-permute-start | bytes 393224 | tf_op jit(solution)/shard_map/ppermute | solution.py:24
  72.0 10.7 %collective-permute-start.26 = (bf16[128,512]{1,0:T(8,128)(2,1)S(1)}, bf16[128,512]{1,0:T(8,128)(2,1)S(1)}, u32[]{:S(2)}, u32[]{:S(2)}) collective-permute-start(bf16[128,512]{1,0:T(8,128)(2,1)S(1)} %shard_map.127), channel_id=1, source_target_pairs={{0,16},{2,18},{4,20},{6,22},{8,24},{10,26},{12,28},{14,30},{16,0},... | collective-permute-start | bytes 393224 | tf_op jit(solution)/shard_map/ppermute | solution.py:24
  75.9 4.3 %collective-permute-start.22 = (bf16[128,256]{1,0:T(8,128)(2,1)S(1)}, bf16[128,256]{1,0:T(8,128)(2,1)S(1)}, u32[]{:S(2)}, u32[]{:S(2)}) collective-permute-start(bf16[128,256]{1,0:T(8,128)(2,1)S(1)} %get-tuple-element.64), channel_id=1, source_target_pairs={{0,1},{1,0},{2,3},{3,2},{4,5},{5,4},{6,7},{7,6},{8,9},{9,8},{10,11... | collective-permute-start | bytes 196616 | tf_op jit(solution)/shard_map/ppermute | solution.py:24
  80.3 6.8 %copy-start.5 = (bf16[128,2048]{1,0:T(8,128)(2,1)S(1)}, bf16[128,2048]{1,0:T(8,128)(2,1)}, u32[]{:S(2)}) copy-start(bf16[128,2048]{1,0:T(8,128)(2,1)} %x_ref.2) | copy-start | bytes 1572868
  80.3 6.8 %copy-start.9 = (f32[2048]{0:T(1024)S(1)}, f32[2048]{0:T(1024)}, u32[]{:S(2)}) copy-start(f32[2048]{0:T(1024)} %param.11) | copy-start | bytes 24580
  82.1 5.0 %collective-permute-start.16 = (bf16[128,512]{1,0:T(8,128)(2,1)S(1)}, bf16[128,512]{1,0:T(8,128)(2,1)S(1)}, u32[]{:S(2)}, u32[]{:S(2)}) collective-permute-start(bf16[128,512]{1,0:T(8,128)(2,1)S(1)} %get-tuple-element.54.refs_0_), channel_id=1, source_target_pairs={{0,1},{1,0},{2,3},{3,2},{4,5},{5,4},{6,7},{7,6},{8,9},{9,8},{10,11... | collective-permute-start | bytes 393224 | tf_op jit(solution)/shard_map/ppermute | solution.py:24

commit v2 on v1

--- a/solution.py
+++ b/solution.py
@@ -154,80 +154,83 @@
 def grads_kernel(nb, rows, v_ref, kt_ref, p_ref, *refs):
     qs, gs = refs[:nb], refs[nb : 2 * nb]
     ds_ref, dq_ref = refs[2 * nb :]
-    for h in range(p_ref.shape[0]):
+    items = [(h, pair) for h in range(p_ref.shape[0]) for pair in range(nb // 2)]
+
+    def d_weights(h, pair):
         lanes = slice(h * HD, (h + 1) * HD)
-        for pair in range(nb // 2):
-            both = (2 * pair, 2 * pair + 1)
-            g = jnp.concatenate([gs[i][:, lanes] for i in both], axis=0)
-            delta = jnp.concatenate([qs[i][rows : rows + 1, lanes] for i in both], axis=1).astype(F32)
-            cols = slice(pair * 2 * rows, (pair + 1) * 2 * rows)
-            dw = dot(v_ref[...], g, 1, 1)
-            ds = (p_ref[h, :, cols].astype(F32) * (dw - delta)).astype(BF16)
-            ds_ref[h, :, cols] = ds
-            dq_ref[h, :, cols] = dot(kt_ref[...], ds, 1, 0)
-
-
-def lse_kernel(heads, a_ref, b_ref, o_ref):
+        g = jnp.concatenate([gs[2 * pair + i][:, lanes] for i in range(2)], axis=0)
+        return dot(v_ref[...], g, 1, 1)
+
+    ahead = d_weights(*items[0])
+    for n, (h, pair) in enumerate(items):
+        lanes = slice(h * HD, (h + 1) * HD)
+        cols = slice(pair * 2 * rows, (pair + 1) * 2 * rows)
+        delta = jnp.concatenate(
+            [qs[2 * pair + i][rows : rows + 1, lanes] for i in range(2)], axis=1
+        ).astype(F32)
+        ds = (p_ref[h, :, cols].astype(F32) * (ahead - delta)).astype(BF16)
+        ds_ref[h, :, cols] = ds
+        if n + 1 < len(items):
+            ahead = d_weights(*items[n + 1])
+        dq_ref[h, :, cols] = dot(kt_ref[...], ds, 1, 0)
+
+
+def lse_kernel(heads, *refs):
+    o_ref = refs[-1]
     o_ref[...] = jnp.zeros_like(o_ref)
     for h in range(heads):
-        ta, tb = a_ref[h, 0:1, :], b_ref[h, 0:1, :]
-        top = jnp.maximum(ta, tb)
-        total = a_ref[h, 1:2, :] * jnp.exp2(ta - top) + b_ref[h, 1:2, :] * jnp.exp2(tb - top)
+        tops = [r[h, 0:1, :] for r in refs[:-1]]
+        top = functools.reduce(jnp.maximum, tops)
+        total = sum(r[h, 1:2, :] * jnp.exp2(t - top) for r, t in zip(refs[:-1], tops))
         o_ref[h : h + 1, :] = top
         o_ref[heads + h : heads + h + 1, :] = total
 
 
-def scale_kernel(nb, rows, heads, scaling, *refs):
-    own_a, own_b = refs[:2]
-    sts = refs[2 : nb + 1]
-    dqa_ref, dqb_ref, c_ref, sent_ref, kept_ref = refs[nb + 1 :]
+def scale_kernel(nc, nb, rows, heads, scaling, *refs):
+    owns, sts, dqs = refs[:nc], refs[nc : nc + nb - 1], refs[nc + nb - 1 : 2 * nc + nb - 1]
+    c_ref, sent_ref, kept_ref = refs[2 * nc + nb - 1 :]
     places = [(kept_ref, 0), (sent_ref, 0), (kept_ref, 1), (sent_ref, 1)]
     for h in range(heads):
-        tops = [own_a[h, 0:1, :], own_b[h, 0:1, :]]
-        sums = [own_a[h, 1:2, :], own_b[h, 1:2, :]]
+        tops = [r[h, 0:1, :] for r in owns]
+        sums = [r[h, 1:2, :] for r in owns]
         for k in range(1, nb):
             order = [slice((j ^ k) * rows, (j ^ k) * rows + rows) for j in range(nb)]
-            st = sts[k - 1]
+            st, low = sts[k - 1], heads + h
             tops.append(jnp.concatenate([st[h : h + 1, o] for o in order], axis=1))
-            low = heads + h
             sums.append(jnp.concatenate([st[low : low + 1, o] for o in order], axis=1))
         top = functools.reduce(jnp.maximum, tops)
         total = sum(s * jnp.exp2(t - top) for t, s in zip(tops, sums))
-        ca = jnp.exp2(tops[0] - top) / total
-        cb = jnp.exp2(tops[1] - top) / total
-        c_ref[h, 0:1, :] = ca
-        c_ref[h, 1:2, :] = cb
+        cs = [jnp.exp2(t - top) / total for t in tops[:nc]]
+        for i, c in enumerate(cs):
+            c_ref[h, i : i + 1, :] = c
         for k in range(nb):
             part = slice(k * rows, (k + 1) * rows)
-            block = dqa_ref[h, :, part] * (ca[:, part] * scaling)
-            block = block + dqb_ref[h, :, part] * (cb[:, part] * scaling)
+            block = sum(r[h, :, part] * (c[:, part] * scaling) for r, c in zip(dqs, cs))
             ref, spot = places[k]
             ref[spot * rows : (spot + 1) * rows, h * HD : (h + 1) * HD] = block.T.astype(ref.dtype)
 
 
-def keyvalue_kernel(nz, nb, rows, scaling, *refs):
-    qs, gs = refs[:nb], refs[nb : 2 * nb]
-    c_ref, pa_ref, pb_ref, dsa_ref, dsb_ref = refs[2 * nb : 2 * nb + 5]
-    outs = refs[2 * nb + 5 :]
+def keyvalue_kernel(places, nc, nb, rows, scaling, *refs):
+    qs, gs, c_ref = refs[:nb], refs[nb : 2 * nb], refs[2 * nb]
+    ps, dss = refs[2 * nb + 1 : 2 * nb + 1 + nc], refs[2 * nb + 1 + nc : 2 * nb + 1 + 2 * nc]
+    outs = refs[2 * nb + 1 + 2 * nc :]
     size = outs[0].shape[0]
-    for i, (p_ref, ds_ref) in enumerate(((pa_ref, dsa_ref), (pb_ref, dsb_ref))):
-        count = p_ref.shape[1] // size
-        key_acc, value_acc = [None] * count, [None] * count
-        for h in range(p_ref.shape[0]):
-            lanes = slice(h * HD, (h + 1) * HD)
-            c = c_ref[h, i : i + 1, :].astype(BF16)
-            q = jnp.concatenate([m[:rows, lanes] for m in qs], axis=0)
-            g = jnp.concatenate([m[:, lanes] for m in gs], axis=0)
-            for z in range(count):
-                part = slice(z * size, (z + 1) * size)
-                key = dot(ds_ref[h, part, :] * c, q, 1, 0)
-                value = dot(p_ref[h, part, :] * c, g, 1, 0)
-                key_acc[z] = key if h == 0 else key_acc[z] + key
-                value_acc[z] = value if h == 0 else value_acc[z] + value
-        for z in range(count):
-            out = outs[i * (nz // 2) + z]
-            out[:, :HD] = (key_acc[z] * scaling).astype(out.dtype)
-            out[:, HD:] = value_acc[z].astype(out.dtype)
+    count = len(places)
+    key_acc, value_acc = [None] * count, [None] * count
+    for h in range(ps[0].shape[0]):
+        lanes = slice(h * HD, (h + 1) * HD)
+        q = jnp.concatenate([m[:rows, lanes] for m in qs], axis=0)
+        g = jnp.concatenate([m[:, lanes] for m in gs], axis=0)
+        for i, (chunk, spot) in enumerate(places):
+            c = c_ref[h, chunk : chunk + 1, :].astype(BF16)
+            part = slice(spot * size, (spot + 1) * size)
+            key = dot(dss[chunk][h, part, :] * c, q, 1, 0)
+            value = dot(ps[chunk][h, part, :] * c, g, 1, 0)
+            key_acc[i] = key if h == 0 else key_acc[i] + key
+            value_acc[i] = value if h == 0 else value_acc[i] + value
+    for i, out in enumerate(outs):
+        out[:, :HD] = (key_acc[i] * scaling).astype(out.dtype)
+        out[:, HD:] = value_acc[i].astype(out.dtype)
 
 
 def first_kernel(nz, dblk, rows, pair_ref, other_ref, near_ref, far_ref, dq_ref, own_ref, o_ref):
@@ -392,10 +395,14 @@
 
     rest = [swap(by_head[d // group], "tp", d) for d in range(1, tp)]
     kv_own = jnp.concatenate([by_head[0]] + rest, axis=0)
-    chunks = [range(nz // 2), range(nz // 2, nz)]
-    kvs = []
-    for ks in chunks:
-        kvs.append([kv_own if k == 0 else away(kv_own, k) for k in ks])
+    late = list(range(nz // 2 + 1, nz, 2))
+    chunks = [[k for k in range(nz) if k not in late], late]
+    chunk_of = {k: c for c, ks in enumerate(chunks) for k in ks}
+    at_hand = {0: kv_own}
+    for k in list(range(2, nz, 2)) + list(range(1, nz, 2)):
+        at_hand[k] = away(at_hand[k - 1] if k % 2 else kv_own, k, 1 if k % 2 else k)
+    kvs = [[at_hand[k] for k in ks] for ks in chunks]
+
     qs = [q_ext] + [swap(q_ext, "sp", k) for k in range(1, nb)]
     gs = [d_attended] + [swap(d_attended, "sp", k) for k in range(1, nb)]
     far = swap(far, "sp", half)
@@ -432,24 +439,33 @@
             flops=6 * probs.size * HD,
         )
 
-    p_a, st_a, _, v_a, kt_a = scores(0)
-    ds_a, dq_a = grads(p_a, v_a, kt_a)
-    p_b, st_b, _, v_b, kt_b = scores(1)
-    stats = call(functools.partial(lse_kernel, heads), shape((8 * -(-heads // 4), trows), F32), (st_a, st_b), mib=1)
+    nc = len(chunks)
+    probs, own_stats, _, values, keys_t = zip(*[scores(c) for c in range(nc)])
+    stats = call(
+        functools.partial(lse_kernel, heads),
+        shape((8 * -(-heads // 4), trows), F32),
+        own_stats,
+        mib=1,
+    )
     sts = [swap(stats, "sp", k) for k in range(1, nb)]
-    ds_b, dq_b = grads(p_b, v_b, kt_b)
+    d_scores, dq_parts = zip(*[grads(probs[c], values[c], keys_t[c]) for c in range(nc)])
     coef, sent, kept = call(
-        functools.partial(scale_kernel, nb, rows, heads, scaling),
+        functools.partial(scale_kernel, nc, nb, rows, heads, scaling),
         [stshape, shape((2 * rows, width), BF16), shape((2 * rows, width), F32)],
-        (st_a, st_b, *sts, dq_a, dq_b),
+        (*own_stats, *sts, *dq_parts),
     )
     src = tp * srows
-    dkvs = call(
-        functools.partial(keyvalue_kernel, nz, nb, rows, scaling),
-        [shape((src, 2 * HD), BF16 if z % 2 else F32) for z in range(nz)],
-        (*qs, *gs, coef, p_a, p_b, ds_a, ds_b),
-        flops=6 * heads * nz * src * trows * HD,
-    )
+    dkvs = [None] * nz
+    for ks in (range(1, nz, 2), range(0, nz, 2)):
+        places = [(chunk_of[k], chunks[chunk_of[k]].index(k)) for k in ks]
+        results = call(
+            functools.partial(keyvalue_kernel, places, nc, nb, rows, scaling),
+            [shape((src, 2 * HD), BF16 if k % 2 else F32) for k in ks],
+            (*qs, *gs, coef, *probs, *d_scores),
+            flops=3 * heads * nz * src * trows * HD,
+        )
+        for k, x in zip(ks, results):
+            dkvs[k] = x
 
     pair_b = (kept + swap(sent, "sp", 1).astype(F32)).astype(BF16)
     other = swap(pair_b, "sp", half)

time: 90.7 us -> 85.7 us (0.945)
  starting transfers between devices: 32.4 us -> 28.8 us
  Pallas kernels: 22.6 us -> 20.7 us
  waiting for transfers between devices: 32 us -> 33.3 us
    ppermute x27, starting transfers between devices: 32.4 us -> 28.8 us  [swap(): return lax.ppermute(x, axis, [(i, i ^ k) for i in range(n)])]
    pallas_call x16 -> x17, Pallas kernels: 22.6 us -> 20.7 us  [call(): pl.pallas_call(body, grid_spec=pltpu.PrefetchScalarGridSpec(num_scalar_pr...]
    ppermute x27, waiting for transfers between devices: 32 us -> 33.3 us  [swap(): return lax.ppermute(x, axis, [(i, i ^ k) for i in range(n)])]
  transfers between devices with their start and end apart: 27 -> 27, of which waited for: 9 -> 12; matrix products, arithmetic and copies ran while one was open for 2% -> 2% of each run, Pallas kernels for 19% -> 17%
where the time goes in v2:
time: 85.7 us; the launch traced here: 85.5 us
  waiting for transfers between devices  33.3 us (39%)
  starting transfers between devices  28.8 us (34%)
  Pallas kernels  20.7 us (24%)
  local copies, waits for them, and re-layouts  0.98 us (1%)
  between operations  0.92 us (1%)
    ppermute x27, waiting for transfers between devices, swap(): return lax.ppermute(x, axis, [(i, i ^ k) for i in range(n)])  33.3 us
    ppermute x27, starting transfers between devices, swap(): return lax.ppermute(x, axis, [(i, i ^ k) for i in range(n)])  28.8 us
    pallas_call x17, Pallas kernels, call(): pl.pallas_call(body, grid_spec=pltpu.PrefetchScalarGridSpec(num_scalar_pr...  20.7 us
  transfers between devices with their start and end apart: 27, of which 12 were waited for; matrix products, arithmetic and copies ran while one was open for 2% of the time, Pallas kernels for 17%

profile of v2, /device:TPU:0, one launch (start us, length us, event | category | flops | bytes accessed | tf_op | source)
XLA Modules:
  0.0 85.5 jit_solution(11613551136113124959)
XLA Ops:
  0.7 3.3 %shard_map.113 = (bf16[144,512]{1,0:T(8,128)(2,1)}, bf16[1024,128]{1,0:T(8,128)(2,1)}, bf16[1024,128]{1,0:T(8,128)(2,1)}) custom-call(s32[1]{0:T(128)} %bitcast.4.me_ref, bf16[128,2048]{1,0:T(8,128)(2,1)} %x_ref.2, f32[1,2048]{1,0:T(1,128)} %bitcast.7, bf16[2048,512]{1,0:T(8,128)(2,1)} %refs_2_.1, bf16[128,512]{1,0:T(8,128)(2,1)} %at_any.1, ...), custom_call_target="tpu_custom_call" | custom-call | flops 268435456 | bytes 2097152 | tf_op jit(solution)/shard_map/pallas_call | solution.py:309
  4.0 0.6 collective-permute-start.3
  4.5 2.6 %collective-permute-start.4 = (bf16[144,512]{1,0:T(8,128)(2,1)}, bf16[144,512]{1,0:T(8,128)(2,1)S(1)}, u32[]{:S(2)}, u32[]{:S(2)}) collective-permute-start(bf16[144,512]{1,0:T(8,128)(2,1)} %get-tuple-element.39.refs_3_.refs_1_.refs_0_), channel_id=1, source_target_pairs={{0,4},{2,6},{4,0},{6,2},{8,12},{10,14},{12,8},{14,10},{16,20},{18,... | collective-permute-start | bytes 442376 | tf_op jit(solution)/shard_map/ppermute | solution.py:24
  7.3 3.3 %shard_map.112 = (bf16[128,256]{1,0:T(8,128)(2,1)}, bf16[128,256]{1,0:T(8,128)(2,1)}) custom-call(s32[1]{0:T(128)} %bitcast.2.kv_ref.idx_ref, bf16[128,2048]{1,0:T(8,128)(2,1)} %x_ref.3, f32[1,2048]{1,0:T(1,128)} %bitcast.5, bf16[2048,256]{1,0:T(8,128)(2,1)} %wk_ref.1, bf16[2048,256]{1,0:T(8,128)(2,1)} %wv_ref.1), custom_call_target="tpu_custom_call" | custom-call | flops 268435456 | bytes 2097152 | tf_op jit(solution)/shard_map/pallas_call | solution.py:309
  10.6 2.0 %collective-permute-start = (bf16[128,256]{1,0:T(8,128)(2,1)}, bf16[128,256]{1,0:T(8,128)(2,1)S(1)}, u32[]{:S(2)}, u32[]{:S(2)}) collective-permute-start(bf16[128,256]{1,0:T(8,128)(2,1)} %get-tuple-element.38), channel_id=1, source_target_pairs={{0,1},{1,0},{2,3},{3,2},{4,5},{5,4},{6,7},{7,6},{8,9},{9,8},{10,11... | collective-permute-start | bytes 196616 | tf_op jit(solution)/shard_map/ppermute | solution.py:24
  12.6 0.8 constant_dynamic-update-slice_fusion.1
  13.4 1.8 %collective-permute-done = bf16[128,256]{1,0:T(8,128)(2,1)S(1)} collective-permute-done((bf16[128,256]{1,0:T(8,128)(2,1)}, bf16[128,256]{1,0:T(8,128)(2,1)S(1)}, u32[]{:S(2)}, u32[]{:S(2)}) %collective-permute-start) | collective-permute-done | bytes 65568 | tf_op jit(solution)/shard_map/ppermute | solution.py:24
  15.2 1.9 %collective-permute-start.11 = (bf16[128,512]{1,0:T(8,128)(2,1)S(1)}, bf16[128,512]{1,0:T(8,128)(2,1)S(1)}, u32[]{:S(2)}, u32[]{:S(2)}) collective-permute-start(bf16[128,512]{1,0:T(8,128)(2,1)S(1)} %copy-done.3), channel_id=1, source_target_pairs={{0,4},{2,6},{4,0},{6,2},{8,12},{10,14},{12,8},{14,10},{16,20},{18,... | collective-permute-start | bytes 393224 | tf_op jit(solution)/shard_map/ppermute | solution.py:24
  17.2 2.7 %collective-permute-start.2 = (bf16[256,256]{1,0:T(8,128)(2,1)S(1)}, bf16[256,256]{1,0:T(8,128)(2,1)S(1)}, u32[]{:S(2)}, u32[]{:S(2)}) collective-permute-start(bf16[256,256]{1,0:T(8,128)(2,1)S(1)} %constant_dynamic-update-slice_fusion.refs_0_), channel_id=1, source_target_pairs={{0,16},{2,18},{4,20},{6,22},{8,24},{10,26},{12,28},{14,30},{16,0},... | collective-permute-start | bytes 393224 | tf_op jit(solution)/shard_map/ppermute | solution.py:24
  19.9 1.6 %collective-permute-start.1 = (bf16[256,256]{1,0:T(8,128)(2,1)S(1)}, bf16[256,256]{1,0:T(8,128)(2,1)S(1)}, u32[]{:S(2)}, u32[]{:S(2)}) collective-permute-start(bf16[256,256]{1,0:T(8,128)(2,1)S(1)} %constant_dynamic-update-slice_fusion.refs_0_), channel_id=1, source_target_pairs={{0,8},{2,10},{4,12},{6,14},{8,0},{10,2},{12,4},{14,6},{16,24},{18,... | collective-permute-start | bytes 393224 | tf_op jit(solution)/shard_map/ppermute | solution.py:24
  21.5 5.5 %collective-permute-done.2.refs_2_ = bf16[256,256]{1,0:T(8,128)(2,1)S(1)} collective-permute-done((bf16[256,256]{1,0:T(8,128)(2,1)S(1)}, bf16[256,256]{1,0:T(8,128)(2,1)S(1)}, u32[]{:S(2)}, u32[]{:S(2)}) %collective-permute-start.2) | collective-permute-done | bytes 131104 | tf_op jit(solution)/shard_map/ppermute | solution.py:24
  27.0 1.5 %collective-permute-start.17 = (bf16[1024,512]{1,0:T(8,128)(2,1)S(1)}, bf16[1024,512]{1,0:T(8,128)(2,1)S(1)}, u32[]{:S(2)}, u32[]{:S(2)}) collective-permute-start(bf16[1024,512]{1,0:T(8,128)(2,1)S(1)} %constant_dynamic-slice_fusion), channel_id=1, source_target_pairs={{0,1},{1,0},{2,3},{3,2},{4,5},{5,4},{6,7},{7,6},{8,9},{9,8},{10,11... | collective-permute-start | bytes 3145736 | tf_op jit(solution)/shard_map/ppermute | solution.py:24
  28.5 0.6 collective-permute-start.6
  29.1 2.3 %shard_map.114 = (bf16[4,768,512]{2,1,0:T(8,128)(2,1)S(1)}, f32[4,8,512]{2,1,0:T(8,128)S(1)}, bf16[768,128]{1,0:T(8,128)(2,1)}, bf16[768,128]{1,0:T(8,128)(2,1)S(1)}, bf16[128,768]{1,0:T(8,128)(2,1)S(1)}) custom-call(bf16[256,256]{1,0:T(8,128)(2,1)S(1)} %constant_dynamic-update-slice_fusion.refs_0_, bf16[256,256]{1,0:T(8,128)(2,1)S(1)} %collective-permute-done.1.refs_1_, ...), custom_call_target="tpu_custom_call" | custom-call | flops 805306368 | bytes 2097152 | tf_op jit(solution)/shard_map/pallas_call | solution.py:309
  31.5 1.7 %shard_map.117 = (bf16[4,768,512]{2,1,0:T(8,128)(2,1)S(1)}, f32[4,128,512]{2,1,0:T(8,128)S(1)}) custom-call(bf16[768,128]{1,0:T(8,128)(2,1)S(1)} %get-tuple-element.42.v_ref, bf16[128,768]{1,0:T(8,128)(2,1)S(1)} %get-tuple-element.43.kt_ref, bf16[4,768,512]{2,1,0:T(8,128)(2,1)S(1)} %get-tuple-element.44.p_ref.refs_9_, bf16[144,512]{1,0:T(8,128)(2,1)S(1)} %copy-done.4, ...), custom_call_target="tpu_custom_call" | custom-call | flops 1207959552 | bytes 2097152 | tf_op jit(solution)/shard_map/pallas_call | solution.py:309
  33.2 0.3 collective-permute-done.6.refs_0_
  33.5 0.8 shard_map.115
  34.3 1.0 %collective-permute-start.8 = (f32[8,512]{1,0:T(8,128)S(1)}, f32[8,512]{1,0:T(8,128)S(1)}, u32[]{:S(2)}, u32[]{:S(2)}) collective-permute-start(f32[8,512]{1,0:T(8,128)S(1)} %shard_map.116), channel_id=1, source_target_pairs={{0,4},{2,6},{4,0},{6,2},{8,12},{10,14},{12,8},{14,10},{16,20},{18,... | collective-permute-start | bytes 49160 | tf_op jit(solution)/shard_map/ppermute | solution.py:24
  35.3 0.9 %collective-permute-start.9 = (f32[8,512]{1,0:T(8,128)S(1)}, f32[8,512]{1,0:T(8,128)S(1)}, u32[]{:S(2)}, u32[]{:S(2)}) collective-permute-start(f32[8,512]{1,0:T(8,128)S(1)} %shard_map.116), channel_id=1, source_target_pairs={{0,6},{2,4},{4,2},{6,0},{8,14},{10,12},{12,10},{14,8},{16,22},{18,... | collective-permute-start | bytes 49160 | tf_op jit(solution)/shard_map/ppermute | solution.py:24
  36.2 1.1 %shard_map.118 = (bf16[4,256,512]{2,1,0:T(8,128)(2,1)S(1)}, f32[4,128,512]{2,1,0:T(8,128)S(1)}) custom-call(bf16[256,128]{1,0:T(8,128)(2,1)S(1)} %get-tuple-element.46.v_ref, bf16[128,256]{1,0:T(8,128)(2,1)S(1)} %get-tuple-element.47.kt_ref, bf16[4,256,512]{2,1,0:T(8,128)(2,1)S(1)} %get-tuple-element.48.p_ref.refs_10_, bf16[144,512]{1,0:T(8,128)(2,1)S(1)} %copy-done.4, ...), custom_call_target="tpu_custom_call" | custom-call | flops 402653184 | bytes 2097152 | tf_op jit(solution)/shard_map/pallas_call | solution.py:309
  37.3 0.9 %collective-permute-done.8.refs_3_ = f32[8,512]{1,0:T(8,128)S(1)} collective-permute-done((f32[8,512]{1,0:T(8,128)S(1)}, f32[8,512]{1,0:T(8,128)S(1)}, u32[]{:S(2)}, u32[]{:S(2)}) %collective-permute-start.8) | collective-permute-done | bytes 16416 | tf_op jit(solution)/shard_map/ppermute | solution.py:24
  38.2 0.3 collective-permute-done.9.refs_4_
  38.5 0.3 shard_map.119
  38.8 0.5 collective-permute-start.13
  39.3 1.1 %collective-permute-start.15 = (bf16[1024,128]{1,0:T(8,128)(2,1)S(1)}, bf16[1024,128]{1,0:T(8,128)(2,1)S(1)}, u32[]{:S(2)}, u32[]{:S(2)}) collective-permute-start(bf16[1024,128]{1,0:T(8,128)(2,1)S(1)} %copy-done.10), channel_id=1, source_target_pairs={{0,4},{2,6},{4,0},{6,2},{8,12},{10,14},{12,8},{14,10},{16,20},{18,... | collective-permute-start | bytes 786440 | tf_op jit(solution)/shard_map/ppermute | solution.py:24
  40.6 1.2 %collective-permute-start.14 = (bf16[256,512]{1,0:T(8,128)(2,1)S(1)}, bf16[256,512]{1,0:T(8,128)(2,1)S(1)}, u32[]{:S(2)}, u32[]{:S(2)}) collective-permute-start(bf16[256,512]{1,0:T(8,128)(2,1)S(1)} %add_convert_fusion.pair_ref), channel_id=1, source_target_pairs={{0,4},{2,6},{4,0},{6,2},{8,12},{10,14},{12,8},{14,10},{16,20},{18,... | collective-permute-start | bytes 786440 | tf_op jit(solution)/shard_map/ppermute | solution.py:24
  41.8 6.8 %collective-permute-done.15.far_ref = bf16[1024,128]{1,0:T(8,128)(2,1)S(1)} collective-permute-done((bf16[1024,128]{1,0:T(8,128)(2,1)S(1)}, bf16[1024,128]{1,0:T(8,128)(2,1)S(1)}, u32[]{:S(2)}, u32[]{:S(2)}) %collective-permute-start.15) | collective-permute-done | bytes 262176 | tf_op jit(solution)/shard_map/ppermute | solution.py:24
  48.5 4.7 %collective-permute-done.14.other_ref = bf16[256,512]{1,0:T(8,128)(2,1)S(1)} collective-permute-done((bf16[256,512]{1,0:T(8,128)(2,1)S(1)}, bf16[256,512]{1,0:T(8,128)(2,1)S(1)}, u32[]{:S(2)}, u32[]{:S(2)}) %collective-permute-start.14) | collective-permute-done | bytes 262176 | tf_op jit(solution)/shard_map/ppermute | solution.py:24
  53.3 0.3 shard_map.120
  53.7 0.5 collective-permute-start.18
  54.2 1.2 %shard_map.123 = (bf16[256,256]{1,0:T(8,128)(2,1)S(1)}, bf16[256,256]{1,0:T(8,128)(2,1)S(1)}) custom-call(bf16[144,512]{1,0:T(8,128)(2,1)S(1)} %copy-done.4, bf16[144,512]{1,0:T(8,128)(2,1)S(1)} %collective-permute-done.3.refs_4_.refs_2_.refs_1_, bf16[144,512]{1,0:T(8,128)(2,1)S(1)} %collective-permute-done.4.refs_5_.refs_3_.refs_2_, ...), custom_call_target="tpu_custom_call" | custom-call | flops 805306368 | bytes 2097152 | tf_op jit(solution)/shard_map/pallas_call | solution.py:309
  55.4 1.0 %collective-permute-start.20 = (bf16[256,256]{1,0:T(8,128)(2,1)S(1)}, bf16[256,256]{1,0:T(8,128)(2,1)S(1)}, u32[]{:S(2)}, u32[]{:S(2)}) collective-permute-start(bf16[256,256]{1,0:T(8,128)(2,1)S(1)} %get-tuple-element.62), channel_id=1, source_target_pairs={{0,8},{2,10},{4,12},{6,14},{8,0},{10,2},{12,4},{14,6},{16,24},{18,... | collective-permute-start | bytes 393224 | tf_op jit(solution)/shard_map/ppermute | solution.py:24
  56.5 1.1 %collective-permute-start.19 = (bf16[256,256]{1,0:T(8,128)(2,1)S(1)}, bf16[256,256]{1,0:T(8,128)(2,1)S(1)}, u32[]{:S(2)}, u32[]{:S(2)}) collective-permute-start(bf16[256,256]{1,0:T(8,128)(2,1)S(1)} %get-tuple-element.60), channel_id=1, source_target_pairs={{0,8},{2,10},{4,12},{6,14},{8,0},{10,2},{12,4},{14,6},{16,24},{18,... | collective-permute-start | bytes 393224 | tf_op jit(solution)/shard_map/ppermute | solution.py:24
  57.5 0.3 shard_map.127
  57.9 1.0 %collective-permute-start.25 = (bf16[128,512]{1,0:T(8,128)(2,1)S(1)}, bf16[128,512]{1,0:T(8,128)(2,1)S(1)}, u32[]{:S(2)}, u32[]{:S(2)}) collective-permute-start(bf16[128,512]{1,0:T(8,128)(2,1)S(1)} %get-tuple-element.70), channel_id=1, source_target_pairs={{0,8},{2,10},{4,12},{6,14},{8,0},{10,2},{12,4},{14,6},{16,24},{18,... | collective-permute-start | bytes 393224 | tf_op jit(solution)/shard_map/ppermute | solution.py:24
  58.9 1.5 %shard_map.122 = (f32[256,256]{1,0:T(8,128)S(1)}, f32[256,256]{1,0:T(8,128)S(1)}) custom-call(bf16[144,512]{1,0:T(8,128)(2,1)S(1)} %copy-done.4, bf16[144,512]{1,0:T(8,128)(2,1)S(1)} %collective-permute-done.3.refs_4_.refs_2_.refs_1_, bf16[144,512]{1,0:T(8,128)(2,1)S(1)} %collective-permute-done.4.refs_5_.refs_3_.refs_2_, ...), custom_call_target="tpu_custom_call" | custom-call | flops 805306368 | bytes 2097152 | tf_op jit(solution)/shard_map/pallas_call | solution.py:309
  60.4 1.5 %collective-permute-done.20.refs_1_ = bf16[256,256]{1,0:T(8,128)(2,1)S(1)} collective-permute-done((bf16[256,256]{1,0:T(8,128)(2,1)S(1)}, bf16[256,256]{1,0:T(8,128)(2,1)S(1)}, u32[]{:S(2)}, u32[]{:S(2)}) %collective-permute-start.20) | collective-permute-done | bytes 131104 | tf_op jit(solution)/shard_map/ppermute | solution.py:24
  61.9 3.1 %collective-permute-start.21 = (bf16[256,256]{1,0:T(8,128)(2,1)S(1)}, bf16[256,256]{1,0:T(8,128)(2,1)S(1)}, u32[]{:S(2)}, u32[]{:S(2)}) collective-permute-start(bf16[256,256]{1,0:T(8,128)(2,1)S(1)} %shard_map.124), channel_id=1, source_target_pairs={{0,16},{2,18},{4,20},{6,22},{8,24},{10,26},{12,28},{14,30},{16,0},... | collective-permute-start | bytes 393224 | tf_op jit(solution)/shard_map/ppermute | solution.py:24
  65.0 1.1 %collective-permute-start.24 = (bf16[128,512]{1,0:T(8,128)(2,1)S(1)}, bf16[128,512]{1,0:T(8,128)(2,1)S(1)}, u32[]{:S(2)}, u32[]{:S(2)}) collective-permute-start(bf16[128,512]{1,0:T(8,128)(2,1)S(1)} %get-tuple-element.68), channel_id=1, source_target_pairs={{0,8},{2,10},{4,12},{6,14},{8,0},{10,2},{12,4},{14,6},{16,24},{18,... | collective-permute-start | bytes 393224 | tf_op jit(solution)/shard_map/ppermute | solution.py:24
  66.2 4.1 %collective-permute-done.25.refs_1_ = bf16[128,512]{1,0:T(8,128)(2,1)S(1)} collective-permute-done((bf16[128,512]{1,0:T(8,128)(2,1)S(1)}, bf16[128,512]{1,0:T(8,128)(2,1)S(1)}, u32[]{:S(2)}, u32[]{:S(2)}) %collective-permute-start.25) | collective-permute-done | bytes 131104 | tf_op jit(solution)/shard_map/ppermute | solution.py:24
  70.3 1.3 %collective-permute-start.26 = (bf16[128,512]{1,0:T(8,128)(2,1)S(1)}, bf16[128,512]{1,0:T(8,128)(2,1)S(1)}, u32[]{:S(2)}, u32[]{:S(2)}) collective-permute-start(bf16[128,512]{1,0:T(8,128)(2,1)S(1)} %shard_map.128), channel_id=1, source_target_pairs={{0,16},{2,18},{4,20},{6,22},{8,24},{10,26},{12,28},{14,30},{16,0},... | collective-permute-start | bytes 393224 | tf_op jit(solution)/shard_map/ppermute | solution.py:24
  71.7 0.6 collective-permute-start.22
  72.3 3.7 %collective-permute-done.22.refs_1_ = bf16[128,256]{1,0:T(8,128)(2,1)S(1)} collective-permute-done((bf16[128,256]{1,0:T(8,128)(2,1)S(1)}, bf16[128,256]{1,0:T(8,128)(2,1)S(1)}, u32[]{:S(2)}, u32[]{:S(2)}) %collective-permute-start.22) | collective-permute-done | bytes 65568 | tf_op jit(solution)/shard_map/ppermute | solution.py:24
  76.1 1.8 %shard_map.126 = f32[128,2048]{1,0:T(8,128)} custom-call(s32[1]{0:T(128)} %bitcast.2.kv_ref.idx_ref, bf16[128,2048]{1,0:T(8,128)(2,1)S(1)} %copy-done.5, f32[1,2048]{1,0:T(1,128)S(1)} %bitcast.6, bf16[2048,256]{1,0:T(8,128)(2,1)S(1)} %copy-done.1, bf16[2048,256]{1,0:T(8,128)(2,1)S(1)} %copy-done.2, bf16[128,256]{1,0:T(8,128)(2,1)S(1)} %get-tuple-element.63.refs_0_, ...), custom_call_target="tpu_custom_call" | custom-call | flops 268435456 | bytes 2097152 | tf_op jit(solution)/shard_map/pallas_call | solution.py:309
  77.9 0.5 collective-permute-start.16
  78.5 0.7 convert_add_fusion
  79.3 3.6 %collective-permute-done.16.refs_1_ = bf16[128,512]{1,0:T(8,128)(2,1)S(1)} collective-permute-done((bf16[128,512]{1,0:T(8,128)(2,1)S(1)}, bf16[128,512]{1,0:T(8,128)(2,1)S(1)}, u32[]{:S(2)}, u32[]{:S(2)}) %collective-permute-start.16) | collective-permute-done | bytes 131104 | tf_op jit(solution)/shard_map/ppermute | solution.py:24
  82.9 2.6 %shard_map.121 = bf16[128,2048]{1,0:T(8,128)(2,1)} custom-call(s32[1]{0:T(128)} %bitcast.idx_ref, bf16[128,2048]{1,0:T(8,128)(2,1)S(1)} %copy-done.6, f32[1,2048]{1,0:T(1,128)S(1)} %bitcast.8, bf16[128,512]{1,0:T(8,128)(2,1)S(1)} %get-tuple-element.54.refs_0_, bf16[128,512]{1,0:T(8,128)(2,1)S(1)} %collective-permute-done.16.refs_1_, ...), custom_call_target="tpu_custom_call" | custom-call | flops 536870912 | bytes 2097152 | tf_op jit(solution)/shard_map/pallas_call | solution.py:309
  (50 shorter events, 0.9 us)
Async XLA Ops:
  0.6 20.8 %copy-start = (bf16[2048,512]{1,0:T(8,128)(2,1)S(1)}, bf16[2048,512]{1,0:T(8,128)(2,1)}, u32[]{:S(2)}) copy-start(bf16[2048,512]{1,0:T(8,128)(2,1)} %refs_2_.1) | copy-start | bytes 6291460
  0.6 14.6 %copy-start.3 = (bf16[128,512]{1,0:T(8,128)(2,1)S(1)}, bf16[128,512]{1,0:T(8,128)(2,1)}, u32[]{:S(2)}) copy-start(bf16[128,512]{1,0:T(8,128)(2,1)} %refs_4_.7) | copy-start | bytes 393220
  3.9 25.2 %copy-start.4 = (bf16[144,512]{1,0:T(8,128)(2,1)S(1)}, bf16[144,512]{1,0:T(8,128)(2,1)}, u32[]{:S(2)}) copy-start(bf16[144,512]{1,0:T(8,128)(2,1)} %get-tuple-element.39.refs_3_.refs_1_.refs_0_) | copy-start | bytes 442372
  4.0 13.2 %collective-permute-start.3 = (bf16[144,512]{1,0:T(8,128)(2,1)}, bf16[144,512]{1,0:T(8,128)(2,1)S(1)}, u32[]{:S(2)}, u32[]{:S(2)}) collective-permute-start(bf16[144,512]{1,0:T(8,128)(2,1)} %get-tuple-element.39.refs_3_.refs_1_.refs_0_), channel_id=1, source_target_pairs={{0,2},{2,0},{4,6},{6,4},{8,10},{10,8},{12,14},{14,12},{16,18},{18,... | collective-permute-start | bytes 442376 | tf_op jit(solution)/shard_map/ppermute | solution.py:24
  4.5 12.7 %collective-permute-start.4 = (bf16[144,512]{1,0:T(8,128)(2,1)}, bf16[144,512]{1,0:T(8,128)(2,1)S(1)}, u32[]{:S(2)}, u32[]{:S(2)}) collective-permute-start(bf16[144,512]{1,0:T(8,128)(2,1)} %get-tuple-element.39.refs_3_.refs_1_.refs_0_), channel_id=1, source_target_pairs={{0,4},{2,6},{4,0},{6,2},{8,12},{10,14},{12,8},{14,10},{16,20},{18,... | collective-permute-start | bytes 442376 | tf_op jit(solution)/shard_map/ppermute | solution.py:24
  7.1 12.8 %collective-permute-start.5 = (bf16[144,512]{1,0:T(8,128)(2,1)}, bf16[144,512]{1,0:T(8,128)(2,1)S(1)}, u32[]{:S(2)}, u32[]{:S(2)}) collective-permute-start(bf16[144,512]{1,0:T(8,128)(2,1)} %get-tuple-element.39.refs_3_.refs_1_.refs_0_), channel_id=1, source_target_pairs={{0,6},{2,4},{4,2},{6,0},{8,14},{10,12},{12,10},{14,8},{16,22},{18,... | collective-permute-start | bytes 442376 | tf_op jit(solution)/shard_map/ppermute | solution.py:24
  7.1 24.3 %collective-permute-start.10 = (bf16[128,512]{1,0:T(8,128)(2,1)}, bf16[128,512]{1,0:T(8,128)(2,1)S(1)}, u32[]{:S(2)}, u32[]{:S(2)}) collective-permute-start(bf16[128,512]{1,0:T(8,128)(2,1)} %refs_4_.7), channel_id=1, source_target_pairs={{0,2},{2,0},{4,6},{6,4},{8,10},{10,8},{12,14},{14,12},{16,18},{18,... | collective-permute-start | bytes 393224 | tf_op jit(solution)/shard_map/ppermute | solution.py:24
  10.6 4.6 %collective-permute-start = (bf16[128,256]{1,0:T(8,128)(2,1)}, bf16[128,256]{1,0:T(8,128)(2,1)S(1)}, u32[]{:S(2)}, u32[]{:S(2)}) collective-permute-start(bf16[128,256]{1,0:T(8,128)(2,1)} %get-tuple-element.38), channel_id=1, source_target_pairs={{0,1},{1,0},{2,3},{3,2},{4,5},{5,4},{6,7},{7,6},{8,9},{9,8},{10,11... | collective-permute-start | bytes 196616 | tf_op jit(solution)/shard_map/ppermute | solution.py:24
  15.2 16.2 %collective-permute-start.11 = (bf16[128,512]{1,0:T(8,128)(2,1)S(1)}, bf16[128,512]{1,0:T(8,128)(2,1)S(1)}, u32[]{:S(2)}, u32[]{:S(2)}) collective-permute-start(bf16[128,512]{1,0:T(8,128)(2,1)S(1)} %copy-done.3), channel_id=1, source_target_pairs={{0,4},{2,6},{4,0},{6,2},{8,12},{10,14},{12,8},{14,10},{16,20},{18,... | collective-permute-start | bytes 393224 | tf_op jit(solution)/shard_map/ppermute | solution.py:24
  17.1 14.3 %collective-permute-start.12 = (bf16[128,512]{1,0:T(8,128)(2,1)S(1)}, bf16[128,512]{1,0:T(8,128)(2,1)S(1)}, u32[]{:S(2)}, u32[]{:S(2)}) collective-permute-start(bf16[128,512]{1,0:T(8,128)(2,1)S(1)} %copy-done.3), channel_id=1, source_target_pairs={{0,6},{2,4},{4,2},{6,0},{8,14},{10,12},{12,10},{14,8},{16,22},{18,... | collective-permute-start | bytes 393224 | tf_op jit(solution)/shard_map/ppermute | solution.py:24
  17.2 9.8 %collective-permute-start.2 = (bf16[256,256]{1,0:T(8,128)(2,1)S(1)}, bf16[256,256]{1,0:T(8,128)(2,1)S(1)}, u32[]{:S(2)}, u32[]{:S(2)}) collective-permute-start(bf16[256,256]{1,0:T(8,128)(2,1)S(1)} %constant_dynamic-update-slice_fusion.refs_0_), channel_id=1, source_target_pairs={{0,16},{2,18},{4,20},{6,22},{8,24},{10,26},{12,28},{14,30},{16,0},... | collective-permute-start | bytes 393224 | tf_op jit(solution)/shard_map/ppermute | solution.py:24
  19.9 8.6 %collective-permute-start.1 = (bf16[256,256]{1,0:T(8,128)(2,1)S(1)}, bf16[256,256]{1,0:T(8,128)(2,1)S(1)}, u32[]{:S(2)}, u32[]{:S(2)}) collective-permute-start(bf16[256,256]{1,0:T(8,128)(2,1)S(1)} %constant_dynamic-update-slice_fusion.refs_0_), channel_id=1, source_target_pairs={{0,8},{2,10},{4,12},{6,14},{8,0},{10,2},{12,4},{14,6},{16,24},{18,... | collective-permute-start | bytes 393224 | tf_op jit(solution)/shard_map/ppermute | solution.py:24
  27.0 26.7 %collective-permute-start.17 = (bf16[1024,512]{1,0:T(8,128)(2,1)S(1)}, bf16[1024,512]{1,0:T(8,128)(2,1)S(1)}, u32[]{:S(2)}, u32[]{:S(2)}) collective-permute-start(bf16[1024,512]{1,0:T(8,128)(2,1)S(1)} %constant_dynamic-slice_fusion), channel_id=1, source_target_pairs={{0,1},{1,0},{2,3},{3,2},{4,5},{5,4},{6,7},{7,6},{8,9},{9,8},{10,11... | collective-permute-start | bytes 3145736 | tf_op jit(solution)/shard_map/ppermute | solution.py:24
  28.5 5.0 %collective-permute-start.6 = (bf16[256,256]{1,0:T(8,128)(2,1)S(1)}, bf16[256,256]{1,0:T(8,128)(2,1)S(1)}, u32[]{:S(2)}, u32[]{:S(2)}) collective-permute-start(bf16[256,256]{1,0:T(8,128)(2,1)S(1)} %collective-permute-done.2.refs_2_), channel_id=1, source_target_pairs={{0,8},{2,10},{4,12},{6,14},{8,0},{10,2},{12,4},{14,6},{16,24},{18,... | collective-permute-start | bytes 393224 | tf_op jit(solution)/shard_map/ppermute | solution.py:24
  33.2 6.2 %copy-start.10 = (bf16[1024,128]{1,0:T(8,128)(2,1)S(1)}, bf16[1024,128]{1,0:T(8,128)(2,1)}, u32[]{:S(2)}) copy-start(bf16[1024,128]{1,0:T(8,128)(2,1)} %get-tuple-element.53) | copy-start | bytes 786436
  33.2 20.1 %copy-start.7 = (bf16[1024,128]{1,0:T(8,128)(2,1)S(1)}, bf16[1024,128]{1,0:T(8,128)(2,1)}, u32[]{:S(2)}) copy-start(bf16[1024,128]{1,0:T(8,128)(2,1)} %get-tuple-element.52.near_ref) | copy-start | bytes 786436
  34.3 3.0 %collective-permute-start.7 = (f32[8,512]{1,0:T(8,128)S(1)}, f32[8,512]{1,0:T(8,128)S(1)}, u32[]{:S(2)}, u32[]{:S(2)}) collective-permute-start(f32[8,512]{1,0:T(8,128)S(1)} %shard_map.116), channel_id=1, source_target_pairs={{0,2},{2,0},{4,6},{6,4},{8,10},{10,8},{12,14},{14,12},{16,18},{18,... | collective-permute-start | bytes 49160 | tf_op jit(solution)/shard_map/ppermute | solution.py:24
  34.3 3.8 %collective-permute-start.8 = (f32[8,512]{1,0:T(8,128)S(1)}, f32[8,512]{1,0:T(8,128)S(1)}, u32[]{:S(2)}, u32[]{:S(2)}) collective-permute-start(f32[8,512]{1,0:T(8,128)S(1)} %shard_map.116), channel_id=1, source_target_pairs={{0,4},{2,6},{4,0},{6,2},{8,12},{10,14},{12,8},{14,10},{16,20},{18,... | collective-permute-start | bytes 49160 | tf_op jit(solution)/shard_map/ppermute | solution.py:24
  35.3 3.2 %collective-permute-start.9 = (f32[8,512]{1,0:T(8,128)S(1)}, f32[8,512]{1,0:T(8,128)S(1)}, u32[]{:S(2)}, u32[]{:S(2)}) collective-permute-start(f32[8,512]{1,0:T(8,128)S(1)} %shard_map.116), channel_id=1, source_target_pairs={{0,6},{2,4},{4,2},{6,0},{8,14},{10,12},{12,10},{14,8},{16,22},{18,... | collective-permute-start | bytes 49160 | tf_op jit(solution)/shard_map/ppermute | solution.py:24
  38.8 1.7 %collective-permute-start.13 = (bf16[256,512]{1,0:T(8,128)(2,1)S(1)}, bf16[256,512]{1,0:T(8,128)(2,1)S(1)}, u32[]{:S(2)}, u32[]{:S(2)}) collective-permute-start(bf16[256,512]{1,0:T(8,128)(2,1)S(1)} %get-tuple-element.51), channel_id=1, source_target_pairs={{0,2},{2,0},{4,6},{6,4},{8,10},{10,8},{12,14},{14,12},{16,18},{18,... | collective-permute-start | bytes 786440 | tf_op jit(solution)/shard_map/ppermute | solution.py:24
  39.3 9.2 %collective-permute-start.15 = (bf16[1024,128]{1,0:T(8,128)(2,1)S(1)}, bf16[1024,128]{1,0:T(8,128)(2,1)S(1)}, u32[]{:S(2)}, u32[]{:S(2)}) collective-permute-start(bf16[1024,128]{1,0:T(8,128)(2,1)S(1)} %copy-done.10), channel_id=1, source_target_pairs={{0,4},{2,6},{4,0},{6,2},{8,12},{10,14},{12,8},{14,10},{16,20},{18,... | collective-permute-start | bytes 786440 | tf_op jit(solution)/shard_map/ppermute | solution.py:24
  40.6 12.7 %collective-permute-start.14 = (bf16[256,512]{1,0:T(8,128)(2,1)S(1)}, bf16[256,512]{1,0:T(8,128)(2,1)S(1)}, u32[]{:S(2)}, u32[]{:S(2)}) collective-permute-start(bf16[256,512]{1,0:T(8,128)(2,1)S(1)} %add_convert_fusion.pair_ref), channel_id=1, source_target_pairs={{0,4},{2,6},{4,0},{6,2},{8,12},{10,14},{12,8},{14,10},{16,20},{18,... | collective-permute-start | bytes 786440 | tf_op jit(solution)/shard_map/ppermute | solution.py:24
  53.6 3.9 %collective-permute-start.23 = (bf16[512,512]{1,0:T(8,128)(2,1)S(1)}, bf16[512,512]{1,0:T(8,128)(2,1)S(1)}, u32[]{:S(2)}, u32[]{:S(2)}) collective-permute-start(bf16[512,512]{1,0:T(8,128)(2,1)S(1)} %get-tuple-element.66), channel_id=1, source_target_pairs={{0,2},{2,0},{4,6},{6,4},{8,10},{10,8},{12,14},{14,12},{16,18},{18,... | collective-permute-start | bytes 1572872 | tf_op jit(solution)/shard_map/ppermute | solution.py:24
  53.7 29.2 %collective-permute-start.18 = (bf16[1024,512]{1,0:T(8,128)(2,1)S(1)}, bf16[1024,512]{1,0:T(8,128)(2,1)S(1)}, u32[]{:S(2)}, u32[]{:S(2)}) collective-permute-start(bf16[1024,512]{1,0:T(8,128)(2,1)S(1)} %collective-permute-done.17.refs_3_), channel_id=1, source_target_pairs={{0,2},{2,0},{4,6},{6,4},{8,10},{10,8},{12,14},{14,12},{16,18},{18,... | collective-permute-start | bytes 3145736 | tf_op jit(solution)/shard_map/ppermute | solution.py:24
  55.4 6.4 %collective-permute-start.20 = (bf16[256,256]{1,0:T(8,128)(2,1)S(1)}, bf16[256,256]{1,0:T(8,128)(2,1)S(1)}, u32[]{:S(2)}, u32[]{:S(2)}) collective-permute-start(bf16[256,256]{1,0:T(8,128)(2,1)S(1)} %get-tuple-element.62), channel_id=1, source_target_pairs={{0,8},{2,10},{4,12},{6,14},{8,0},{10,2},{12,4},{14,6},{16,24},{18,... | collective-permute-start | bytes 393224 | tf_op jit(solution)/shard_map/ppermute | solution.py:24
  56.5 15.2 %collective-permute-start.19 = (bf16[256,256]{1,0:T(8,128)(2,1)S(1)}, bf16[256,256]{1,0:T(8,128)(2,1)S(1)}, u32[]{:S(2)}, u32[]{:S(2)}) collective-permute-start(bf16[256,256]{1,0:T(8,128)(2,1)S(1)} %get-tuple-element.60), channel_id=1, source_target_pairs={{0,8},{2,10},{4,12},{6,14},{8,0},{10,2},{12,4},{14,6},{16,24},{18,... | collective-permute-start | bytes 393224 | tf_op jit(solution)/shard_map/ppermute | solution.py:24
  57.8 18.2 %copy-start.1 = (bf16[2048,256]{1,0:T(8,128)(2,1)S(1)}, bf16[2048,256]{1,0:T(8,128)(2,1)}, u32[]{:S(2)}) copy-start(bf16[2048,256]{1,0:T(8,128)(2,1)} %wk_ref.1) | copy-start | bytes 3145732
  57.9 18.2 %copy-start.2 = (bf16[2048,256]{1,0:T(8,128)(2,1)S(1)}, bf16[2048,256]{1,0:T(8,128)(2,1)}, u32[]{:S(2)}) copy-start(bf16[2048,256]{1,0:T(8,128)(2,1)} %wv_ref.1) | copy-start | bytes 3145732
  57.9 18.2 %copy-start.5 = (bf16[128,2048]{1,0:T(8,128)(2,1)S(1)}, bf16[128,2048]{1,0:T(8,128)(2,1)}, u32[]{:S(2)}) copy-start(bf16[128,2048]{1,0:T(8,128)(2,1)} %x_ref.3) | copy-start | bytes 1572868
  57.9 18.2 %copy-start.8 = (f32[2048]{0:T(1024)S(1)}, f32[2048]{0:T(1024)}, u32[]{:S(2)}) copy-start(f32[2048]{0:T(1024)} %param.12) | copy-start | bytes 24580
  57.9 12.4 %collective-permute-start.25 = (bf16[128,512]{1,0:T(8,128)(2,1)S(1)}, bf16[128,512]{1,0:T(8,128)(2,1)S(1)}, u32[]{:S(2)}, u32[]{:S(2)}) collective-permute-start(bf16[128,512]{1,0:T(8,128)(2,1)S(1)} %get-tuple-element.70), channel_id=1, source_target_pairs={{0,8},{2,10},{4,12},{6,14},{8,0},{10,2},{12,4},{14,6},{16,24},{18,... | collective-permute-start | bytes 393224 | tf_op jit(solution)/shard_map/ppermute | solution.py:24
  60.4 22.5 %copy-start.6 = (bf16[128,2048]{1,0:T(8,128)(2,1)S(1)}, bf16[128,2048]{1,0:T(8,128)(2,1)}, u32[]{:S(2)}) copy-start(bf16[128,2048]{1,0:T(8,128)(2,1)} %x_ref.2) | copy-start | bytes 1572868
  60.4 22.5 %copy-start.9 = (f32[2048]{0:T(1024)S(1)}, f32[2048]{0:T(1024)}, u32[]{:S(2)}) copy-start(f32[2048]{0:T(1024)} %param.11) | copy-start | bytes 24580
  61.9 9.8 %collective-permute-start.21 = (bf16[256,256]{1,0:T(8,128)(2,1)S(1)}, bf16[256,256]{1,0:T(8,128)(2,1)S(1)}, u32[]{:S(2)}, u32[]{:S(2)}) collective-permute-start(bf16[256,256]{1,0:T(8,128)(2,1)S(1)} %shard_map.124), channel_id=1, source_target_pairs={{0,16},{2,18},{4,20},{6,22},{8,24},{10,26},{12,28},{14,30},{16,0},... | collective-permute-start | bytes 393224 | tf_op jit(solution)/shard_map/ppermute | solution.py:24
  65.0 13.5 %collective-permute-start.24 = (bf16[128,512]{1,0:T(8,128)(2,1)S(1)}, bf16[128,512]{1,0:T(8,128)(2,1)S(1)}, u32[]{:S(2)}, u32[]{:S(2)}) collective-permute-start(bf16[128,512]{1,0:T(8,128)(2,1)S(1)} %get-tuple-element.68), channel_id=1, source_target_pairs={{0,8},{2,10},{4,12},{6,14},{8,0},{10,2},{12,4},{14,6},{16,24},{18,... | collective-permute-start | bytes 393224 | tf_op jit(solution)/shard_map/ppermute | solution.py:24
  70.3 8.2 %collective-permute-start.26 = (bf16[128,512]{1,0:T(8,128)(2,1)S(1)}, bf16[128,512]{1,0:T(8,128)(2,1)S(1)}, u32[]{:S(2)}, u32[]{:S(2)}) collective-permute-start(bf16[128,512]{1,0:T(8,128)(2,1)S(1)} %shard_map.128), channel_id=1, source_target_pairs={{0,16},{2,18},{4,20},{6,22},{8,24},{10,26},{12,28},{14,30},{16,0},... | collective-permute-start | bytes 393224 | tf_op jit(solution)/shard_map/ppermute | solution.py:24
  71.7 4.3 %collective-permute-start.22 = (bf16[128,256]{1,0:T(8,128)(2,1)S(1)}, bf16[128,256]{1,0:T(8,128)(2,1)S(1)}, u32[]{:S(2)}, u32[]{:S(2)}) collective-permute-start(bf16[128,256]{1,0:T(8,128)(2,1)S(1)} %get-tuple-element.64), channel_id=1, source_target_pairs={{0,1},{1,0},{2,3},{3,2},{4,5},{5,4},{6,7},{7,6},{8,9},{9,8},{10,11... | collective-permute-start | bytes 196616 | tf_op jit(solution)/shard_map/ppermute | solution.py:24
  77.9 5.0 %collective-permute-start.16 = (bf16[128,512]{1,0:T(8,128)(2,1)S(1)}, bf16[128,512]{1,0:T(8,128)(2,1)S(1)}, u32[]{:S(2)}, u32[]{:S(2)}) collective-permute-start(bf16[128,512]{1,0:T(8,128)(2,1)S(1)} %get-tuple-element.54.refs_0_), channel_id=1, source_target_pairs={{0,1},{1,0},{2,3},{3,2},{4,5},{5,4},{6,7},{7,6},{8,9},{9,8},{10,11... | collective-permute-start | bytes 393224 | tf_op jit(solution)/shard_map/ppermute | solution.py:24

commit v3 on v2

--- a/solution.py
+++ b/solution.py
@@ -12,7 +12,7 @@
 HD = 128
 EPS = 1e-06
 LOG2E = 1.4426950408889634
-FRONT_MIB = 60
+FRONT_MIB = 16
 
 
 F32 = jnp.float32
@@ -126,15 +126,24 @@
     q_ref[:rows, :] = q_acc.astype(BF16)
 
 
+def cat_kernel(*refs):
+    *parts, k_out, v_out = refs
+    size = parts[0].shape[0]
+    for i, r in enumerate(parts):
+        k_out[i * size : (i + 1) * size, :] = r[:, :HD]
+        v_out[i * size : (i + 1) * size, :] = r[:, HD:]
+
+
+def stack(parts, out):
+    size = parts[0].shape[0]
+    for i, r in enumerate(parts):
+        out[i * size : (i + 1) * size, :] = r[...]
+
+
 def scores_kernel(nk, nb, rows, scaling, *refs):
-    kvs, qs = refs[:nk], refs[nk : nk + nb]
-    p_ref, st_ref, k_ref, v_ref, kt_ref = refs[nk + nb :]
-    at = 0
-    for kv in kvs:
-        size = kv.shape[0]
-        k_ref[at : at + size, :] = kv[:, :HD]
-        v_ref[at : at + size, :] = kv[:, HD:]
-        at += size
+    qs = refs[nk : nk + nb]
+    p_ref, st_ref, kt_ref, k_ref = refs[nk + nb :]
+    stack(refs[:nk], k_ref)
     kt_ref[...] = k_ref[...].T
     for h in range(p_ref.shape[0]):
         lanes = slice(h * HD, (h + 1) * HD)
@@ -151,9 +160,11 @@
             st_ref[h, 1:2, cols] = jnp.sum(p, axis=0, keepdims=True)
 
 
-def grads_kernel(nb, rows, v_ref, kt_ref, p_ref, *refs):
-    qs, gs = refs[:nb], refs[nb : 2 * nb]
-    ds_ref, dq_ref = refs[2 * nb :]
+def grads_kernel(nk, nb, rows, *refs):
+    kt_ref, p_ref = refs[nk : nk + 2]
+    qs, gs = refs[nk + 2 : nk + 2 + nb], refs[nk + 2 + nb : nk + 2 + 2 * nb]
+    ds_ref, dq_ref, v_ref = refs[nk + 2 + 2 * nb :]
+    stack(refs[:nk], v_ref)
     items = [(h, pair) for h in range(p_ref.shape[0]) for pair in range(nb // 2)]
 
     def d_weights(h, pair):
@@ -322,6 +333,10 @@
     return got if isinstance(out_shape, list) else got[0]
 
 
+def in_hbm(*arrays):
+    return tuple(pltpu.with_memory_space_constraint(x, pltpu.HBM) for x in arrays)
+
+
 def local(target, source, target_gain, source_gain, w_query, w_key, w_value, attended, d_attended):
     sp, tp = lax.axis_size("sp"), lax.axis_size("tp")
     me, mt = lax.axis_index("sp"), lax.axis_index("tp")
@@ -336,7 +351,7 @@
     scaling = HD ** (-0.5)
     kv_index = mt // group
     dblk = dim // sp
-    steps = 4
+    steps = 2
     kvw = KVH * HD
     shape = jax.ShapeDtypeStruct
     t_gain, s_gain = target_gain.reshape(1, dim), source_gain.reshape(1, dim)
@@ -346,7 +361,7 @@
     by_head = call(
         functools.partial(source_kernel, steps),
         [shape((srows, 2 * HD), BF16)] * KVH,
-        (source, s_gain, w_key, w_value),
+        in_hbm(source, s_gain, w_key, w_value),
         flops=4 * srows * dim * kvw,
         mb=FRONT_MIB,
         index=(kv_index,),
@@ -366,7 +381,7 @@
     q_ext, near, far = call(
         functools.partial(target_kernel, steps, sp, half),
         [shape((rows + 16, width), BF16)] + [shape((near_rows, rows), BF16)] * 2,
-        (target, t_gain, w_query, attended, d_attended),
+        in_hbm(target, t_gain, w_query, attended, d_attended),
         flops=2 * rows * dim * width,
         mb=FRONT_MIB,
         index=(me,),
@@ -394,20 +409,25 @@
         return [blocks[0], odd[0]] + [away(x, 2 * i + 2) for i, x in enumerate(pairs)]
 
     rest = [swap(by_head[d // group], "tp", d) for d in range(1, tp)]
-    kv_own = jnp.concatenate([by_head[0]] + rest, axis=0)
+    tables = call(cat_kernel, [shape((tp * srows, HD), BF16)] * 2, (by_head[0], *rest), mib=1)
     late = list(range(nz // 2 + 1, nz, 2))
     chunks = [[k for k in range(nz) if k not in late], late]
     chunk_of = {k: c for c, ks in enumerate(chunks) for k in ks}
-    at_hand = {0: kv_own}
-    for k in list(range(2, nz, 2)) + list(range(1, nz, 2)):
-        at_hand[k] = away(at_hand[k - 1] if k % 2 else kv_own, k, 1 if k % 2 else k)
-    kvs = [[at_hand[k] for k in ks] for ks in chunks]
-
-    qs = [q_ext] + [swap(q_ext, "sp", k) for k in range(1, nb)]
-    gs = [d_attended] + [swap(d_attended, "sp", k) for k in range(1, nb)]
+    key_parts, value_parts = [], []
+    for own, places in ((tables[0], key_parts), (tables[1], value_parts)):
+        at_hand = {0: own}
+        for k in list(range(2, nz, 2)) + list(range(1, nz, 2)):
+            at_hand[k] = away(at_hand[k - 1], k, 1) if k % 2 else away(own, k)
+        places.extend([[at_hand[k] for k in ks] for ks in chunks])
+
+    def around(x):
+        far, near = swap(x, "sp", half), swap(x, "sp", 1)
+        return [x, near, far, swap(far, "sp", 1)]
+
+    qs, gs = around(q_ext), around(d_attended)
     far = swap(far, "sp", half)
 
-    held, _ = lax.optimization_barrier((w_query, kv_own))
+    held, _ = lax.optimization_barrier((w_query, tables[0]))
     piece = lax.dynamic_slice_in_dim(held, (me & 1) * (dim // 2), dim // 2, 0)
     wq_mine = [swap(piece, "tp", d) for d in range(1, tp)]
     wq_theirs = [swap(w, "sp", 1) for w in wq_mine]
@@ -417,30 +437,28 @@
     dqshape = shape((heads, HD, trows), F32)
 
     def scores(c):
-        part = sum(kv.shape[0] for kv in kvs[c])
+        parts = key_parts[c]
+        part = sum(x.shape[0] for x in parts)
         return call(
-            functools.partial(scores_kernel, len(kvs[c]), nb, rows, scaling),
-            [
-                shape((heads, part, trows), BF16),
-                stshape,
-                shape((part, HD), BF16),
-                shape((part, HD), BF16),
-                shape((HD, part), BF16),
-            ],
-            (*kvs[c], *qs),
+            functools.partial(scores_kernel, len(parts), nb, rows, scaling),
+            [shape((heads, part, trows), BF16), stshape, shape((HD, part), BF16)],
+            (*parts, *qs),
             flops=4 * heads * part * trows * HD,
+            scratch=[pltpu.VMEM((part, HD), BF16)],
         )
 
-    def grads(probs, values, keys_t):
+    def grads(c, probs, keys_t):
+        parts = value_parts[c]
         return call(
-            functools.partial(grads_kernel, nb, rows),
+            functools.partial(grads_kernel, len(parts), nb, rows),
             [shape(probs.shape, BF16), dqshape],
-            (values, keys_t, probs, *qs, *gs),
+            (*parts, keys_t, probs, *qs, *gs),
             flops=6 * probs.size * HD,
+            scratch=[pltpu.VMEM((probs.shape[1], HD), BF16)],
         )
 
     nc = len(chunks)
-    probs, own_stats, _, values, keys_t = zip(*[scores(c) for c in range(nc)])
+    probs, own_stats, keys_t = zip(*[scores(c) for c in range(nc)])
     stats = call(
         functools.partial(lse_kernel, heads),
         shape((8 * -(-heads // 4), trows), F32),
@@ -448,7 +466,7 @@
         mib=1,
     )
     sts = [swap(stats, "sp", k) for k in range(1, nb)]
-    d_scores, dq_parts = zip(*[grads(probs[c], values[c], keys_t[c]) for c in range(nc)])
+    d_scores, dq_parts = zip(*[grads(c, probs[c], keys_t[c]) for c in range(nc)])
     coef, sent, kept = call(
         functools.partial(scale_kernel, nc, nb, rows, heads, scaling),
         [stshape, shape((2 * rows, width), BF16), shape((2 * rows, width), F32)],

time: 85.7 us -> 81.7 us (0.953)
  waiting for transfers between devices: 33.3 us -> 29.6 us
  Pallas kernels: 20.7 us -> 19.6 us
  starting transfers between devices: 28.8 us -> 29.8 us
    ppermute x27 -> x30, waiting for transfers between devices: 33.3 us -> 29.6 us  [swap(): return lax.ppermute(x, axis, [(i, i ^ k) for i in range(n)])]
    pallas_call x17 -> x18, Pallas kernels: 20.7 us -> 19.6 us  [call(): pl.pallas_call(body, grid_spec=pltpu.PrefetchScalarGridSpec(num_scalar_pr...]
    ppermute x27 -> x30, starting transfers between devices: 28.8 us -> 29.8 us  [swap(): return lax.ppermute(x, axis, [(i, i ^ k) for i in range(n)])]
  transfers between devices with their start and end apart: 27 -> 30, of which waited for: 12 -> 12; matrix products, arithmetic and copies ran while one was open for 2% -> 1% of each run, Pallas kernels for 17% -> 18%
where the time goes in v3:
time: 81.7 us; the launch traced here: 81.5 us
  starting transfers between devices  29.8 us (36%)
  waiting for transfers between devices  29.6 us (36%)
  Pallas kernels  19.6 us (24%)
  between operations  0.93 us (1%)
  local copies, waits for them, and re-layouts  0.82 us (1%)
    ppermute x30, starting transfers between devices, swap(): return lax.ppermute(x, axis, [(i, i ^ k) for i in range(n)])  29.8 us
    ppermute x30, waiting for transfers between devices, swap(): return lax.ppermute(x, axis, [(i, i ^ k) for i in range(n)])  29.6 us
    pallas_call x18, Pallas kernels, call(): pl.pallas_call(body, grid_spec=pltpu.PrefetchScalarGridSpec(num_scalar_pr...  19.6 us
  transfers between devices with their start and end apart: 30, of which 12 were waited for; matrix products, arithmetic and copies ran while one was open for 1% of the time, Pallas kernels for 18%

profile of v3, /device:TPU:0, one launch (start us, length us, event | category | flops | bytes accessed | tf_op | source)
XLA Modules:
  0.0 81.5 jit_solution(2118487790077184533)
XLA Ops:
  0.7 2.4 %shard_map.112 = (bf16[128,256]{1,0:T(8,128)(2,1)S(1)}, bf16[128,256]{1,0:T(8,128)(2,1)S(1)}) custom-call(s32[1]{0:T(128)} %bitcast.2.kv_ref.idx_ref, bf16[128,2048]{1,0:T(8,128)(2,1)} %x_ref.3, f32[1,2048]{1,0:T(1,128)} %bitcast.5, bf16[2048,256]{1,0:T(8,128)(2,1)} %wk_ref.1, bf16[2048,256]{1,0:T(8,128)(2,1)} %wv_ref.1), custom_call_target="tpu_custom_call" | custom-call | flops 268435456 | bytes 2097152 | tf_op jit(solution)/shard_map/pallas_call | solution.py:320
  3.1 3.0 %collective-permute-start = (bf16[128,256]{1,0:T(8,128)(2,1)S(1)}, bf16[128,256]{1,0:T(8,128)(2,1)S(1)}, u32[]{:S(2)}, u32[]{:S(2)}) collective-permute-start(bf16[128,256]{1,0:T(8,128)(2,1)S(1)} %get-tuple-element.38), channel_id=1, source_target_pairs={{0,1},{1,0},{2,3},{3,2},{4,5},{5,4},{6,7},{7,6},{8,9},{9,8},{10,11... | collective-permute-start | bytes 196616 | tf_op jit(solution)/shard_map/ppermute | solution.py:24
  6.1 2.3 %shard_map.114 = (bf16[144,512]{1,0:T(8,128)(2,1)S(1)}, bf16[1024,128]{1,0:T(8,128)(2,1)S(1)}, bf16[1024,128]{1,0:T(8,128)(2,1)S(1)}) custom-call(s32[1]{0:T(128)} %bitcast.4.me_ref, bf16[128,2048]{1,0:T(8,128)(2,1)} %x_ref.2, f32[1,2048]{1,0:T(1,128)} %bitcast.7, bf16[2048,512]{1,0:T(8,128)(2,1)} %refs_2_.1, bf16[128,512]{1,0:T(8,128)(2,1)} %at_any.1, ...), custom_call_target="tpu_custom_call" | custom-call | flops 268435456 | bytes 2097152 | tf_op jit(solution)/shard_map/pallas_call | solution.py:320
  8.4 0.7 copy-done.8
  9.1 1.5 %collective-permute-start.4 = (bf16[144,512]{1,0:T(8,128)(2,1)S(1)}, bf16[144,512]{1,0:T(8,128)(2,1)S(1)}, u32[]{:S(2)}, u32[]{:S(2)}) collective-permute-start(bf16[144,512]{1,0:T(8,128)(2,1)S(1)} %get-tuple-element.40.refs_3_.refs_1_.refs_5_.refs_0_), channel_id=1, source_target_pairs={{0,4},{2,6},{4,0},{6,2},{8,12},{10,14},{12,8},{14,10},{16,20},{18,... | collective-permute-start | bytes 442376 | tf_op jit(solution)/shard_map/ppermute | solution.py:24
  10.6 0.5 collective-permute-start.13
  11.2 2.7 %collective-permute-start.2 = (bf16[256,128]{1,0:T(8,128)(2,1)S(1)}, bf16[256,128]{1,0:T(8,128)(2,1)S(1)}, u32[]{:S(2)}, u32[]{:S(2)}) collective-permute-start(bf16[256,128]{1,0:T(8,128)(2,1)S(1)} %get-tuple-element.39.refs_0_), channel_id=1, source_target_pairs={{0,16},{2,18},{4,20},{6,22},{8,24},{10,26},{12,28},{14,30},{16,0},... | collective-permute-start | bytes 196616 | tf_op jit(solution)/shard_map/ppermute | solution.py:24
  13.8 4.0 %collective-permute-done.2.refs_2_ = bf16[256,128]{1,0:T(8,128)(2,1)S(1)} collective-permute-done((bf16[256,128]{1,0:T(8,128)(2,1)S(1)}, bf16[256,128]{1,0:T(8,128)(2,1)S(1)}, u32[]{:S(2)}, u32[]{:S(2)}) %collective-permute-start.2) | collective-permute-done | bytes 65568 | tf_op jit(solution)/shard_map/ppermute | solution.py:24
  17.8 0.6 collective-permute-start.6
  18.4 0.5 collective-permute-start.12
  18.9 1.4 %collective-permute-start.1 = (bf16[256,128]{1,0:T(8,128)(2,1)S(1)}, bf16[256,128]{1,0:T(8,128)(2,1)S(1)}, u32[]{:S(2)}, u32[]{:S(2)}) collective-permute-start(bf16[256,128]{1,0:T(8,128)(2,1)S(1)} %get-tuple-element.39.refs_0_), channel_id=1, source_target_pairs={{0,8},{2,10},{4,12},{6,14},{8,0},{10,2},{12,4},{14,6},{16,24},{18,... | collective-permute-start | bytes 196616 | tf_op jit(solution)/shard_map/ppermute | solution.py:24
  20.3 2.1 %collective-permute-start.11 = (bf16[256,128]{1,0:T(8,128)(2,1)S(1)}, bf16[256,128]{1,0:T(8,128)(2,1)S(1)}, u32[]{:S(2)}, u32[]{:S(2)}) collective-permute-start(bf16[256,128]{1,0:T(8,128)(2,1)S(1)} %get-tuple-element.43.refs_0_), channel_id=1, source_target_pairs={{0,16},{2,18},{4,20},{6,22},{8,24},{10,26},{12,28},{14,30},{16,0},... | collective-permute-start | bytes 196616 | tf_op jit(solution)/shard_map/ppermute | solution.py:24
  22.4 0.3 collective-permute-done.6.refs_0_
  22.8 1.8 %collective-permute-start.10 = (bf16[256,128]{1,0:T(8,128)(2,1)S(1)}, bf16[256,128]{1,0:T(8,128)(2,1)S(1)}, u32[]{:S(2)}, u32[]{:S(2)}) collective-permute-start(bf16[256,128]{1,0:T(8,128)(2,1)S(1)} %get-tuple-element.43.refs_0_), channel_id=1, source_target_pairs={{0,8},{2,10},{4,12},{6,14},{8,0},{10,2},{12,4},{14,6},{16,24},{18,... | collective-permute-start | bytes 196616 | tf_op jit(solution)/shard_map/ppermute | solution.py:24
  24.5 1.6 %shard_map.116 = (bf16[4,256,512]{2,1,0:T(8,128)(2,1)S(1)}, f32[4,8,512]{2,1,0:T(8,128)S(1)}, bf16[128,256]{1,0:T(8,128)(2,1)S(1)}) custom-call(bf16[256,128]{1,0:T(8,128)(2,1)} %collective-permute-done.6.refs_0_, bf16[144,512]{1,0:T(8,128)(2,1)S(1)} %get-tuple-element.40.refs_3_.refs_1_.refs_5_.refs_0_, ...), custom_call_target="tpu_custom_call" | custom-call | flops 268435456 | bytes 2097152 | tf_op jit(solution)/shard_map/pallas_call | solution.py:320
  26.3 0.4 collective-permute-start.20
  26.7 1.5 %collective-permute-start.15 = (bf16[256,128]{1,0:T(8,128)(2,1)S(1)}, bf16[256,128]{1,0:T(8,128)(2,1)S(1)}, u32[]{:S(2)}, u32[]{:S(2)}) collective-permute-start(bf16[256,128]{1,0:T(8,128)(2,1)S(1)} %collective-permute-done.11.refs_2_), channel_id=1, source_target_pairs={{0,8},{2,10},{4,12},{6,14},{8,0},{10,2},{12,4},{14,6},{16,24},{18,... | collective-permute-start | bytes 196616 | tf_op jit(solution)/shard_map/ppermute | solution.py:24
  28.3 2.3 %shard_map.115 = (bf16[4,768,512]{2,1,0:T(8,128)(2,1)S(1)}, f32[4,8,512]{2,1,0:T(8,128)S(1)}, bf16[128,768]{1,0:T(8,128)(2,1)S(1)}) custom-call(bf16[256,128]{1,0:T(8,128)(2,1)S(1)} %get-tuple-element.39.refs_0_, bf16[256,128]{1,0:T(8,128)(2,1)S(1)} %collective-permute-done.1.refs_1_, bf16[256,128]{1,0:T(8,128)(2,1)S(1)} %collective-permute-done.2.refs_2_, ...), custom_call_target="tpu_custom_call" | custom-call | flops 805306368 | bytes 2097152 | tf_op jit(solution)/shard_map/pallas_call | solution.py:320
  30.7 1.6 %collective-permute-start.8 = (f32[8,512]{1,0:T(8,128)S(1)}, f32[8,512]{1,0:T(8,128)S(1)}, u32[]{:S(2)}, u32[]{:S(2)}) collective-permute-start(f32[8,512]{1,0:T(8,128)S(1)} %shard_map.117), channel_id=1, source_target_pairs={{0,4},{2,6},{4,0},{6,2},{8,12},{10,14},{12,8},{14,10},{16,20},{18,... | collective-permute-start | bytes 49160 | tf_op jit(solution)/shard_map/ppermute | solution.py:24
  32.3 0.2 collective-permute-start.9
  32.6 1.7 %shard_map.118 = (bf16[4,768,512]{2,1,0:T(8,128)(2,1)S(1)}, f32[4,128,512]{2,1,0:T(8,128)S(1)}) custom-call(bf16[256,128]{1,0:T(8,128)(2,1)S(1)} %get-tuple-element.43.refs_0_, bf16[256,128]{1,0:T(8,128)(2,1)S(1)} %collective-permute-done.10.refs_1_, bf16[256,128]{1,0:T(8,128)(2,1)S(1)} %collective-permute-done.11.refs_2_, ...), custom_call_target="tpu_custom_call" | custom-call | flops 1207959552 | bytes 2097152 | tf_op jit(solution)/shard_map/pallas_call | solution.py:320
  34.3 1.1 %shard_map.119 = (bf16[4,256,512]{2,1,0:T(8,128)(2,1)S(1)}, f32[4,128,512]{2,1,0:T(8,128)S(1)}) custom-call(bf16[256,128]{1,0:T(8,128)(2,1)S(1)} %collective-permute-done.15.refs_0_, bf16[128,256]{1,0:T(8,128)(2,1)S(1)} %get-tuple-element.47.refs_1_, bf16[4,256,512]{2,1,0:T(8,128)(2,1)S(1)} %get-tuple-element.48.refs_2_.refs_10_, ...), custom_call_target="tpu_custom_call" | custom-call | flops 402653184 | bytes 2097152 | tf_op jit(solution)/shard_map/pallas_call | solution.py:320
  35.5 0.3 shard_map.120
  35.8 0.5 collective-permute-start.16
  36.3 1.4 %collective-permute-start.18 = (bf16[1024,128]{1,0:T(8,128)(2,1)S(1)}, bf16[1024,128]{1,0:T(8,128)(2,1)S(1)}, u32[]{:S(2)}, u32[]{:S(2)}) collective-permute-start(bf16[1024,128]{1,0:T(8,128)(2,1)S(1)} %copy-done.9), channel_id=1, source_target_pairs={{0,4},{2,6},{4,0},{6,2},{8,12},{10,14},{12,8},{14,10},{16,20},{18,... | collective-permute-start | bytes 786440 | tf_op jit(solution)/shard_map/ppermute | solution.py:24
  37.8 1.2 %collective-permute-start.17 = (bf16[256,512]{1,0:T(8,128)(2,1)S(1)}, bf16[256,512]{1,0:T(8,128)(2,1)S(1)}, u32[]{:S(2)}, u32[]{:S(2)}) collective-permute-start(bf16[256,512]{1,0:T(8,128)(2,1)S(1)} %add_convert_fusion.pair_ref), channel_id=1, source_target_pairs={{0,4},{2,6},{4,0},{6,2},{8,12},{10,14},{12,8},{14,10},{16,20},{18,... | collective-permute-start | bytes 786440 | tf_op jit(solution)/shard_map/ppermute | solution.py:24
  39.0 6.5 %collective-permute-done.18.far_ref = bf16[1024,128]{1,0:T(8,128)(2,1)S(1)} collective-permute-done((bf16[1024,128]{1,0:T(8,128)(2,1)S(1)}, bf16[1024,128]{1,0:T(8,128)(2,1)S(1)}, u32[]{:S(2)}, u32[]{:S(2)}) %collective-permute-start.18) | collective-permute-done | bytes 262176 | tf_op jit(solution)/shard_map/ppermute | solution.py:24
  45.5 4.7 %collective-permute-done.17.other_ref = bf16[256,512]{1,0:T(8,128)(2,1)S(1)} collective-permute-done((bf16[256,512]{1,0:T(8,128)(2,1)S(1)}, bf16[256,512]{1,0:T(8,128)(2,1)S(1)}, u32[]{:S(2)}, u32[]{:S(2)}) %collective-permute-start.17) | collective-permute-done | bytes 262176 | tf_op jit(solution)/shard_map/ppermute | solution.py:24
  50.2 0.3 shard_map.121
  50.6 0.8 %collective-permute-done.20.refs_3_ = bf16[1024,512]{1,0:T(8,128)(2,1)S(1)} collective-permute-done((bf16[1024,512]{1,0:T(8,128)(2,1)S(1)}, bf16[1024,512]{1,0:T(8,128)(2,1)S(1)}, u32[]{:S(2)}, u32[]{:S(2)}) %collective-permute-start.20) | collective-permute-done | bytes 1048608 | tf_op jit(solution)/shard_map/ppermute | solution.py:24
  51.5 1.3 %shard_map.124 = (bf16[256,256]{1,0:T(8,128)(2,1)S(1)}, bf16[256,256]{1,0:T(8,128)(2,1)S(1)}) custom-call(bf16[144,512]{1,0:T(8,128)(2,1)S(1)} %get-tuple-element.40.refs_3_.refs_1_.refs_5_.refs_0_, bf16[144,512]{1,0:T(8,128)(2,1)S(1)} %collective-permute-done.3.refs_4_.refs_2_.refs_6_.refs_1_, ...), custom_call_target="tpu_custom_call" | custom-call | flops 805306368 | bytes 2097152 | tf_op jit(solution)/shard_map/pallas_call | solution.py:320
  52.7 0.4 collective-permute-start.23
  53.2 1.7 %collective-permute-start.22 = (bf16[256,256]{1,0:T(8,128)(2,1)S(1)}, bf16[256,256]{1,0:T(8,128)(2,1)S(1)}, u32[]{:S(2)}, u32[]{:S(2)}) collective-permute-start(bf16[256,256]{1,0:T(8,128)(2,1)S(1)} %get-tuple-element.60), channel_id=1, source_target_pairs={{0,8},{2,10},{4,12},{6,14},{8,0},{10,2},{12,4},{14,6},{16,24},{18,... | collective-permute-start | bytes 393224 | tf_op jit(solution)/shard_map/ppermute | solution.py:24
  54.8 0.3 shard_map.128
  55.2 0.4 collective-permute-start.28
  55.6 1.5 %shard_map.123 = (f32[256,256]{1,0:T(8,128)S(1)}, f32[256,256]{1,0:T(8,128)S(1)}) custom-call(bf16[144,512]{1,0:T(8,128)(2,1)S(1)} %get-tuple-element.40.refs_3_.refs_1_.refs_5_.refs_0_, bf16[144,512]{1,0:T(8,128)(2,1)S(1)} %collective-permute-done.3.refs_4_.refs_2_.refs_6_.refs_1_, ...), custom_call_target="tpu_custom_call" | custom-call | flops 805306368 | bytes 2097152 | tf_op jit(solution)/shard_map/pallas_call | solution.py:320
  57.1 2.1 %collective-permute-done.23.refs_1_ = bf16[256,256]{1,0:T(8,128)(2,1)S(1)} collective-permute-done((bf16[256,256]{1,0:T(8,128)(2,1)S(1)}, bf16[256,256]{1,0:T(8,128)(2,1)S(1)}, u32[]{:S(2)}, u32[]{:S(2)}) %collective-permute-start.23) | collective-permute-done | bytes 131104 | tf_op jit(solution)/shard_map/ppermute | solution.py:24
  59.2 2.4 %collective-permute-start.24 = (bf16[256,256]{1,0:T(8,128)(2,1)S(1)}, bf16[256,256]{1,0:T(8,128)(2,1)S(1)}, u32[]{:S(2)}, u32[]{:S(2)}) collective-permute-start(bf16[256,256]{1,0:T(8,128)(2,1)S(1)} %shard_map.125), channel_id=1, source_target_pairs={{0,16},{2,18},{4,20},{6,22},{8,24},{10,26},{12,28},{14,30},{16,0},... | collective-permute-start | bytes 393224 | tf_op jit(solution)/shard_map/ppermute | solution.py:24
  61.6 1.3 %collective-permute-start.27 = (bf16[128,512]{1,0:T(8,128)(2,1)S(1)}, bf16[128,512]{1,0:T(8,128)(2,1)S(1)}, u32[]{:S(2)}, u32[]{:S(2)}) collective-permute-start(bf16[128,512]{1,0:T(8,128)(2,1)S(1)} %get-tuple-element.68), channel_id=1, source_target_pairs={{0,8},{2,10},{4,12},{6,14},{8,0},{10,2},{12,4},{14,6},{16,24},{18,... | collective-permute-start | bytes 393224 | tf_op jit(solution)/shard_map/ppermute | solution.py:24
  62.9 4.7 %collective-permute-done.28.refs_1_ = bf16[128,512]{1,0:T(8,128)(2,1)S(1)} collective-permute-done((bf16[128,512]{1,0:T(8,128)(2,1)S(1)}, bf16[128,512]{1,0:T(8,128)(2,1)S(1)}, u32[]{:S(2)}, u32[]{:S(2)}) %collective-permute-start.28) | collective-permute-done | bytes 131104 | tf_op jit(solution)/shard_map/ppermute | solution.py:24
  67.8 1.2 %collective-permute-start.25 = (bf16[128,256]{1,0:T(8,128)(2,1)S(1)}, bf16[128,256]{1,0:T(8,128)(2,1)S(1)}, u32[]{:S(2)}, u32[]{:S(2)}) collective-permute-start(bf16[128,256]{1,0:T(8,128)(2,1)S(1)} %get-tuple-element.64), channel_id=1, source_target_pairs={{0,1},{1,0},{2,3},{3,2},{4,5},{5,4},{6,7},{7,6},{8,9},{9,8},{10,11... | collective-permute-start | bytes 196616 | tf_op jit(solution)/shard_map/ppermute | solution.py:24
  69.0 3.1 %collective-permute-done.25.refs_1_ = bf16[128,256]{1,0:T(8,128)(2,1)S(1)} collective-permute-done((bf16[128,256]{1,0:T(8,128)(2,1)S(1)}, bf16[128,256]{1,0:T(8,128)(2,1)S(1)}, u32[]{:S(2)}, u32[]{:S(2)}) %collective-permute-start.25) | collective-permute-done | bytes 65568 | tf_op jit(solution)/shard_map/ppermute | solution.py:24
  72.1 1.8 %shard_map.127 = f32[128,2048]{1,0:T(8,128)} custom-call(s32[1]{0:T(128)} %bitcast.2.kv_ref.idx_ref, bf16[128,2048]{1,0:T(8,128)(2,1)S(1)} %copy-done.4, f32[1,2048]{1,0:T(1,128)S(1)} %bitcast.6, bf16[2048,256]{1,0:T(8,128)(2,1)S(1)} %copy-done.1, bf16[2048,256]{1,0:T(8,128)(2,1)S(1)} %copy-done.2, bf16[128,256]{1,0:T(8,128)(2,1)S(1)} %get-tuple-element.63.refs_0_, ...), custom_call_target="tpu_custom_call" | custom-call | flops 268435456 | bytes 2097152 | tf_op jit(solution)/shard_map/pallas_call | solution.py:320
  74.0 1.2 %collective-permute-start.19 = (bf16[128,512]{1,0:T(8,128)(2,1)S(1)}, bf16[128,512]{1,0:T(8,128)(2,1)S(1)}, u32[]{:S(2)}, u32[]{:S(2)}) collective-permute-start(bf16[128,512]{1,0:T(8,128)(2,1)S(1)} %get-tuple-element.54.refs_0_), channel_id=1, source_target_pairs={{0,1},{1,0},{2,3},{3,2},{4,5},{5,4},{6,7},{7,6},{8,9},{9,8},{10,11... | collective-permute-start | bytes 393224 | tf_op jit(solution)/shard_map/ppermute | solution.py:24
  75.1 0.8 %collective-permute-done.29 = bf16[128,512]{1,0:T(8,128)(2,1)S(1)} collective-permute-done((bf16[128,512]{1,0:T(8,128)(2,1)S(1)}, bf16[128,512]{1,0:T(8,128)(2,1)S(1)}, u32[]{:S(2)}, u32[]{:S(2)}) %collective-permute-start.29) | collective-permute-done | bytes 131104 | tf_op jit(solution)/shard_map/ppermute | solution.py:24
  76.0 0.7 convert_add_fusion
  76.7 2.2 %collective-permute-done.19.refs_1_ = bf16[128,512]{1,0:T(8,128)(2,1)S(1)} collective-permute-done((bf16[128,512]{1,0:T(8,128)(2,1)S(1)}, bf16[128,512]{1,0:T(8,128)(2,1)S(1)}, u32[]{:S(2)}, u32[]{:S(2)}) %collective-permute-start.19) | collective-permute-done | bytes 131104 | tf_op jit(solution)/shard_map/ppermute | solution.py:24
  79.0 2.6 %shard_map.122 = bf16[128,2048]{1,0:T(8,128)(2,1)} custom-call(s32[1]{0:T(128)} %bitcast.idx_ref, bf16[128,2048]{1,0:T(8,128)(2,1)S(1)} %copy-done.5, f32[1,2048]{1,0:T(1,128)S(1)} %bitcast.8, bf16[128,512]{1,0:T(8,128)(2,1)S(1)} %get-tuple-element.54.refs_0_, bf16[128,512]{1,0:T(8,128)(2,1)S(1)} %collective-permute-done.19.refs_1_, ...), custom_call_target="tpu_custom_call" | custom-call | flops 536870912 | bytes 2097152 | tf_op jit(solution)/shard_map/pallas_call | solution.py:320
  (53 shorter events, 0.9 us)
Async XLA Ops:
  0.6 22.1 %copy-start = (bf16[2048,512]{1,0:T(8,128)(2,1)S(1)}, bf16[2048,512]{1,0:T(8,128)(2,1)}, u32[]{:S(2)}) copy-start(bf16[2048,512]{1,0:T(8,128)(2,1)} %refs_2_.1) | copy-start | bytes 6291460
  0.6 10.0 %copy-start.3 = (bf16[128,512]{1,0:T(8,128)(2,1)S(1)}, bf16[128,512]{1,0:T(8,128)(2,1)}, u32[]{:S(2)}) copy-start(bf16[128,512]{1,0:T(8,128)(2,1)} %refs_4_.3) | copy-start | bytes 393220
  3.1 8.1 %collective-permute-start = (bf16[128,256]{1,0:T(8,128)(2,1)S(1)}, bf16[128,256]{1,0:T(8,128)(2,1)S(1)}, u32[]{:S(2)}, u32[]{:S(2)}) collective-permute-start(bf16[128,256]{1,0:T(8,128)(2,1)S(1)} %get-tuple-element.38), channel_id=1, source_target_pairs={{0,1},{1,0},{2,3},{3,2},{4,5},{5,4},{6,7},{7,6},{8,9},{9,8},{10,11... | collective-permute-start | bytes 196616 | tf_op jit(solution)/shard_map/ppermute | solution.py:24
  8.4 0.7 copy-start.8
  9.1 9.3 %collective-permute-start.4 = (bf16[144,512]{1,0:T(8,128)(2,1)S(1)}, bf16[144,512]{1,0:T(8,128)(2,1)S(1)}, u32[]{:S(2)}, u32[]{:S(2)}) collective-permute-start(bf16[144,512]{1,0:T(8,128)(2,1)S(1)} %get-tuple-element.40.refs_3_.refs_1_.refs_5_.refs_0_), channel_id=1, source_target_pairs={{0,4},{2,6},{4,0},{6,2},{8,12},{10,14},{12,8},{14,10},{16,20},{18,... | collective-permute-start | bytes 442376 | tf_op jit(solution)/shard_map/ppermute | solution.py:24
  10.6 9.7 %collective-permute-start.3 = (bf16[144,512]{1,0:T(8,128)(2,1)S(1)}, bf16[144,512]{1,0:T(8,128)(2,1)S(1)}, u32[]{:S(2)}, u32[]{:S(2)}) collective-permute-start(bf16[144,512]{1,0:T(8,128)(2,1)S(1)} %get-tuple-element.40.refs_3_.refs_1_.refs_5_.refs_0_), channel_id=1, source_target_pairs={{0,2},{2,0},{4,6},{6,4},{8,10},{10,8},{12,14},{14,12},{16,18},{18,... | collective-permute-start | bytes 442376 | tf_op jit(solution)/shard_map/ppermute | solution.py:24
  10.6 8.3 %collective-permute-start.13 = (bf16[128,512]{1,0:T(8,128)(2,1)S(1)}, bf16[128,512]{1,0:T(8,128)(2,1)S(1)}, u32[]{:S(2)}, u32[]{:S(2)}) collective-permute-start(bf16[128,512]{1,0:T(8,128)(2,1)S(1)} %copy-done.3), channel_id=1, source_target_pairs={{0,4},{2,6},{4,0},{6,2},{8,12},{10,14},{12,8},{14,10},{16,20},{18,... | collective-permute-start | bytes 393224 | tf_op jit(solution)/shard_map/ppermute | solution.py:24
  11.2 6.6 %collective-permute-start.2 = (bf16[256,128]{1,0:T(8,128)(2,1)S(1)}, bf16[256,128]{1,0:T(8,128)(2,1)S(1)}, u32[]{:S(2)}, u32[]{:S(2)}) collective-permute-start(bf16[256,128]{1,0:T(8,128)(2,1)S(1)} %get-tuple-element.39.refs_0_), channel_id=1, source_target_pairs={{0,16},{2,18},{4,20},{6,22},{8,24},{10,26},{12,28},{14,30},{16,0},... | collective-permute-start | bytes 196616 | tf_op jit(solution)/shard_map/ppermute | solution.py:24
  17.8 4.9 %collective-permute-start.6 = (bf16[256,128]{1,0:T(8,128)(2,1)S(1)}, bf16[256,128]{1,0:T(8,128)(2,1)}, u32[]{:S(2)}, u32[]{:S(2)}) collective-permute-start(bf16[256,128]{1,0:T(8,128)(2,1)S(1)} %collective-permute-done.2.refs_2_), channel_id=1, source_target_pairs={{0,8},{2,10},{4,12},{6,14},{8,0},{10,2},{12,4},{14,6},{16,24},{18,... | collective-permute-start | bytes 196616 | tf_op jit(solution)/shard_map/ppermute | solution.py:24
  18.4 4.3 %collective-permute-start.5 = (bf16[144,512]{1,0:T(8,128)(2,1)S(1)}, bf16[144,512]{1,0:T(8,128)(2,1)S(1)}, u32[]{:S(2)}, u32[]{:S(2)}) collective-permute-start(bf16[144,512]{1,0:T(8,128)(2,1)S(1)} %collective-permute-done.4.refs_5_.refs_3_.refs_7_.refs_2_), channel_id=1, source_target_pairs={{0,2},{2,0},{4,6},{6,4},{8,10},{10,8},{12,14},{14,12},{16,18},{18,... | collective-permute-start | bytes 442376 | tf_op jit(solution)/shard_map/ppermute | solution.py:24
  18.4 12.2 %collective-permute-start.12 = (bf16[128,512]{1,0:T(8,128)(2,1)S(1)}, bf16[128,512]{1,0:T(8,128)(2,1)S(1)}, u32[]{:S(2)}, u32[]{:S(2)}) collective-permute-start(bf16[128,512]{1,0:T(8,128)(2,1)S(1)} %copy-done.3), channel_id=1, source_target_pairs={{0,2},{2,0},{4,6},{6,4},{8,10},{10,8},{12,14},{14,12},{16,18},{18,... | collective-permute-start | bytes 393224 | tf_op jit(solution)/shard_map/ppermute | solution.py:24
  18.9 7.8 %collective-permute-start.1 = (bf16[256,128]{1,0:T(8,128)(2,1)S(1)}, bf16[256,128]{1,0:T(8,128)(2,1)S(1)}, u32[]{:S(2)}, u32[]{:S(2)}) collective-permute-start(bf16[256,128]{1,0:T(8,128)(2,1)S(1)} %get-tuple-element.39.refs_0_), channel_id=1, source_target_pairs={{0,8},{2,10},{4,12},{6,14},{8,0},{10,2},{12,4},{14,6},{16,24},{18,... | collective-permute-start | bytes 196616 | tf_op jit(solution)/shard_map/ppermute | solution.py:24
  20.3 6.0 %collective-permute-start.11 = (bf16[256,128]{1,0:T(8,128)(2,1)S(1)}, bf16[256,128]{1,0:T(8,128)(2,1)S(1)}, u32[]{:S(2)}, u32[]{:S(2)}) collective-permute-start(bf16[256,128]{1,0:T(8,128)(2,1)S(1)} %get-tuple-element.43.refs_0_), channel_id=1, source_target_pairs={{0,16},{2,18},{4,20},{6,22},{8,24},{10,26},{12,28},{14,30},{16,0},... | collective-permute-start | bytes 196616 | tf_op jit(solution)/shard_map/ppermute | solution.py:24
  22.7 9.6 %collective-permute-start.14 = (bf16[128,512]{1,0:T(8,128)(2,1)S(1)}, bf16[128,512]{1,0:T(8,128)(2,1)S(1)}, u32[]{:S(2)}, u32[]{:S(2)}) collective-permute-start(bf16[128,512]{1,0:T(8,128)(2,1)S(1)} %collective-permute-done.13.refs_11_.refs_9_.refs_6_), channel_id=1, source_target_pairs={{0,2},{2,0},{4,6},{6,4},{8,10},{10,8},{12,14},{14,12},{16,18},{18,... | collective-permute-start | bytes 393224 | tf_op jit(solution)/shard_map/ppermute | solution.py:24
  22.8 7.9 %collective-permute-start.10 = (bf16[256,128]{1,0:T(8,128)(2,1)S(1)}, bf16[256,128]{1,0:T(8,128)(2,1)S(1)}, u32[]{:S(2)}, u32[]{:S(2)}) collective-permute-start(bf16[256,128]{1,0:T(8,128)(2,1)S(1)} %get-tuple-element.43.refs_0_), channel_id=1, source_target_pairs={{0,8},{2,10},{4,12},{6,14},{8,0},{10,2},{12,4},{14,6},{16,24},{18,... | collective-permute-start | bytes 196616 | tf_op jit(solution)/shard_map/ppermute | solution.py:24
  26.3 25.2 %collective-permute-start.20 = (bf16[1024,512]{1,0:T(8,128)(2,1)S(1)}, bf16[1024,512]{1,0:T(8,128)(2,1)S(1)}, u32[]{:S(2)}, u32[]{:S(2)}) collective-permute-start(bf16[1024,512]{1,0:T(8,128)(2,1)S(1)} %constant_dynamic-slice_fusion), channel_id=1, source_target_pairs={{0,1},{1,0},{2,3},{3,2},{4,5},{5,4},{6,7},{7,6},{8,9},{9,8},{10,11... | collective-permute-start | bytes 3145736 | tf_op jit(solution)/shard_map/ppermute | solution.py:24
  26.7 7.5 %collective-permute-start.15 = (bf16[256,128]{1,0:T(8,128)(2,1)S(1)}, bf16[256,128]{1,0:T(8,128)(2,1)S(1)}, u32[]{:S(2)}, u32[]{:S(2)}) collective-permute-start(bf16[256,128]{1,0:T(8,128)(2,1)S(1)} %collective-permute-done.11.refs_2_), channel_id=1, source_target_pairs={{0,8},{2,10},{4,12},{6,14},{8,0},{10,2},{12,4},{14,6},{16,24},{18,... | collective-permute-start | bytes 196616 | tf_op jit(solution)/shard_map/ppermute | solution.py:24
  30.6 4.8 %collective-permute-start.7 = (f32[8,512]{1,0:T(8,128)S(1)}, f32[8,512]{1,0:T(8,128)S(1)}, u32[]{:S(2)}, u32[]{:S(2)}) collective-permute-start(f32[8,512]{1,0:T(8,128)S(1)} %shard_map.117), channel_id=1, source_target_pairs={{0,2},{2,0},{4,6},{6,4},{8,10},{10,8},{12,14},{14,12},{16,18},{18,... | collective-permute-start | bytes 49160 | tf_op jit(solution)/shard_map/ppermute | solution.py:24
  30.7 4.7 %collective-permute-start.8 = (f32[8,512]{1,0:T(8,128)S(1)}, f32[8,512]{1,0:T(8,128)S(1)}, u32[]{:S(2)}, u32[]{:S(2)}) collective-permute-start(f32[8,512]{1,0:T(8,128)S(1)} %shard_map.117), channel_id=1, source_target_pairs={{0,4},{2,6},{4,0},{6,2},{8,12},{10,14},{12,8},{14,10},{16,20},{18,... | collective-permute-start | bytes 49160 | tf_op jit(solution)/shard_map/ppermute | solution.py:24
  32.3 3.2 %collective-permute-start.9 = (f32[8,512]{1,0:T(8,128)S(1)}, f32[8,512]{1,0:T(8,128)S(1)}, u32[]{:S(2)}, u32[]{:S(2)}) collective-permute-start(f32[8,512]{1,0:T(8,128)S(1)} %shard_map.117), channel_id=1, source_target_pairs={{0,6},{2,4},{4,2},{6,0},{8,14},{10,12},{12,10},{14,8},{16,22},{18,... | collective-permute-start | bytes 49160 | tf_op jit(solution)/shard_map/ppermute | solution.py:24
  34.3 2.0 %copy-start.9 = (bf16[1024,128]{1,0:T(8,128)(2,1)S(1)}, bf16[1024,128]{1,0:T(8,128)(2,1)}, u32[]{:S(2)}) copy-start(bf16[1024,128]{1,0:T(8,128)(2,1)} %copy-done.8) | copy-start | bytes 786436
  35.8 1.9 %collective-permute-start.16 = (bf16[256,512]{1,0:T(8,128)(2,1)S(1)}, bf16[256,512]{1,0:T(8,128)(2,1)S(1)}, u32[]{:S(2)}, u32[]{:S(2)}) collective-permute-start(bf16[256,512]{1,0:T(8,128)(2,1)S(1)} %get-tuple-element.51), channel_id=1, source_target_pairs={{0,2},{2,0},{4,6},{6,4},{8,10},{10,8},{12,14},{14,12},{16,18},{18,... | collective-permute-start | bytes 786440 | tf_op jit(solution)/shard_map/ppermute | solution.py:24
  36.3 9.2 %collective-permute-start.18 = (bf16[1024,128]{1,0:T(8,128)(2,1)S(1)}, bf16[1024,128]{1,0:T(8,128)(2,1)S(1)}, u32[]{:S(2)}, u32[]{:S(2)}) collective-permute-start(bf16[1024,128]{1,0:T(8,128)(2,1)S(1)} %copy-done.9), channel_id=1, source_target_pairs={{0,4},{2,6},{4,0},{6,2},{8,12},{10,14},{12,8},{14,10},{16,20},{18,... | collective-permute-start | bytes 786440 | tf_op jit(solution)/shard_map/ppermute | solution.py:24
  37.8 12.4 %collective-permute-start.17 = (bf16[256,512]{1,0:T(8,128)(2,1)S(1)}, bf16[256,512]{1,0:T(8,128)(2,1)S(1)}, u32[]{:S(2)}, u32[]{:S(2)}) collective-permute-start(bf16[256,512]{1,0:T(8,128)(2,1)S(1)} %add_convert_fusion.pair_ref), channel_id=1, source_target_pairs={{0,4},{2,6},{4,0},{6,2},{8,12},{10,14},{12,8},{14,10},{16,20},{18,... | collective-permute-start | bytes 786440 | tf_op jit(solution)/shard_map/ppermute | solution.py:24
  50.6 4.3 %collective-permute-start.26 = (bf16[512,512]{1,0:T(8,128)(2,1)S(1)}, bf16[512,512]{1,0:T(8,128)(2,1)S(1)}, u32[]{:S(2)}, u32[]{:S(2)}) collective-permute-start(bf16[512,512]{1,0:T(8,128)(2,1)S(1)} %get-tuple-element.66), channel_id=1, source_target_pairs={{0,2},{2,0},{4,6},{6,4},{8,10},{10,8},{12,14},{14,12},{16,18},{18,... | collective-permute-start | bytes 1572872 | tf_op jit(solution)/shard_map/ppermute | solution.py:24
  51.5 27.5 %collective-permute-start.21 = (bf16[1024,512]{1,0:T(8,128)(2,1)S(1)}, bf16[1024,512]{1,0:T(8,128)(2,1)S(1)}, u32[]{:S(2)}, u32[]{:S(2)}) collective-permute-start(bf16[1024,512]{1,0:T(8,128)(2,1)S(1)} %collective-permute-done.20.refs_3_), channel_id=1, source_target_pairs={{0,2},{2,0},{4,6},{6,4},{8,10},{10,8},{12,14},{14,12},{16,18},{18,... | collective-permute-start | bytes 3145736 | tf_op jit(solution)/shard_map/ppermute | solution.py:24
  52.7 6.4 %collective-permute-start.23 = (bf16[256,256]{1,0:T(8,128)(2,1)S(1)}, bf16[256,256]{1,0:T(8,128)(2,1)S(1)}, u32[]{:S(2)}, u32[]{:S(2)}) collective-permute-start(bf16[256,256]{1,0:T(8,128)(2,1)S(1)} %get-tuple-element.62), channel_id=1, source_target_pairs={{0,8},{2,10},{4,12},{6,14},{8,0},{10,2},{12,4},{14,6},{16,24},{18,... | collective-permute-start | bytes 393224 | tf_op jit(solution)/shard_map/ppermute | solution.py:24
  53.2 14.5 %collective-permute-start.22 = (bf16[256,256]{1,0:T(8,128)(2,1)S(1)}, bf16[256,256]{1,0:T(8,128)(2,1)S(1)}, u32[]{:S(2)}, u32[]{:S(2)}) collective-permute-start(bf16[256,256]{1,0:T(8,128)(2,1)S(1)} %get-tuple-element.60), channel_id=1, source_target_pairs={{0,8},{2,10},{4,12},{6,14},{8,0},{10,2},{12,4},{14,6},{16,24},{18,... | collective-permute-start | bytes 393224 | tf_op jit(solution)/shard_map/ppermute | solution.py:24
  55.1 17.0 %copy-start.1 = (bf16[2048,256]{1,0:T(8,128)(2,1)S(1)}, bf16[2048,256]{1,0:T(8,128)(2,1)}, u32[]{:S(2)}) copy-start(bf16[2048,256]{1,0:T(8,128)(2,1)} %wk_ref.1) | copy-start | bytes 3145732
  55.2 17.0 %copy-start.2 = (bf16[2048,256]{1,0:T(8,128)(2,1)S(1)}, bf16[2048,256]{1,0:T(8,128)(2,1)}, u32[]{:S(2)}) copy-start(bf16[2048,256]{1,0:T(8,128)(2,1)} %wv_ref.1) | copy-start | bytes 3145732
  55.2 16.9 %copy-start.4 = (bf16[128,2048]{1,0:T(8,128)(2,1)S(1)}, bf16[128,2048]{1,0:T(8,128)(2,1)}, u32[]{:S(2)}) copy-start(bf16[128,2048]{1,0:T(8,128)(2,1)} %x_ref.3) | copy-start | bytes 1572868
  55.2 16.9 %copy-start.6 = (f32[2048]{0:T(1024)S(1)}, f32[2048]{0:T(1024)}, u32[]{:S(2)}) copy-start(f32[2048]{0:T(1024)} %param.12) | copy-start | bytes 24580
  55.2 12.4 %collective-permute-start.28 = (bf16[128,512]{1,0:T(8,128)(2,1)S(1)}, bf16[128,512]{1,0:T(8,128)(2,1)S(1)}, u32[]{:S(2)}, u32[]{:S(2)}) collective-permute-start(bf16[128,512]{1,0:T(8,128)(2,1)S(1)} %get-tuple-element.70), channel_id=1, source_target_pairs={{0,8},{2,10},{4,12},{6,14},{8,0},{10,2},{12,4},{14,6},{16,24},{18,... | collective-permute-start | bytes 393224 | tf_op jit(solution)/shard_map/ppermute | solution.py:24
  57.1 21.9 %copy-start.5 = (bf16[128,2048]{1,0:T(8,128)(2,1)S(1)}, bf16[128,2048]{1,0:T(8,128)(2,1)}, u32[]{:S(2)}) copy-start(bf16[128,2048]{1,0:T(8,128)(2,1)} %x_ref.2) | copy-start | bytes 1572868
  57.1 21.9 %copy-start.7 = (f32[2048]{0:T(1024)S(1)}, f32[2048]{0:T(1024)}, u32[]{:S(2)}) copy-start(f32[2048]{0:T(1024)} %param.11) | copy-start | bytes 24580
  59.2 8.5 %collective-permute-start.24 = (bf16[256,256]{1,0:T(8,128)(2,1)S(1)}, bf16[256,256]{1,0:T(8,128)(2,1)S(1)}, u32[]{:S(2)}, u32[]{:S(2)}) collective-permute-start(bf16[256,256]{1,0:T(8,128)(2,1)S(1)} %shard_map.125), channel_id=1, source_target_pairs={{0,16},{2,18},{4,20},{6,22},{8,24},{10,26},{12,28},{14,30},{16,0},... | collective-permute-start | bytes 393224 | tf_op jit(solution)/shard_map/ppermute | solution.py:24
  61.6 13.5 %collective-permute-start.27 = (bf16[128,512]{1,0:T(8,128)(2,1)S(1)}, bf16[128,512]{1,0:T(8,128)(2,1)S(1)}, u32[]{:S(2)}, u32[]{:S(2)}) collective-permute-start(bf16[128,512]{1,0:T(8,128)(2,1)S(1)} %get-tuple-element.68), channel_id=1, source_target_pairs={{0,8},{2,10},{4,12},{6,14},{8,0},{10,2},{12,4},{14,6},{16,24},{18,... | collective-permute-start | bytes 393224 | tf_op jit(solution)/shard_map/ppermute | solution.py:24
  67.6 8.4 %collective-permute-start.29 = (bf16[128,512]{1,0:T(8,128)(2,1)S(1)}, bf16[128,512]{1,0:T(8,128)(2,1)S(1)}, u32[]{:S(2)}, u32[]{:S(2)}) collective-permute-start(bf16[128,512]{1,0:T(8,128)(2,1)S(1)} %shard_map.129), channel_id=1, source_target_pairs={{0,16},{2,18},{4,20},{6,22},{8,24},{10,26},{12,28},{14,30},{16,0},... | collective-permute-start | bytes 393224 | tf_op jit(solution)/shard_map/ppermute | solution.py:24
  67.8 4.3 %collective-permute-start.25 = (bf16[128,256]{1,0:T(8,128)(2,1)S(1)}, bf16[128,256]{1,0:T(8,128)(2,1)S(1)}, u32[]{:S(2)}, u32[]{:S(2)}) collective-permute-start(bf16[128,256]{1,0:T(8,128)(2,1)S(1)} %get-tuple-element.64), channel_id=1, source_target_pairs={{0,1},{1,0},{2,3},{3,2},{4,5},{5,4},{6,7},{7,6},{8,9},{9,8},{10,11... | collective-permute-start | bytes 196616 | tf_op jit(solution)/shard_map/ppermute | solution.py:24
  74.0 5.0 %collective-permute-start.19 = (bf16[128,512]{1,0:T(8,128)(2,1)S(1)}, bf16[128,512]{1,0:T(8,128)(2,1)S(1)}, u32[]{:S(2)}, u32[]{:S(2)}) collective-permute-start(bf16[128,512]{1,0:T(8,128)(2,1)S(1)} %get-tuple-element.54.refs_0_), channel_id=1, source_target_pairs={{0,1},{1,0},{2,3},{3,2},{4,5},{5,4},{6,7},{7,6},{8,9},{9,8},{10,11... | collective-permute-start | bytes 393224 | tf_op jit(solution)/shard_map/ppermute | solution.py:24
